TPU v7x, 32 devices: a whole 2x2x4 slice. The times are simulated.
32 devices in a mesh: sp: 4 (over y, core), tp: 8 (over z, x).
Axes of the slice: x: 2, y: 2, z: 4, core: 2. Of those that a mesh axis runs over, the one named last changes fastest.
Arguments:
- latent: bfloat16 [960, 2048], P(('sp', 'tp')), may hold values from -40 to 40
- context: bfloat16 [768, 2048], P('sp'), may hold values from -6 to 6
- cond_latent: float32 [2048], P('sp'), may hold values from -6 to 6
- cond_context: float32 [2048], P('sp'), may hold values from -6 to 6
- mod_weight: bfloat16 [2048, 6144], P('sp', 'tp'), may hold values from -0.125 to 0.125
- w_query: bfloat16 [2048, 1024], P(None, 'tp'), may hold values from -5 to 5
- w_key: bfloat16 [2048, 1024], P(None, 'tp'), may hold values from -5 to 5
- w_value: bfloat16 [2048, 1024], P(None, 'tp'), may hold values from -0.125 to 0.125
- w_out: bfloat16 [1024, 2048], P('tp'), may hold values from -0.1875 to 0.1875
- head_lambda: float32 [8], P('tp'), may hold values from 0.3 to 0.8
Outputs:
- mixed_latent: bfloat16 [960, 2048], P(('sp', 'tp'))
All inputs are finite; a program needn't handle non-finite values.
Results may differ from a plain program's by a relative error of at most 0.011.
Values may be sent and summed in bfloat16 or wider, within the bound.
No kernel may reach another device: no remote copies, remote signals or barrier semaphores. Data moves between devices by JAX's collectives and lax.ppermute only.
A program may use at most 64 MiB of HBM per device.

v0:
```python
import functools

import jax
import jax.numpy as jnp
import numpy as np
from jax import lax
from jax.experimental import pallas as pl
from jax.experimental.pallas import tpu as pltpu
from jax.sharding import PartitionSpec as P

QK_DIM = 64
VAL_DIM = 128
GRID_W = 64

NORM_EPS = 0.01
HEAD_EPS = 0.001
THETA = 10000.0

F32 = jnp.float32
BF16 = jnp.bfloat16
VMEM = pl.BlockSpec(memory_space=pltpu.VMEM)
SMEM = pl.BlockSpec(memory_space=pltpu.SMEM)
HBM = pl.BlockSpec(memory_space=pltpu.HBM)


def ahead(i, k, n):
    return i ^ k if n & (n - 1) == 0 else (i + k) % n


def behind(i, k, n):
    return i ^ k if n & (n - 1) == 0 else (i - k) % n


def split_of(size):
    inner = max(d for d in range(1, size + 1) if size % d == 0 and d * d <= size)
    return size // inner, inner


def size_of(v):
    return int(np.prod(v.shape)) * jnp.dtype(v.dtype).itemsize


def call(body, outs, *args, scratch=(), extra=0, local=False, flops=2000000, in_specs=None):
    held = sum(size_of(v) for v in args) + sum(size_of(v) for v in jax.tree.leaves(outs))
    held += sum(size_of(v) for v in scratch if hasattr(v, "dtype") and v.dtype in (F32, BF16))
    limit = min(60 * 1024 * 1024, held + extra + 6 * 1024 * 1024)
    in_specs = in_specs or [VMEM] * len(args)
    args = [
        pltpu.with_memory_space_constraint(v, pltpu.HBM) if spec is HBM else v
        for v, spec in zip(args, in_specs)
    ]
    if local:
        outs = jax.tree.map(lambda v: pltpu.VMEM(v.shape, v.dtype), outs)
    return pl.pallas_call(
        body,
        out_shape=outs,
        in_specs=in_specs,
        out_specs=jax.tree.map(lambda _: VMEM, outs),
        scratch_shapes=list(scratch),
        compiler_params=pltpu.CompilerParams(vmem_limit_bytes=limit),
        cost_estimate=pl.CostEstimate(flops=flops, bytes_accessed=0, transcendentals=0),
    )(*args)


def sds(shape, dtype):
    return jax.ShapeDtypeStruct(shape, dtype)


def partial_body(latent_hbm, context_hbm, weight_hbm, out_ref, cond_ref, weight_ref, sems):
    moves = [
        pltpu.make_async_copy(weight_hbm, weight_ref, sems.at[0]),
        pltpu.make_async_copy(latent_hbm, cond_ref.at[0:1], sems.at[1]),
        pltpu.make_async_copy(context_hbm, cond_ref.at[1:2], sems.at[2]),
    ]
    for move in moves:
        move.start()
    moves[1].wait()
    moves[2].wait()
    rows = cond_ref[...]
    rows = (rows / (1.0 + jnp.exp(-rows))).astype(BF16)
    moves[0].wait()
    part = jnp.dot(rows, weight_ref[...], preferred_element_type=F32)
    for i in range(out_ref.shape[0]):
        out_ref[i] = part


def table_body(number, pad, ranks, outer, inner, *refs):
    here_ref = refs[0]
    sources, (out_ref, weight_ref, sems) = refs[1:4], refs[4:]
    moves = fetch_weights(sources, weight_ref, sems)
    here = here_ref[0]
    group, rank = lax.div(here, ranks), lax.rem(here, ranks)
    here_outer, here_inner = lax.div(rank, inner), lax.rem(rank, inner)
    lane = lax.broadcasted_iota(jnp.int32, (pad, 2 * QK_DIM), 1)
    line = lax.broadcasted_iota(jnp.int32, (pad, 2 * QK_DIM), 0)
    low = lane < QK_DIM
    by_row = (lane & (QK_DIM - 1)) < QK_DIM // 2
    sign = jnp.where((lane & (QK_DIM // 4)) == 0, -1.0, 1.0)
    phase = jnp.where(low, np.float32(np.pi / 2), np.float32(0))
    shift = GRID_W.bit_length() - 1
    quarter = QK_DIM // 4
    inverse = jnp.ones(lane.shape, F32)
    for i in range(1, quarter):
        inverse = jnp.where((lane & (quarter - 1)) == i, np.float32(THETA ** (-i / quarter)), inverse)

    def owner(i, k, n):
        return i ^ k if n & (n - 1) == 0 else lax.rem(i + (n - k), n)

    for j in range(inner):
        for k in range(outer):
            rank_at = owner(here_outer, k, outer) * inner + owner(here_inner, j, inner)
            position = line + (group * ranks + rank_at) * number
            place = jnp.where(by_row, position >> shift, position & (GRID_W - 1)).astype(F32)
            wave = jnp.sin(place * inverse + phase)
            other = pltpu.roll(wave, QK_DIM, 1)
            out_ref[j, 0, k * pad : (k + 1) * pad, :] = jnp.where(low, wave, other)
            out_ref[j, 1, k * pad : (k + 1) * pad, :] = jnp.where(low, other, wave) * sign
    for move in moves:
        move.wait()


def fetch_weights(sources, weight_ref, sems):
    moves, start = [], 0
    for i, source in enumerate(sources):
        columns = source.shape[1]
        moves.append(
            pltpu.make_async_copy(source, weight_ref.at[:, start : start + columns], sems.at[i])
        )
        moves[-1].start()
        start += columns
    return moves


def modulated(values, shift, scale):
    values = values.astype(F32)
    mean = jnp.mean(values * values, axis=-1, keepdims=True)
    return (values * lax.rsqrt(mean + NORM_EPS) * scale + shift).astype(BF16)


def fill_rows(blocks, rows_ref, pad, shift, scale):
    number = blocks[0].shape[0]
    for k, block in enumerate(blocks):
        rows_ref[k * pad : k * pad + number, :] = modulated(block[...], shift, scale)
        if pad > number:
            rows_ref[k * pad + number : (k + 1) * pad, :] = jnp.zeros(
                (pad - number, rows_ref.shape[1]), BF16
            )


def turn(u, cosine, sine):
    lane = lax.broadcasted_iota(jnp.int32, u.shape, 1)
    quarter = QK_DIM // 4
    width = u.shape[1]
    even = (lane // quarter) % 2 == 0
    turned = jnp.where(even, pltpu.roll(u, width - quarter, 1), pltpu.roll(u, quarter, 1))
    return (u * cosine + turned * sine).astype(BF16)


def project_rows(rows, weight_ref, table_ref, j, q_ref, kv_ref):
    number = rows.shape[0]
    wide = 2 * QK_DIM
    cosine, sine = table_ref[j, 0], table_ref[j, 1]
    u = jnp.dot(rows, weight_ref[...], preferred_element_type=F32)
    q_ref[...] = turn(u[:, :wide], cosine, sine)
    kv_ref[0:number, :wide] = turn(u[:, wide : 2 * wide], cosine, sine)
    kv_ref[0:number, wide:] = u[:, 2 * wide :].astype(BF16)


def first_body(pad, ranks, count, *refs):
    pieces_ref, context_ref, table_ref, weight_ref = refs[:4]
    blocks = refs[4 : 4 + count]
    mod_ref, q_ref, kv_ref, rows_ref, ctx_ref = refs[4 + count :]
    width = context_ref.shape[1]
    columns = pieces_ref.shape[2]
    groups = pieces_ref.shape[0] // ranks
    for t in range(ranks):
        total = pieces_ref[t]
        for s in range(1, groups):
            total = total + pieces_ref[s * ranks + t]
        mod_ref[:, t * columns : (t + 1) * columns] = total
    mod = mod_ref[...]
    shift, scale = mod[1:2, :width], 1.0 + mod[1:2, width : 2 * width]
    held = context_ref.shape[0]
    step = 16 if held % 16 == 0 else held
    for i in range(0, held, step):
        ctx_ref[i : i + step, :] = modulated(context_ref[i : i + step, :], shift, scale)
    fill_rows(blocks, rows_ref, pad, mod[0:1, :width], 1.0 + mod[0:1, width : 2 * width])
    base = count * pad
    wide = 2 * QK_DIM
    kv_ref[base : base + held, :] = jnp.dot(
        ctx_ref[...], weight_ref[:, wide:], preferred_element_type=F32
    ).astype(BF16)
    project_rows(rows_ref[...], weight_ref, table_ref, 0, q_ref, kv_ref)


def second_body(pad, count, j, *refs):
    mod_ref, table_ref, weight_ref = refs[:3]
    blocks = refs[3 : 3 + count]
    q_ref, kv_ref, rows_ref = refs[3 + count :]
    width = blocks[0].shape[1]
    fill_rows(
        blocks, rows_ref, pad, mod_ref[0:1, :width], 1.0 + mod_ref[0:1, width : 2 * width]
    )
    project_rows(rows_ref[...], weight_ref, table_ref, j, q_ref, kv_ref)


def attend_body(number, pad, outer, inner, members, *refs):
    factor_ref = refs[0]
    q_refs = refs[1 : 1 + inner]
    kv_refs = refs[1 + inner : 1 + inner + inner * members]
    out_ref, q_all, k_all, v_all = refs[1 + inner + inner * members :]
    wide = 2 * QK_DIM
    tile = outer * pad
    for j in range(inner):
        q_all[j] = q_refs[j][...] * jnp.asarray(QK_DIM ** (-0.5), BF16)
    row = 0
    for piece in kv_refs:
        k_all[row : row + tile, :] = piece[0:tile, :wide]
        v_all[row : row + tile, :] = piece[0:tile, wide:]
        row += tile
    latents = row
    for piece in kv_refs[:members]:
        held = piece.shape[0] - tile
        k_all[row : row + held, :] = piece[tile : tile + held, :wide]
        v_all[row : row + held, :] = piece[tile : tile + held, wide:]
        row += held
    column = lax.broadcasted_iota(jnp.int32, (1, row), 1)
    valid = (column >= latents) | (column % pad < number)
    bias = jnp.where(valid, 0.0, -1e30)
    lane = lax.broadcasted_iota(jnp.int32, (tile, wide), 1)

    def one(j, carry):
        queries = q_all[j]
        mixed = []
        for m in range(2):
            own = jnp.where((lane // QK_DIM) == m, queries, jnp.zeros_like(queries))
            scores = lax.dot_general(
                own, k_all[...], (((1,), (1,)), ((), ())), preferred_element_type=F32
            )
            scores = scores + bias
            highest = jnp.max(scores, axis=-1, keepdims=True)
            weights = jnp.exp(scores - highest)
            totals = jnp.sum(weights, axis=-1, keepdims=True)
            mix = jnp.dot(weights.astype(BF16), v_all[...], preferred_element_type=F32)
            mixed.append(mix / totals)
        head = mixed[0] - factor_ref[0] * mixed[1]
        head = head * lax.rsqrt(jnp.mean(head * head, axis=-1, keepdims=True) + HEAD_EPS)
        head = head.astype(BF16)
        for k in range(outer):
            out_ref[k, j] = head[k * pad : (k + 1) * pad]
        return carry

    if inner <= 4:
        for j in range(inner):
            one(j, 0)
    else:
        lax.fori_loop(0, inner, one, 0)


def partial_out_body(share, outer, inner, pad, *refs):
    side_ref, weight_ref = refs[:2]
    mine = refs[2 : 1 + outer]
    theirs = refs[1 + outer : 1 + outer + (outer - 1) * (share - 1)]
    rest = refs[1 + outer + (outer - 1) * (share - 1) :]
    parts, own_ref, others = rest[:outer], rest[outer], rest[1 + outer :]
    rows = inner * pad
    half = VAL_DIM // share
    total = jnp.dot(
        parts[0][...].reshape(rows, VAL_DIM), weight_ref[...], preferred_element_type=F32
    )
    for k in range(1, outer):
        part = parts[k][...].reshape(rows, VAL_DIM)
        if share == 1:
            total += jnp.dot(part, mine[k - 1][...], preferred_element_type=F32)
            continue
        first = jnp.broadcast_to(side_ref[0], (rows, half)) == 0
        left, right = part[:, :half], part[:, half:]
        total += jnp.dot(
            jnp.where(first, left, right), mine[k - 1][...], preferred_element_type=F32
        )
        total += jnp.dot(
            jnp.where(first, right, left), theirs[k - 1][...], preferred_element_type=F32
        )
    own_ref[...] = total[:pad]
    for j in range(1, inner):
        others[j - 1][...] = total[j * pad : (j + 1) * pad].astype(BF16)


def final_body(count, *refs):
    latent_ref, mod_ref, own_ref = refs[:3]
    others = refs[3 : 3 + count]
    out_ref = refs[3 + count]
    number, width = out_ref.shape
    total = own_ref[...]
    for other in others:
        total = total + other[...].astype(F32)
    total = total[:number]
    total = total * lax.rsqrt(jnp.mean(total * total, axis=-1, keepdims=True) + NORM_EPS)
    gate = mod_ref[0:1, 2 * width :]
    out_ref[...] = (latent_ref[...].astype(F32) + gate * total).astype(BF16)


def shards(
    latent,
    context,
    cond_latent,
    cond_context,
    mod_weight,
    w_query,
    w_key,
    w_value,
    w_out,
    head_lambda,
):
    number, width = latent.shape
    groups, ranks = lax.axis_size("sp"), lax.axis_size("tp")
    outer, inner = split_of(ranks)
    pad = -(-number // 16) * 16
    wide = 2 * QK_DIM
    tile = outer * pad
    held = context.shape[0]
    here_sp, here_tp = lax.axis_index("sp"), lax.axis_index("tp")

    def along_outer(value, k, way):
        pairs = [
            (o * inner + i, way(o, k, outer) * inner + i)
            for o in range(outer)
            for i in range(inner)
        ]
        return lax.ppermute(value, "tp", pairs)

    def along_inner(value, j, way):
        pairs = [
            (o * inner + i, o * inner + way(i, j, inner))
            for o in range(outer)
            for i in range(inner)
        ]
        return lax.ppermute(value, "tp", pairs)

    def along_sp(value, s):
        return lax.ppermute(value, "sp", [(i, ahead(i, s, groups)) for i in range(groups)])

    columns = mod_weight.shape[1]
    copies = call(
        partial_body,
        sds((groups * ranks, 2, columns), F32),
        cond_latent.reshape(1, -1),
        cond_context.reshape(1, -1),
        mod_weight,
        scratch=[
            pltpu.VMEM((2, cond_latent.shape[0]), F32),
            pltpu.VMEM(mod_weight.shape, BF16),
            pltpu.SemaphoreType.DMA((3,)),
        ],
        in_specs=[HBM] * 3,
        local=True,
    )
    pieces = lax.all_to_all(copies, ("sp", "tp"), 0, 0)

    blocks = {(0, 0): latent}
    for k in range(1, outer):
        blocks[k, 0] = along_outer(latent, k, ahead)
    for j in range(1, inner):
        for k in range(outer):
            blocks[k, j] = along_inner(blocks[k, 0], j, ahead)

    here = (here_sp * ranks + here_tp).astype(jnp.int32).reshape(1)
    joined = wide + wide + VAL_DIM
    table, weight = call(
        functools.partial(table_body, number, pad, ranks, outer, inner),
        (sds((inner, 2, tile, wide), F32), sds((width, joined), BF16)),
        here,
        w_query,
        w_key,
        w_value,
        scratch=[pltpu.SemaphoreType.DMA((3,))],
        in_specs=[SMEM] + [HBM] * 3,
        local=True,
    )
    mod, q_first, kv_first = call(
        functools.partial(first_body, pad, ranks, outer),
        (
            sds((2, columns * ranks), F32),
            sds((tile, wide), BF16),
            sds((tile + held, wide + VAL_DIM), BF16),
        ),
        pieces,
        context,
        table,
        weight,
        *[blocks[k, 0] for k in range(outer)],
        scratch=[pltpu.VMEM((tile, width), BF16), pltpu.VMEM((held, width), BF16)],
    )
    queries, kv = [q_first], [kv_first]
    for j in range(1, inner):
        q_next, kv_next = call(
            functools.partial(second_body, pad, outer, j),
            (sds((tile, wide), BF16), sds((tile, wide + VAL_DIM), BF16)),
            mod,
            table,
            weight,
            *[blocks[k, j] for k in range(outer)],
            scratch=[pltpu.VMEM((tile, width), BF16)],
        )
        queries.append(q_next)
        kv.append(kv_next)
    pieces_kv = []
    for part in kv:
        pieces_kv.append(part)
        for s in range(1, groups):
            pieces_kv.append(along_sp(part, s))
    keys = groups * (inner * tile + held)
    attended = call(
        functools.partial(attend_body, number, pad, outer, inner, groups),
        sds((outer, inner, pad, VAL_DIM), BF16),
        head_lambda,
        *queries,
        *pieces_kv,
        scratch=[
            pltpu.VMEM((inner, tile, wide), BF16),
            pltpu.VMEM((keys, wide), BF16),
            pltpu.VMEM((keys, VAL_DIM), BF16),
        ],
        extra=tile * keys * 12,
        in_specs=[SMEM] + [VMEM] * (inner + inner * groups),
    )
    parts = [attended[0]]
    for k in range(1, outer):
        parts.append(along_outer(attended[k], k, behind))

    share = 2 if groups % 2 == 0 else 1
    depth = w_out.shape[0]
    side = here_sp % share
    half = lax.dynamic_slice(w_out, (side * (depth // share), 0), (depth // share, width))
    swap = [(i, i ^ 1) for i in range(groups)]
    mine, theirs = [], []
    for k in range(1, outer):
        mine.append(along_outer(half, k, behind))
        if share > 1:
            theirs.append(lax.ppermute(mine[-1], "sp", swap))
    total = call(
        functools.partial(partial_out_body, share, outer, inner, pad),
        (sds((pad, width), F32),) + (sds((pad, width), BF16),) * (inner - 1),
        side.reshape(1).astype(jnp.int32),
        w_out,
        *mine,
        *theirs,
        *parts,
        in_specs=[SMEM] + [VMEM] * (1 + len(mine) + len(theirs) + outer),
    )
    arrived = []
    for j in range(1, inner):
        arrived.append(along_inner(total[j], j, behind))
    return call(
        functools.partial(final_body, inner - 1),
        sds((number, width), BF16),
        latent,
        mod,
        total[0],
        *arrived,
    )


def solution(mesh):
    placed = (
        P(("sp", "tp"), None),
        P("sp", None),
        P("sp"),
        P("sp"),
        P("sp", "tp"),
        P(None, "tp"),
        P(None, "tp"),
        P(None, "tp"),
        P("tp", None),
        P("tp"),
    )
    return jax.shard_map(
        shards, mesh=mesh, in_specs=placed, out_specs=P(("sp", "tp"), None), check_vma=False
    )
```

profile of v0, /device:TPU:0, one launch (start us, length us, event | category | flops | bytes accessed | tf_op | source)
XLA Modules:
  0.0 68.3 jit_solution(195636807526704099)
XLA Ops:
  0.0 3.1 %collective-permute-start = (bf16[30,2048]{1,0:T(8,128)(2,1)}, bf16[30,2048]{1,0:T(8,128)(2,1)S(1)}, u32[]{:S(2)}, u32[]{:S(2)}) collective-permute-start(bf16[30,2048]{1,0:T(8,128)(2,1)} %refs_0_.2), channel_id=1, source_target_pairs={{0,2},{1,3},{2,0},{3,1},{4,6},{5,7},{6,4},{7,5},{8,10},{9,11},{10,... | collective-permute-start | bytes 368648 | tf_op jit(solution)/shard_map/ppermute | solution.py:330
  3.1 2.6 %collective-permute-start.1 = (bf16[30,2048]{1,0:T(8,128)(2,1)}, bf16[30,2048]{1,0:T(8,128)(2,1)}, u32[]{:S(2)}, u32[]{:S(2)}) collective-permute-start(bf16[30,2048]{1,0:T(8,128)(2,1)} %refs_0_.2), channel_id=1, source_target_pairs={{0,4},{1,5},{2,6},{3,7},{4,0},{5,1},{6,2},{7,3},{8,12},{9,13},{10,... | collective-permute-start | bytes 368648 | tf_op jit(solution)/shard_map/ppermute | solution.py:330
  5.6 1.7 %collective-permute-start.9 = (bf16[30,2048]{1,0:T(8,128)(2,1)}, bf16[30,2048]{1,0:T(8,128)(2,1)S(1)}, u32[]{:S(2)}, u32[]{:S(2)}) collective-permute-start(bf16[30,2048]{1,0:T(8,128)(2,1)} %refs_0_.2), channel_id=1, source_target_pairs={{0,1},{1,0},{2,3},{3,2},{4,5},{5,4},{6,7},{7,6},{8,9},{9,8},{10,11... | collective-permute-start | bytes 368648 | tf_op jit(solution)/shard_map/ppermute | solution.py:338
  7.4 2.2 %shard_map.100 = f32[32,2,768]{2,1,0:T(2,128)} custom-call(f32[1,512]{1,0:T(1,128)} %bitcast.12, f32[1,512]{1,0:T(1,128)} %bitcast.13, bf16[512,768]{1,0:T(8,128)(2,1)} %weight_hbm.1), custom_call_target="tpu_custom_call" | custom-call | flops 2000000 | tf_op jit(solution)/shard_map/pallas_call | solution.py:54
  9.5 4.9 %all-to-all-start = ((f32[32,2,768]{2,1,0:T(2,128)}), f32[32,2,768]{2,1,0:T(2,128)S(1)}, u32[]{:S(2)}, u32[]{:S(2)}) async-start(f32[32,2,768]{2,1,0:T(2,128)} %shard_map.100), calls=%async_computation | async-start | bytes 393216 | tf_op jit(solution)/shard_map/all_to_all | solution.py:358
  15.2 1.8 %collective-permute-start.3 = (bf16[64,2048]{1,0:T(8,128)(2,1)}, bf16[64,2048]{1,0:T(8,128)(2,1)}, u32[]{:S(2)}, u32[]{:S(2)}) collective-permute-start(bf16[64,2048]{1,0:T(8,128)(2,1)} %constant_dynamic-slice_fusion), channel_id=1, source_target_pairs={{0,2},{1,3},{2,0},{3,1},{4,6},{5,7},{6,4},{7,5},{8,10},{9,11},{10,... | collective-permute-start | bytes 786440 | tf_op jit(solution)/shard_map/ppermute | solution.py:330
  17.0 2.4 %collective-permute-start.4 = (bf16[64,2048]{1,0:T(8,128)(2,1)}, bf16[64,2048]{1,0:T(8,128)(2,1)}, u32[]{:S(2)}, u32[]{:S(2)}) collective-permute-start(bf16[64,2048]{1,0:T(8,128)(2,1)} %constant_dynamic-slice_fusion), channel_id=1, source_target_pairs={{0,4},{1,5},{2,6},{3,7},{4,0},{5,1},{6,2},{7,3},{8,12},{9,13},{10,... | collective-permute-start | bytes 786440 | tf_op jit(solution)/shard_map/ppermute | solution.py:330
  19.4 1.5 %collective-permute-start.10 = (bf16[30,2048]{1,0:T(8,128)(2,1)S(1)}, bf16[30,2048]{1,0:T(8,128)(2,1)S(1)}, u32[]{:S(2)}, u32[]{:S(2)}) collective-permute-start(bf16[30,2048]{1,0:T(8,128)(2,1)S(1)} %collective-permute-done.refs_5_), channel_id=1, source_target_pairs={{0,1},{1,0},{2,3},{3,2},{4,5},{5,4},{6,7},{7,6},{8,9},{9,8},{10,11... | collective-permute-start | bytes 368648 | tf_op jit(solution)/shard_map/ppermute | solution.py:338
  22.9 1.9 %collective-permute-done.10.refs_4_ = bf16[30,2048]{1,0:T(8,128)(2,1)S(1)} collective-permute-done((bf16[30,2048]{1,0:T(8,128)(2,1)S(1)}, bf16[30,2048]{1,0:T(8,128)(2,1)S(1)}, u32[]{:S(2)}, u32[]{:S(2)}) %collective-permute-start.10) | collective-permute-done | bytes 122912 | tf_op jit(solution)/shard_map/ppermute | solution.py:338
  25.5 2.5 %collective-permute-start.12 = (bf16[30,2048]{1,0:T(8,128)(2,1)}, bf16[30,2048]{1,0:T(8,128)(2,1)}, u32[]{:S(2)}, u32[]{:S(2)}) collective-permute-start(bf16[30,2048]{1,0:T(8,128)(2,1)} %collective-permute-done.2.refs_7_), channel_id=1, source_target_pairs={{0,1},{1,0},{2,3},{3,2},{4,5},{5,4},{6,7},{7,6},{8,9},{9,8},{10,11... | collective-permute-start | bytes 368648 | tf_op jit(solution)/shard_map/ppermute | solution.py:338
  27.9 1.4 %shard_map.101 = (f32[2,2,128,128]{3,2,1,0:T(8,128)S(1)}, bf16[2048,384]{1,0:T(8,128)(2,1)S(1)}) custom-call(s32[1]{0:T(128)} %bitcast.2.refs_0_, bf16[2048,128]{1,0:T(8,128)(2,1)} %refs_1_.3, bf16[2048,128]{1,0:T(8,128)(2,1)} %refs_2_.1, bf16[2048,128]{1,0:T(8,128)(2,1)} %refs_3_.1), custom_call_target="tpu_custom_call" | custom-call | flops 2000000 | tf_op jit(solution)/shard_map/pallas_call | solution.py:54
  30.3 2.0 %shard_map.102 = (f32[2,6144]{1,0:T(2,128)S(1)}, bf16[128,128]{1,0:T(8,128)(2,1)S(1)}, bf16[320,256]{1,0:T(8,128)(2,1)S(1)}) custom-call(f32[32,2,768]{2,1,0:T(2,128)S(1)} %all-to-all-done.refs_0_, bf16[192,2048]{1,0:T(8,128)(2,1)S(1)} %copy-done.1, f32[2,2,128,128]{3,2,1,0:T(8,128)S(1)} %get-tuple-element.14.refs_2_.refs_1_, ...), custom_call_target="tpu_custom_call" | custom-call | flops 2000000 | tf_op jit(solution)/shard_map/pallas_call | solution.py:54
  32.4 1.6 %collective-permute-start.14 = (bf16[320,256]{1,0:T(8,128)(2,1)S(1)}, bf16[320,256]{1,0:T(8,128)(2,1)S(1)}, u32[]{:S(2)}, u32[]{:S(2)}) collective-permute-start(bf16[320,256]{1,0:T(8,128)(2,1)S(1)} %get-tuple-element.19.refs_3_), channel_id=1, source_target_pairs={{0,16},{8,24},{16,0},{24,8},{1,17},{9,25},{17,1},{25,9},{2,18},{10... | collective-permute-start | bytes 491528 | tf_op jit(solution)/shard_map/ppermute | solution.py:341
  34.3 1.7 %shard_map.103 = (bf16[128,128]{1,0:T(8,128)(2,1)S(1)}, bf16[128,256]{1,0:T(8,128)(2,1)S(1)}) custom-call(f32[2,6144]{1,0:T(2,128)S(1)} %get-tuple-element.16.refs_0_.refs_1_, f32[2,2,128,128]{3,2,1,0:T(8,128)S(1)} %get-tuple-element.14.refs_2_.refs_1_, bf16[2048,384]{1,0:T(8,128)(2,1)S(1)} %get-tuple-element.15.refs_3_.refs_2_, ...), custom_call_target="tpu_custom_call" | custom-call | flops 2000000 | tf_op jit(solution)/shard_map/pallas_call | solution.py:54
  36.0 4.0 %collective-permute-done.4.refs_3_ = bf16[64,2048]{1,0:T(8,128)(2,1)} collective-permute-done((bf16[64,2048]{1,0:T(8,128)(2,1)}, bf16[64,2048]{1,0:T(8,128)(2,1)}, u32[]{:S(2)}, u32[]{:S(2)}) %collective-permute-start.4) | collective-permute-done | bytes 262176 | tf_op jit(solution)/shard_map/ppermute | solution.py:330
  39.9 1.5 %collective-permute-start.17 = (bf16[128,256]{1,0:T(8,128)(2,1)S(1)}, bf16[128,256]{1,0:T(8,128)(2,1)S(1)}, u32[]{:S(2)}, u32[]{:S(2)}) collective-permute-start(bf16[128,256]{1,0:T(8,128)(2,1)S(1)} %get-tuple-element.20.refs_7_), channel_id=1, source_target_pairs={{0,16},{8,24},{16,0},{24,8},{1,17},{9,25},{17,1},{25,9},{2,18},{10... | collective-permute-start | bytes 196616 | tf_op jit(solution)/shard_map/ppermute | solution.py:341
  42.4 2.0 %collective-permute-done.17.refs_9_ = bf16[128,256]{1,0:T(8,128)(2,1)S(1)} collective-permute-done((bf16[128,256]{1,0:T(8,128)(2,1)S(1)}, bf16[128,256]{1,0:T(8,128)(2,1)S(1)}, u32[]{:S(2)}, u32[]{:S(2)}) %collective-permute-start.17) | collective-permute-done | bytes 65568 | tf_op jit(solution)/shard_map/ppermute | solution.py:341
  46.7 2.2 %shard_map.104 = bf16[4,2,32,128]{3,2,1,0:T(8,128)(2,1)S(1)} custom-call(f32[1]{0:T(128)S(6)} %copy.11.refs_0_, bf16[128,128]{1,0:T(8,128)(2,1)S(1)} %get-tuple-element.17.refs_1_, bf16[128,128]{1,0:T(8,128)(2,1)S(1)} %get-tuple-element.18.refs_2_, bf16[320,256]{1,0:T(8,128)(2,1)S(1)} %get-tuple-element.19.refs_3_, ...), custom_call_target="tpu_custom_call" | custom-call | flops 2000000 | tf_op jit(solution)/shard_map/pallas_call | solution.py:54
  48.9 5.8 %collective-permute-start.19 = (bf16[2,32,128]{2,1,0:T(8,128)(2,1)S(1)}, bf16[2,32,128]{2,1,0:T(8,128)(2,1)S(1)}, u32[]{:S(2)}, u32[]{:S(2)}) collective-permute-start(bf16[2,32,128]{2,1,0:T(8,128)(2,1)S(1)} %get-tuple-element.25), channel_id=1, source_target_pairs={{0,2},{1,3},{2,0},{3,1},{4,6},{5,7},{6,4},{7,5},{8,10},{9,11},{10,... | collective-permute-start | bytes 49160 | tf_op jit(solution)/shard_map/ppermute | solution.py:330
  55.2 1.9 %collective-permute-start.21 = (bf16[2,32,128]{2,1,0:T(8,128)(2,1)S(1)}, bf16[2,32,128]{2,1,0:T(8,128)(2,1)S(1)}, u32[]{:S(2)}, u32[]{:S(2)}) collective-permute-start(bf16[2,32,128]{2,1,0:T(8,128)(2,1)S(1)} %get-tuple-element.23), channel_id=1, source_target_pairs={{0,6},{1,7},{2,4},{3,5},{4,2},{5,3},{6,0},{7,1},{8,14},{9,15},{10,... | collective-permute-start | bytes 49160 | tf_op jit(solution)/shard_map/ppermute | solution.py:330
  57.1 2.4 %collective-permute-done.20.refs_10_ = bf16[2,32,128]{2,1,0:T(8,128)(2,1)S(1)} collective-permute-done((bf16[2,32,128]{2,1,0:T(8,128)(2,1)S(1)}, bf16[2,32,128]{2,1,0:T(8,128)(2,1)S(1)}, u32[]{:S(2)}, u32[]{:S(2)}) %collective-permute-start.20) | collective-permute-done | bytes 16416 | tf_op jit(solution)/shard_map/ppermute | solution.py:330
  60.7 1.8 %shard_map.105 = (f32[32,2048]{1,0:T(8,128)S(1)}, bf16[32,2048]{1,0:T(8,128)(2,1)S(1)}) custom-call(s32[1]{0:T(128)} %bitcast.3.refs_0_, bf16[128,2048]{1,0:T(8,128)(2,1)S(1)} %copy-done, bf16[64,2048]{1,0:T(8,128)(2,1)} %collective-permute-done.3.refs_2_, bf16[64,2048]{1,0:T(8,128)(2,1)} %collective-permute-done.4.refs_3_, ...), custom_call_target="tpu_custom_call" | custom-call | flops 2000000 | tf_op jit(solution)/shard_map/pallas_call | solution.py:54
  62.5 1.6 %collective-permute-start.22 = (bf16[32,2048]{1,0:T(8,128)(2,1)S(1)}, bf16[32,2048]{1,0:T(8,128)(2,1)S(1)}, u32[]{:S(2)}, u32[]{:S(2)}) collective-permute-start(bf16[32,2048]{1,0:T(8,128)(2,1)S(1)} %get-tuple-element.22), channel_id=1, source_target_pairs={{0,1},{1,0},{2,3},{3,2},{4,5},{5,4},{6,7},{7,6},{8,9},{9,8},{10,11... | collective-permute-start | bytes 393224 | tf_op jit(solution)/shard_map/ppermute | solution.py:338
  64.1 3.5 %collective-permute-done.22.refs_3_ = bf16[32,2048]{1,0:T(8,128)(2,1)S(1)} collective-permute-done((bf16[32,2048]{1,0:T(8,128)(2,1)S(1)}, bf16[32,2048]{1,0:T(8,128)(2,1)S(1)}, u32[]{:S(2)}, u32[]{:S(2)}) %collective-permute-start.22) | collective-permute-done | bytes 131104 | tf_op jit(solution)/shard_map/ppermute | solution.py:338
  (51 shorter events, 9.8 us)
Async XLA Ops:
  0.0 17.0 %collective-permute-start = (bf16[30,2048]{1,0:T(8,128)(2,1)}, bf16[30,2048]{1,0:T(8,128)(2,1)S(1)}, u32[]{:S(2)}, u32[]{:S(2)}) collective-permute-start(bf16[30,2048]{1,0:T(8,128)(2,1)} %refs_0_.2), channel_id=1, source_target_pairs={{0,2},{1,3},{2,0},{3,1},{4,6},{5,7},{6,4},{7,5},{8,10},{9,11},{10,... | collective-permute-start | bytes 368648 | tf_op jit(solution)/shard_map/ppermute | solution.py:330
  3.1 16.3 %collective-permute-start.1 = (bf16[30,2048]{1,0:T(8,128)(2,1)}, bf16[30,2048]{1,0:T(8,128)(2,1)}, u32[]{:S(2)}, u32[]{:S(2)}) collective-permute-start(bf16[30,2048]{1,0:T(8,128)(2,1)} %refs_0_.2), channel_id=1, source_target_pairs={{0,4},{1,5},{2,6},{3,7},{4,0},{5,1},{6,2},{7,3},{8,12},{9,13},{10,... | collective-permute-start | bytes 368648 | tf_op jit(solution)/shard_map/ppermute | solution.py:330
  5.6 15.9 %collective-permute-start.2 = (bf16[30,2048]{1,0:T(8,128)(2,1)}, bf16[30,2048]{1,0:T(8,128)(2,1)}, u32[]{:S(2)}, u32[]{:S(2)}) collective-permute-start(bf16[30,2048]{1,0:T(8,128)(2,1)} %refs_0_.2), channel_id=1, source_target_pairs={{0,6},{1,7},{2,4},{3,5},{4,2},{5,3},{6,0},{7,1},{8,14},{9,15},{10,... | collective-permute-start | bytes 368648 | tf_op jit(solution)/shard_map/ppermute | solution.py:330
  5.6 16.4 %collective-permute-start.9 = (bf16[30,2048]{1,0:T(8,128)(2,1)}, bf16[30,2048]{1,0:T(8,128)(2,1)S(1)}, u32[]{:S(2)}, u32[]{:S(2)}) collective-permute-start(bf16[30,2048]{1,0:T(8,128)(2,1)} %refs_0_.2), channel_id=1, source_target_pairs={{0,1},{1,0},{2,3},{3,2},{4,5},{5,4},{6,7},{7,6},{8,9},{9,8},{10,11... | collective-permute-start | bytes 368648 | tf_op jit(solution)/shard_map/ppermute | solution.py:338
  9.5 19.8 %all-to-all-start = ((f32[32,2,768]{2,1,0:T(2,128)}), f32[32,2,768]{2,1,0:T(2,128)S(1)}, u32[]{:S(2)}, u32[]{:S(2)}) async-start(f32[32,2,768]{2,1,0:T(2,128)} %shard_map.100), calls=%async_computation | async-start | bytes 393216 | tf_op jit(solution)/shard_map/all_to_all | solution.py:358
  15.2 18.8 %collective-permute-start.3 = (bf16[64,2048]{1,0:T(8,128)(2,1)}, bf16[64,2048]{1,0:T(8,128)(2,1)}, u32[]{:S(2)}, u32[]{:S(2)}) collective-permute-start(bf16[64,2048]{1,0:T(8,128)(2,1)} %constant_dynamic-slice_fusion), channel_id=1, source_target_pairs={{0,2},{1,3},{2,0},{3,1},{4,6},{5,7},{6,4},{7,5},{8,10},{9,11},{10,... | collective-permute-start | bytes 786440 | tf_op jit(solution)/shard_map/ppermute | solution.py:330
  17.0 22.9 %collective-permute-start.4 = (bf16[64,2048]{1,0:T(8,128)(2,1)}, bf16[64,2048]{1,0:T(8,128)(2,1)}, u32[]{:S(2)}, u32[]{:S(2)}) collective-permute-start(bf16[64,2048]{1,0:T(8,128)(2,1)} %constant_dynamic-slice_fusion), channel_id=1, source_target_pairs={{0,4},{1,5},{2,6},{3,7},{4,0},{5,1},{6,2},{7,3},{8,12},{9,13},{10,... | collective-permute-start | bytes 786440 | tf_op jit(solution)/shard_map/ppermute | solution.py:330
  19.4 5.4 %collective-permute-start.10 = (bf16[30,2048]{1,0:T(8,128)(2,1)S(1)}, bf16[30,2048]{1,0:T(8,128)(2,1)S(1)}, u32[]{:S(2)}, u32[]{:S(2)}) collective-permute-start(bf16[30,2048]{1,0:T(8,128)(2,1)S(1)} %collective-permute-done.refs_5_), channel_id=1, source_target_pairs={{0,1},{1,0},{2,3},{3,2},{4,5},{5,4},{6,7},{7,6},{8,9},{9,8},{10,11... | collective-permute-start | bytes 368648 | tf_op jit(solution)/shard_map/ppermute | solution.py:338
  21.5 18.4 %collective-permute-start.5 = (bf16[64,2048]{1,0:T(8,128)(2,1)}, bf16[64,2048]{1,0:T(8,128)(2,1)}, u32[]{:S(2)}, u32[]{:S(2)}) collective-permute-start(bf16[64,2048]{1,0:T(8,128)(2,1)} %constant_dynamic-slice_fusion), channel_id=1, source_target_pairs={{0,6},{1,7},{2,4},{3,5},{4,2},{5,3},{6,0},{7,1},{8,14},{9,15},{10,... | collective-permute-start | bytes 786440 | tf_op jit(solution)/shard_map/ppermute | solution.py:330
  22.7 9.6 %collective-permute-start.11 = (bf16[30,2048]{1,0:T(8,128)(2,1)}, bf16[30,2048]{1,0:T(8,128)(2,1)}, u32[]{:S(2)}, u32[]{:S(2)}) collective-permute-start(bf16[30,2048]{1,0:T(8,128)(2,1)} %collective-permute-done.1.refs_6_), channel_id=1, source_target_pairs={{0,1},{1,0},{2,3},{3,2},{4,5},{5,4},{6,7},{7,6},{8,9},{9,8},{10,11... | collective-permute-start | bytes 368648 | tf_op jit(solution)/shard_map/ppermute | solution.py:338
  25.5 6.9 %collective-permute-start.12 = (bf16[30,2048]{1,0:T(8,128)(2,1)}, bf16[30,2048]{1,0:T(8,128)(2,1)}, u32[]{:S(2)}, u32[]{:S(2)}) collective-permute-start(bf16[30,2048]{1,0:T(8,128)(2,1)} %collective-permute-done.2.refs_7_), channel_id=1, source_target_pairs={{0,1},{1,0},{2,3},{3,2},{4,5},{5,4},{6,7},{7,6},{8,9},{9,8},{10,11... | collective-permute-start | bytes 368648 | tf_op jit(solution)/shard_map/ppermute | solution.py:338
  32.3 13.3 %collective-permute-start.13 = (bf16[320,256]{1,0:T(8,128)(2,1)S(1)}, bf16[320,256]{1,0:T(8,128)(2,1)S(1)}, u32[]{:S(2)}, u32[]{:S(2)}) collective-permute-start(bf16[320,256]{1,0:T(8,128)(2,1)S(1)} %get-tuple-element.19.refs_3_), channel_id=1, source_target_pairs={{0,8},{8,0},{16,24},{24,16},{1,9},{9,1},{17,25},{25,17},{2,10},{10... | collective-permute-start | bytes 491528 | tf_op jit(solution)/shard_map/ppermute | solution.py:341
  32.4 14.2 %collective-permute-start.14 = (bf16[320,256]{1,0:T(8,128)(2,1)S(1)}, bf16[320,256]{1,0:T(8,128)(2,1)S(1)}, u32[]{:S(2)}, u32[]{:S(2)}) collective-permute-start(bf16[320,256]{1,0:T(8,128)(2,1)S(1)} %get-tuple-element.19.refs_3_), channel_id=1, source_target_pairs={{0,16},{8,24},{16,0},{24,8},{1,17},{9,25},{17,1},{25,9},{2,18},{10... | collective-permute-start | bytes 491528 | tf_op jit(solution)/shard_map/ppermute | solution.py:341
  34.0 12.7 %collective-permute-start.15 = (bf16[320,256]{1,0:T(8,128)(2,1)S(1)}, bf16[320,256]{1,0:T(8,128)(2,1)S(1)}, u32[]{:S(2)}, u32[]{:S(2)}) collective-permute-start(bf16[320,256]{1,0:T(8,128)(2,1)S(1)} %get-tuple-element.19.refs_3_), channel_id=1, source_target_pairs={{0,24},{8,16},{16,8},{24,0},{1,25},{9,17},{17,9},{25,1},{2,26},{10... | collective-permute-start | bytes 491528 | tf_op jit(solution)/shard_map/ppermute | solution.py:341
  39.9 1.5 %collective-permute-start.16 = (bf16[128,256]{1,0:T(8,128)(2,1)S(1)}, bf16[128,256]{1,0:T(8,128)(2,1)S(1)}, u32[]{:S(2)}, u32[]{:S(2)}) collective-permute-start(bf16[128,256]{1,0:T(8,128)(2,1)S(1)} %get-tuple-element.20.refs_7_), channel_id=1, source_target_pairs={{0,8},{8,0},{16,24},{24,16},{1,9},{9,1},{17,25},{25,17},{2,10},{10... | collective-permute-start | bytes 196616 | tf_op jit(solution)/shard_map/ppermute | solution.py:341
  39.9 4.5 %collective-permute-start.17 = (bf16[128,256]{1,0:T(8,128)(2,1)S(1)}, bf16[128,256]{1,0:T(8,128)(2,1)S(1)}, u32[]{:S(2)}, u32[]{:S(2)}) collective-permute-start(bf16[128,256]{1,0:T(8,128)(2,1)S(1)} %get-tuple-element.20.refs_7_), channel_id=1, source_target_pairs={{0,16},{8,24},{16,0},{24,8},{1,17},{9,25},{17,1},{25,9},{2,18},{10... | collective-permute-start | bytes 196616 | tf_op jit(solution)/shard_map/ppermute | solution.py:341
  41.4 4.1 %collective-permute-start.18 = (bf16[128,256]{1,0:T(8,128)(2,1)S(1)}, bf16[128,256]{1,0:T(8,128)(2,1)S(1)}, u32[]{:S(2)}, u32[]{:S(2)}) collective-permute-start(bf16[128,256]{1,0:T(8,128)(2,1)S(1)} %get-tuple-element.20.refs_7_), channel_id=1, source_target_pairs={{0,24},{8,16},{16,8},{24,0},{1,25},{9,17},{17,9},{25,1},{2,26},{10... | collective-permute-start | bytes 196616 | tf_op jit(solution)/shard_map/ppermute | solution.py:341
  44.5 10.7 %collective-permute-start.6 = (bf16[64,2048]{1,0:T(8,128)(2,1)}, bf16[64,2048]{1,0:T(8,128)(2,1)S(1)}, u32[]{:S(2)}, u32[]{:S(2)}) collective-permute-start(bf16[64,2048]{1,0:T(8,128)(2,1)} %collective-permute-done.3.refs_2_), channel_id=1, source_target_pairs={{0,8},{8,0},{16,24},{24,16},{1,9},{9,1},{17,25},{25,17},{2,10},{10... | collective-permute-start | bytes 786440 | tf_op jit(solution)/shard_map/ppermute | solution.py:440
  45.5 11.6 %collective-permute-start.7 = (bf16[64,2048]{1,0:T(8,128)(2,1)}, bf16[64,2048]{1,0:T(8,128)(2,1)S(1)}, u32[]{:S(2)}, u32[]{:S(2)}) collective-permute-start(bf16[64,2048]{1,0:T(8,128)(2,1)} %collective-permute-done.4.refs_3_), channel_id=1, source_target_pairs={{0,8},{8,0},{16,24},{24,16},{1,9},{9,1},{17,25},{25,17},{2,10},{10... | collective-permute-start | bytes 786440 | tf_op jit(solution)/shard_map/ppermute | solution.py:440
  45.7 11.4 %collective-permute-start.8 = (bf16[64,2048]{1,0:T(8,128)(2,1)}, bf16[64,2048]{1,0:T(8,128)(2,1)S(1)}, u32[]{:S(2)}, u32[]{:S(2)}) collective-permute-start(bf16[64,2048]{1,0:T(8,128)(2,1)} %collective-permute-done.5.refs_4_), channel_id=1, source_target_pairs={{0,8},{8,0},{16,24},{24,16},{1,9},{9,1},{17,25},{25,17},{2,10},{10... | collective-permute-start | bytes 786440 | tf_op jit(solution)/shard_map/ppermute | solution.py:440
  48.9 8.3 %collective-permute-start.19 = (bf16[2,32,128]{2,1,0:T(8,128)(2,1)S(1)}, bf16[2,32,128]{2,1,0:T(8,128)(2,1)S(1)}, u32[]{:S(2)}, u32[]{:S(2)}) collective-permute-start(bf16[2,32,128]{2,1,0:T(8,128)(2,1)S(1)} %get-tuple-element.25), channel_id=1, source_target_pairs={{0,2},{1,3},{2,0},{3,1},{4,6},{5,7},{6,4},{7,5},{8,10},{9,11},{10,... | collective-permute-start | bytes 49160 | tf_op jit(solution)/shard_map/ppermute | solution.py:330
  54.7 4.8 %collective-permute-start.20 = (bf16[2,32,128]{2,1,0:T(8,128)(2,1)S(1)}, bf16[2,32,128]{2,1,0:T(8,128)(2,1)S(1)}, u32[]{:S(2)}, u32[]{:S(2)}) collective-permute-start(bf16[2,32,128]{2,1,0:T(8,128)(2,1)S(1)} %get-tuple-element.24), channel_id=1, source_target_pairs={{0,4},{1,5},{2,6},{3,7},{4,0},{5,1},{6,2},{7,3},{8,12},{9,13},{10,... | collective-permute-start | bytes 49160 | tf_op jit(solution)/shard_map/ppermute | solution.py:330
  55.2 5.5 %collective-permute-start.21 = (bf16[2,32,128]{2,1,0:T(8,128)(2,1)S(1)}, bf16[2,32,128]{2,1,0:T(8,128)(2,1)S(1)}, u32[]{:S(2)}, u32[]{:S(2)}) collective-permute-start(bf16[2,32,128]{2,1,0:T(8,128)(2,1)S(1)} %get-tuple-element.23), channel_id=1, source_target_pairs={{0,6},{1,7},{2,4},{3,5},{4,2},{5,3},{6,0},{7,1},{8,14},{9,15},{10,... | collective-permute-start | bytes 49160 | tf_op jit(solution)/shard_map/ppermute | solution.py:330
  62.5 5.0 %collective-permute-start.22 = (bf16[32,2048]{1,0:T(8,128)(2,1)S(1)}, bf16[32,2048]{1,0:T(8,128)(2,1)S(1)}, u32[]{:S(2)}, u32[]{:S(2)}) collective-permute-start(bf16[32,2048]{1,0:T(8,128)(2,1)S(1)} %get-tuple-element.22), channel_id=1, source_target_pairs={{0,1},{1,0},{2,3},{3,2},{4,5},{5,4},{6,7},{7,6},{8,9},{9,8},{10,11... | collective-permute-start | bytes 393224 | tf_op jit(solution)/shard_map/ppermute | solution.py:338
  (9 other events, 69.3 us)
where the time goes:
time: 68.6 us; the launch traced here: 68.3 us
  starting transfers between devices  35.9 us (52%)
  waiting for transfers between devices  16 us (23%)
  Pallas kernels  12 us (17%)
  local copies, waits for them, and re-layouts  3.6 us (5%)
  between operations  0.84 us (1%)
    ppermute x9, starting transfers between devices, along_outer(): return lax.ppermute(value, 'tp', pairs)  18.6 us
    pallas_call x7, Pallas kernels, call(): pl.pallas_call(body, out_shape=outs, in_specs=in_specs, out_specs=jax.tre...  12 us
    ppermute x9, waiting for transfers between devices, along_outer(): return lax.ppermute(value, 'tp', pairs)  7.58 us
    ppermute x5, starting transfers between devices, along_inner(): return lax.ppermute(value, 'tp', pairs)  7.47 us
    ppermute x5, waiting for transfers between devices, along_inner(): return lax.ppermute(value, 'tp', pairs)  5.34 us
    all_to_all x1, starting transfers between devices, shards(): pieces = lax.all_to_all(copies, ('sp', 'tp'), 0, 0)  4.93 us
    ppermute x6, starting transfers between devices, along_sp(): lax.ppermute(value, 'sp', [(i, ahead(i, s, groups)) for i in range(groups)])  4.4 us
    ppermute x6, waiting for transfers between devices, along_sp(): lax.ppermute(value, 'sp', [(i, ahead(i, s, groups)) for i in range(groups)])  3.05 us
  transfers between devices with their start and end apart: 24, of which 7 were waited for; matrix products, arithmetic and copies ran while one was open for 1% of the time, Pallas kernels for 14%

commit v1 on v0

--- a/solution.py
+++ b/solution.py
@@ -20,6 +20,7 @@
 BF16 = jnp.bfloat16
 VMEM = pl.BlockSpec(memory_space=pltpu.VMEM)
 SMEM = pl.BlockSpec(memory_space=pltpu.SMEM)
+NEAR = pl.BlockSpec(memory_space=pltpu.VMEM)
 HBM = pl.BlockSpec(memory_space=pltpu.HBM)
 
 
@@ -46,7 +47,11 @@
     limit = min(60 * 1024 * 1024, held + extra + 6 * 1024 * 1024)
     in_specs = in_specs or [VMEM] * len(args)
     args = [
-        pltpu.with_memory_space_constraint(v, pltpu.HBM) if spec is HBM else v
+        pltpu.with_memory_space_constraint(v, pltpu.HBM)
+        if spec is HBM
+        else pltpu.with_memory_space_constraint(v, pltpu.VMEM)
+        if spec is NEAR
+        else v
         for v, spec in zip(args, in_specs)
     ]
     if local:
@@ -204,44 +209,84 @@
     project_rows(rows_ref[...], weight_ref, table_ref, j, q_ref, kv_ref)
 
 
-def attend_body(number, pad, outer, inner, members, *refs):
-    factor_ref = refs[0]
-    q_refs = refs[1 : 1 + inner]
-    kv_refs = refs[1 + inner : 1 + inner + inner * members]
-    out_ref, q_all, k_all, v_all = refs[1 + inner + inner * members :]
+def gather_pieces(pieces, k_all, v_all, number, pad):
     wide = 2 * QK_DIM
-    tile = outer * pad
-    for j in range(inner):
-        q_all[j] = q_refs[j][...] * jnp.asarray(QK_DIM ** (-0.5), BF16)
     row = 0
-    for piece in kv_refs:
-        k_all[row : row + tile, :] = piece[0:tile, :wide]
-        v_all[row : row + tile, :] = piece[0:tile, wide:]
-        row += tile
+    for piece, rows in pieces:
+        k_all[row : row + rows, :] = piece[0:rows, :wide]
+        v_all[row : row + rows, :] = piece[0:rows, wide:]
+        row += rows
     latents = row
-    for piece in kv_refs[:members]:
-        held = piece.shape[0] - tile
-        k_all[row : row + held, :] = piece[tile : tile + held, :wide]
-        v_all[row : row + held, :] = piece[tile : tile + held, wide:]
-        row += held
+    for piece, rows in pieces:
+        held = piece.shape[0] - rows
+        if held:
+            k_all[row : row + held, :] = piece[rows : rows + held, :wide]
+            v_all[row : row + held, :] = piece[rows : rows + held, wide:]
+            row += held
     column = lax.broadcasted_iota(jnp.int32, (1, row), 1)
     valid = (column >= latents) | (column % pad < number)
-    bias = jnp.where(valid, 0.0, -1e30)
-    lane = lax.broadcasted_iota(jnp.int32, (tile, wide), 1)
+    return jnp.where(valid, 0.0, -1e30)
+
+
+def score(q_all, j, m, k_all, bias):
+    queries = q_all[j] * jnp.asarray(QK_DIM ** (-0.5), BF16)
+    lane = lax.broadcasted_iota(jnp.int32, queries.shape, 1)
+    own = jnp.where((lane // QK_DIM) == m, queries, jnp.zeros_like(queries))
+    return bias + lax.dot_general(
+        own, k_all[...], (((1,), (1,)), ((), ())), preferred_element_type=F32
+    )
+
+
+def repeat(count, one):
+    if count <= 4:
+        for j in range(count):
+            one(j, 0)
+    else:
+        lax.fori_loop(0, count, one, 0)
+
+
+def attend_first_body(number, pad, tile, inner, *refs):
+    q_refs, kv_refs = refs[:inner], refs[inner:-6]
+    top_ref, sum_ref, mix_ref, q_all, k_all, v_all = refs[-6:]
+    for j in range(inner):
+        q_all[j] = q_refs[j][...]
+    bias = gather_pieces([(v, tile) for v in kv_refs], k_all, v_all, number, pad)
 
     def one(j, carry):
-        queries = q_all[j]
+        for m in range(2):
+            scores = score(q_all, j, m, k_all, bias)
+            highest = jnp.max(scores, axis=-1, keepdims=True)
+            weights = jnp.exp(scores - highest)
+            top_ref[j, m] = highest
+            sum_ref[j, m] = jnp.sum(weights, axis=-1, keepdims=True)
+            mix_ref[j, m] = jnp.dot(
+                weights.astype(BF16), v_all[...], preferred_element_type=F32
+            )
+        return carry
+
+    repeat(inner, one)
+
+
+def attend_last_body(number, pad, tile, outer, inner, *refs):
+    factor_ref, top_ref, sum_ref, mix_ref = refs[:4]
+    q_refs, kv_refs = refs[4 : 4 + inner], refs[4 + inner : -4]
+    out_ref, q_all, k_all, v_all = refs[-4:]
+    for j in range(inner):
+        q_all[j] = q_refs[j][...]
+    bias = gather_pieces([(v, tile) for v in kv_refs], k_all, v_all, number, pad)
+
+    def one(j, carry):
         mixed = []
         for m in range(2):
-            own = jnp.where((lane // QK_DIM) == m, queries, jnp.zeros_like(queries))
-            scores = lax.dot_general(
-                own, k_all[...], (((1,), (1,)), ((), ())), preferred_element_type=F32
+            scores = score(q_all, j, m, k_all, bias)
+            before = top_ref[j, m]
+            highest = jnp.maximum(before, jnp.max(scores, axis=-1, keepdims=True))
+            fade = jnp.exp(before - highest)
+            weights = jnp.exp(scores - highest)
+            totals = sum_ref[j, m] * fade + jnp.sum(weights, axis=-1, keepdims=True)
+            mix = mix_ref[j, m] * fade + jnp.dot(
+                weights.astype(BF16), v_all[...], preferred_element_type=F32
             )
-            scores = scores + bias
-            highest = jnp.max(scores, axis=-1, keepdims=True)
-            weights = jnp.exp(scores - highest)
-            totals = jnp.sum(weights, axis=-1, keepdims=True)
-            mix = jnp.dot(weights.astype(BF16), v_all[...], preferred_element_type=F32)
             mixed.append(mix / totals)
         head = mixed[0] - factor_ref[0] * mixed[1]
         head = head * lax.rsqrt(jnp.mean(head * head, axis=-1, keepdims=True) + HEAD_EPS)
@@ -250,37 +295,30 @@
             out_ref[k, j] = head[k * pad : (k + 1) * pad]
         return carry
 
-    if inner <= 4:
-        for j in range(inner):
-            one(j, 0)
-    else:
-        lax.fori_loop(0, inner, one, 0)
-
-
-def partial_out_body(share, outer, inner, pad, *refs):
-    side_ref, weight_ref = refs[:2]
-    mine = refs[2 : 1 + outer]
-    theirs = refs[1 + outer : 1 + outer + (outer - 1) * (share - 1)]
-    rest = refs[1 + outer + (outer - 1) * (share - 1) :]
+    repeat(inner, one)
+
+
+def partial_out_body(singles, pairs, inner, pad, *refs):
+    side_ref = refs[0]
+    alone = refs[1 : 2 + len(singles)]
+    paired = refs[2 + len(singles) : 2 + len(singles) + 2 * len(pairs)]
+    rest = refs[2 + len(singles) + 2 * len(pairs) :]
+    outer = 1 + len(singles) + 2 * len(pairs)
     parts, own_ref, others = rest[:outer], rest[outer], rest[1 + outer :]
     rows = inner * pad
-    half = VAL_DIM // share
-    total = jnp.dot(
-        parts[0][...].reshape(rows, VAL_DIM), weight_ref[...], preferred_element_type=F32
-    )
-    for k in range(1, outer):
-        part = parts[k][...].reshape(rows, VAL_DIM)
-        if share == 1:
-            total += jnp.dot(part, mine[k - 1][...], preferred_element_type=F32)
-            continue
-        first = jnp.broadcast_to(side_ref[0], (rows, half)) == 0
-        left, right = part[:, :half], part[:, half:]
-        total += jnp.dot(
-            jnp.where(first, left, right), mine[k - 1][...], preferred_element_type=F32
-        )
-        total += jnp.dot(
-            jnp.where(first, right, left), theirs[k - 1][...], preferred_element_type=F32
-        )
+
+    def part(k):
+        return parts[k][...].reshape(rows, VAL_DIM)
+
+    terms = [(part(0), alone[0])] + [(part(k), w) for k, w in zip(singles, alone[1:])]
+    first = jnp.broadcast_to(side_ref[0], (rows, VAL_DIM)) == 0
+    for i, (a, b) in enumerate(pairs):
+        terms.append((jnp.where(first, part(a), part(b)), paired[2 * i]))
+        terms.append((jnp.where(first, part(b), part(a)), paired[2 * i + 1]))
+    total = None
+    for rows_in, weight in terms:
+        term = jnp.dot(rows_in, weight[...], preferred_element_type=F32)
+        total = term if total is None else total + term
     own_ref[...] = total[:pad]
     for j in range(1, inner):
         others[j - 1][...] = total[j * pad : (j + 1) * pad].astype(BF16)
@@ -337,9 +375,6 @@
         ]
         return lax.ppermute(value, "tp", pairs)
 
-    def along_sp(value, s):
-        return lax.ppermute(value, "sp", [(i, ahead(i, s, groups)) for i in range(groups)])
-
     columns = mod_weight.shape[1]
     copies = call(
         partial_body,
@@ -390,6 +425,7 @@
         weight,
         *[blocks[k, 0] for k in range(outer)],
         scratch=[pltpu.VMEM((tile, width), BF16), pltpu.VMEM((held, width), BF16)],
+        in_specs=[VMEM] * 5 + [NEAR] * (outer - 1),
     )
     queries, kv = [q_first], [kv_first]
     for j in range(1, inner):
@@ -401,52 +437,98 @@
             weight,
             *[blocks[k, j] for k in range(outer)],
             scratch=[pltpu.VMEM((tile, width), BF16)],
+            in_specs=[VMEM] * 3 + [NEAR] * outer,
         )
         queries.append(q_next)
         kv.append(kv_next)
-    pieces_kv = []
-    for part in kv:
-        pieces_kv.append(part)
-        for s in range(1, groups):
-            pieces_kv.append(along_sp(part, s))
-    keys = groups * (inner * tile + held)
-    attended = call(
-        functools.partial(attend_body, number, pad, outer, inner, groups),
-        sds((outer, inner, pad, VAL_DIM), BF16),
-        head_lambda,
-        *queries,
-        *pieces_kv,
-        scratch=[
+    share = share_of(groups)
+    lines = groups // share
+
+    def along_lines(value, s):
+        pairs = [
+            (g * share + c, ahead(g, s, lines) * share + c)
+            for g in range(lines)
+            for c in range(share)
+        ]
+        return lax.ppermute(value, "sp", pairs)
+
+    swap = [(i, i ^ 1) for i in range(groups)]
+
+    def spread(part):
+        pieces = [part]
+        for s in range(1, lines):
+            pieces.append(along_lines(part, s))
+        if share > 1:
+            for piece in list(pieces):
+                pieces.append(lax.ppermute(piece, "sp", swap))
+        return pieces
+
+    kv = [spread(part) for part in kv]
+    early, late = kv[0], sum(kv[1:], [])
+    stats = (
+        sds((inner, 2, tile, 1), F32),
+        sds((inner, 2, tile, 1), F32),
+        sds((inner, 2, tile, VAL_DIM), F32),
+    )
+
+    def room(keys):
+        return [
             pltpu.VMEM((inner, tile, wide), BF16),
             pltpu.VMEM((keys, wide), BF16),
             pltpu.VMEM((keys, VAL_DIM), BF16),
-        ],
+        ]
+
+    keys = groups * (tile + held)
+    first_stats = call(
+        functools.partial(attend_first_body, number, pad, tile, inner),
+        stats,
+        *queries,
+        *early,
+        scratch=room(keys),
         extra=tile * keys * 12,
-        in_specs=[SMEM] + [VMEM] * (inner + inner * groups),
+    )
+    keys = groups * (inner - 1) * tile
+    attended = call(
+        functools.partial(attend_last_body, number, pad, tile, outer, inner),
+        sds((outer, inner, pad, VAL_DIM), BF16),
+        head_lambda,
+        *first_stats,
+        *queries,
+        *late,
+        scratch=room(keys),
+        extra=tile * keys * 12,
+        in_specs=[SMEM] + [VMEM] * (3 + inner + len(late)),
     )
     parts = [attended[0]]
     for k in range(1, outer):
         parts.append(along_outer(attended[k], k, behind))
 
-    share = 2 if groups % 2 == 0 else 1
-    depth = w_out.shape[0]
+    singles, pairs = plan(groups, outer)
     side = here_sp % share
-    half = lax.dynamic_slice(w_out, (side * (depth // share), 0), (depth // share, width))
-    swap = [(i, i ^ 1) for i in range(groups)]
-    mine, theirs = [], []
-    for k in range(1, outer):
-        mine.append(along_outer(half, k, behind))
-        if share > 1:
-            theirs.append(lax.ppermute(mine[-1], "sp", swap))
+    alone, paired = [], []
+    for k in singles:
+        alone.append(along_outer(w_out, k, behind))
+    for a, b in pairs:
+        moves = [
+            (
+                (s * outer + o) * inner + i,
+                (s * outer + behind(o, b if s % 2 else a, outer)) * inner + i,
+            )
+            for s in range(groups)
+            for o in range(outer)
+            for i in range(inner)
+        ]
+        paired.append(lax.ppermute(w_out, ("sp", "tp"), moves))
+        paired.append(lax.ppermute(paired[-1], "sp", swap))
     total = call(
-        functools.partial(partial_out_body, share, outer, inner, pad),
+        functools.partial(partial_out_body, singles, pairs, inner, pad),
         (sds((pad, width), F32),) + (sds((pad, width), BF16),) * (inner - 1),
         side.reshape(1).astype(jnp.int32),
         w_out,
-        *mine,
-        *theirs,
+        *alone,
+        *paired,
         *parts,
-        in_specs=[SMEM] + [VMEM] * (1 + len(mine) + len(theirs) + outer),
+        in_specs=[SMEM, VMEM] + [NEAR] * (len(alone) + len(paired)) + [VMEM] * outer,
     )
     arrived = []
     for j in range(1, inner):
@@ -459,6 +541,18 @@
         total[0],
         *arrived,
     )
+
+
+def share_of(groups):
+    return 2 if groups % 2 == 0 else 1
+
+
+def plan(groups, outer):
+    if share_of(groups) == 1:
+        return tuple(range(1, outer)), ()
+    pairs = tuple((k, k + 1) for k in range(2, outer - 1, 2))
+    paired = {k for pair in pairs for k in pair}
+    return tuple(k for k in range(1, outer) if k not in paired), pairs
 
 
 def solution(mesh):

time: 68.6 us -> 83.1 us (1.21)
  waiting for transfers between devices: 16 us -> 40.6 us
  starting transfers between devices: 35.9 us -> 26.6 us
  local copies, waits for them, and re-layouts: 3.6 us -> 1.57 us
  Pallas kernels: 12 us -> 13.2 us
    ppermute x9 -> x7, waiting for transfers between devices: 7.58 us -> 27.5 us  [along_outer(): return lax.ppermute(value, 'tp', pairs)]
    ppermute x9 -> x7, starting transfers between devices: 18.6 us -> 9.49 us  [along_outer(): return lax.ppermute(value, 'tp', pairs)]
    ppermute x9 -> x8, waiting for transfers between devices: 3.06 us -> 6.45 us  [the longest x2 6.43 us: along_lines(): return lax.ppermute(value, 'sp', pairs)]
    ppermute x9 -> x8, starting transfers between devices: 4.91 us -> 6.9 us  [the longest x1 4.06 us: shards(): paired.append(lax.ppermute(w_out, ('sp', 'tp'), moves))]
    ppermute x5, waiting for transfers between devices: 5.34 us -> 6.68 us  [along_inner(): return lax.ppermute(value, 'tp', pairs)]
    unnamed x18 -> x10, local copies, waits for them, and re-layouts: 2.87 us -> 1.56 us
    pallas_call x7 -> x8, Pallas kernels: 12 us -> 13.2 us  [call(): pl.pallas_call(body, out_shape=outs, in_specs=in_specs, out_specs=jax.tre...]
    all_to_all x1, starting transfers between devices: 4.93 us -> 3.83 us  [shards(): pieces = lax.all_to_all(copies, ('sp', 'tp'), 0, 0)]
  transfers between devices with their start and end apart: 24 -> 21, of which waited for: 7 -> 8; matrix products, arithmetic and copies ran while one was open for 1% -> 0% of each run, Pallas kernels for 14% -> 13%
where the time goes in v1:
time: 83.1 us; the launch traced here: 82.8 us
  waiting for transfers between devices  40.6 us (49%)
  starting transfers between devices  26.6 us (32%)
  Pallas kernels  13.2 us (16%)
  local copies, waits for them, and re-layouts  1.57 us (2%)
    ppermute x7, waiting for transfers between devices, along_outer(): return lax.ppermute(value, 'tp', pairs)  27.5 us
    pallas_call x8, Pallas kernels, call(): pl.pallas_call(body, out_shape=outs, in_specs=in_specs, out_specs=jax.tre...  13.2 us
    ppermute x7, starting transfers between devices, along_outer(): return lax.ppermute(value, 'tp', pairs)  9.49 us
    ppermute x5, waiting for transfers between devices, along_inner(): return lax.ppermute(value, 'tp', pairs)  6.68 us
    ppermute x2, waiting for transfers between devices, along_lines(): return lax.ppermute(value, 'sp', pairs)  6.43 us
    ppermute x5, starting transfers between devices, along_inner(): return lax.ppermute(value, 'tp', pairs)  6.42 us
    ppermute x1, starting transfers between devices, shards(): paired.append(lax.ppermute(w_out, ('sp', 'tp'), moves))  4.06 us
    all_to_all x1, starting transfers between devices, shards(): pieces = lax.all_to_all(copies, ('sp', 'tp'), 0, 0)  3.83 us
  transfers between devices with their start and end apart: 21, of which 8 were waited for; matrix products, arithmetic and copies ran while one was open for 0% of the time, Pallas kernels for 13%

profile of v1, /device:TPU:0, one launch (start us, length us, event | category | flops | bytes accessed | tf_op | source)
XLA Modules:
  0.0 82.8 jit_solution(7963734919783355041)
XLA Ops:
  0.0 4.1 %collective-permute-start.4 = (bf16[128,2048]{1,0:T(8,128)(2,1)}, bf16[128,2048]{1,0:T(8,128)(2,1)}, u32[]{:S(2)}, u32[]{:S(2)}) collective-permute-start(bf16[128,2048]{1,0:T(8,128)(2,1)} %refs_1_.5), channel_id=1, source_target_pairs={{0,4},{1,5},{2,6},{3,7},{4,0},{5,1},{6,2},{7,3},{8,14},{9,15},{10,... | collective-permute-start | bytes 1572872 | tf_op jit(solution)/shard_map/ppermute | solution.py:521
  4.1 2.1 %shard_map.100 = f32[32,2,768]{2,1,0:T(2,128)} custom-call(f32[1,512]{1,0:T(1,128)} %bitcast.12, f32[1,512]{1,0:T(1,128)} %bitcast.13, bf16[512,768]{1,0:T(8,128)(2,1)} %weight_hbm.1), custom_call_target="tpu_custom_call" | custom-call | flops 2000000 | tf_op jit(solution)/shard_map/pallas_call | solution.py:59
  6.2 3.8 %all-to-all-start = ((f32[32,2,768]{2,1,0:T(2,128)}), f32[32,2,768]{2,1,0:T(2,128)S(1)}, u32[]{:S(2)}, u32[]{:S(2)}) async-start(f32[32,2,768]{2,1,0:T(2,128)} %shard_map.100), calls=%async_computation | async-start | bytes 393216 | tf_op jit(solution)/shard_map/all_to_all | solution.py:393
  10.0 1.8 %collective-permute-start = (bf16[30,2048]{1,0:T(8,128)(2,1)}, bf16[30,2048]{1,0:T(8,128)(2,1)}, u32[]{:S(2)}, u32[]{:S(2)}) collective-permute-start(bf16[30,2048]{1,0:T(8,128)(2,1)} %refs_0_.2), channel_id=1, source_target_pairs={{0,2},{1,3},{2,0},{3,1},{4,6},{5,7},{6,4},{7,5},{8,10},{9,11},{10,... | collective-permute-start | bytes 368648 | tf_op jit(solution)/shard_map/ppermute | solution.py:368
  11.8 2.4 %collective-permute-start.1 = (bf16[30,2048]{1,0:T(8,128)(2,1)}, bf16[30,2048]{1,0:T(8,128)(2,1)}, u32[]{:S(2)}, u32[]{:S(2)}) collective-permute-start(bf16[30,2048]{1,0:T(8,128)(2,1)} %refs_0_.2), channel_id=1, source_target_pairs={{0,4},{1,5},{2,6},{3,7},{4,0},{5,1},{6,2},{7,3},{8,12},{9,13},{10,... | collective-permute-start | bytes 368648 | tf_op jit(solution)/shard_map/ppermute | solution.py:368
  14.4 1.8 %collective-permute-start.6 = (bf16[30,2048]{1,0:T(8,128)(2,1)}, bf16[30,2048]{1,0:T(8,128)(2,1)}, u32[]{:S(2)}, u32[]{:S(2)}) collective-permute-start(bf16[30,2048]{1,0:T(8,128)(2,1)} %refs_0_.2), channel_id=1, source_target_pairs={{0,1},{1,0},{2,3},{3,2},{4,5},{5,4},{6,7},{7,6},{8,9},{9,8},{10,11... | collective-permute-start | bytes 368648 | tf_op jit(solution)/shard_map/ppermute | solution.py:376
  16.2 6.5 %collective-permute-done.refs_5_ = bf16[30,2048]{1,0:T(8,128)(2,1)} collective-permute-done((bf16[30,2048]{1,0:T(8,128)(2,1)}, bf16[30,2048]{1,0:T(8,128)(2,1)}, u32[]{:S(2)}, u32[]{:S(2)}) %collective-permute-start) | collective-permute-done | bytes 122912 | tf_op jit(solution)/shard_map/ppermute | solution.py:368
  22.7 1.5 %collective-permute-start.7 = (bf16[30,2048]{1,0:T(8,128)(2,1)}, bf16[30,2048]{1,0:T(8,128)(2,1)}, u32[]{:S(2)}, u32[]{:S(2)}) collective-permute-start(bf16[30,2048]{1,0:T(8,128)(2,1)} %collective-permute-done.refs_5_), channel_id=1, source_target_pairs={{0,1},{1,0},{2,3},{3,2},{4,5},{5,4},{6,7},{7,6},{8,9},{9,8},{10,11... | collective-permute-start | bytes 368648 | tf_op jit(solution)/shard_map/ppermute | solution.py:376
  24.2 16.8 %collective-permute-done.1.refs_6_ = bf16[30,2048]{1,0:T(8,128)(2,1)} collective-permute-done((bf16[30,2048]{1,0:T(8,128)(2,1)}, bf16[30,2048]{1,0:T(8,128)(2,1)}, u32[]{:S(2)}, u32[]{:S(2)}) %collective-permute-start.1) | collective-permute-done | bytes 122912 | tf_op jit(solution)/shard_map/ppermute | solution.py:368
  41.0 1.7 %collective-permute-start.8 = (bf16[30,2048]{1,0:T(8,128)(2,1)}, bf16[30,2048]{1,0:T(8,128)(2,1)}, u32[]{:S(2)}, u32[]{:S(2)}) collective-permute-start(bf16[30,2048]{1,0:T(8,128)(2,1)} %collective-permute-done.1.refs_6_), channel_id=1, source_target_pairs={{0,1},{1,0},{2,3},{3,2},{4,5},{5,4},{6,7},{7,6},{8,9},{9,8},{10,11... | collective-permute-start | bytes 368648 | tf_op jit(solution)/shard_map/ppermute | solution.py:376
  45.8 2.0 %shard_map.102 = (f32[2,6144]{1,0:T(2,128)S(1)}, bf16[128,128]{1,0:T(8,128)(2,1)S(1)}, bf16[320,256]{1,0:T(8,128)(2,1)S(1)}) custom-call(f32[32,2,768]{2,1,0:T(2,128)S(1)} %all-to-all-done.refs_0_, bf16[192,2048]{1,0:T(8,128)(2,1)S(1)} %copy-done, f32[2,2,128,128]{3,2,1,0:T(8,128)S(1)} %get-tuple-element.17.refs_2_.refs_1_, ...), custom_call_target="tpu_custom_call" | custom-call | flops 2000000 | tf_op jit(solution)/shard_map/pallas_call | solution.py:59
  47.8 1.6 %collective-permute-start.10 = (bf16[320,256]{1,0:T(8,128)(2,1)S(1)}, bf16[320,256]{1,0:T(8,128)(2,1)S(1)}, u32[]{:S(2)}, u32[]{:S(2)}) collective-permute-start(bf16[320,256]{1,0:T(8,128)(2,1)S(1)} %get-tuple-element.22.refs_2_), channel_id=1, source_target_pairs={{0,16},{8,24},{16,0},{24,8},{1,17},{9,25},{17,1},{25,9},{2,18},{10... | collective-permute-start | bytes 491528 | tf_op jit(solution)/shard_map/ppermute | solution.py:453
  50.5 2.7 %collective-permute-done.10.refs_3_ = bf16[320,256]{1,0:T(8,128)(2,1)S(1)} collective-permute-done((bf16[320,256]{1,0:T(8,128)(2,1)S(1)}, bf16[320,256]{1,0:T(8,128)(2,1)S(1)}, u32[]{:S(2)}, u32[]{:S(2)}) %collective-permute-start.10) | collective-permute-done | bytes 163872 | tf_op jit(solution)/shard_map/ppermute | solution.py:453
  53.2 2.2 %collective-permute-done.9.refs_6_ = bf16[30,2048]{1,0:T(8,128)(2,1)S(1)} collective-permute-done((bf16[30,2048]{1,0:T(8,128)(2,1)S(1)}, bf16[30,2048]{1,0:T(8,128)(2,1)S(1)}, u32[]{:S(2)}, u32[]{:S(2)}) %collective-permute-start.9) | collective-permute-done | bytes 122912 | tf_op jit(solution)/shard_map/ppermute | solution.py:376
  55.5 1.7 %shard_map.103 = (bf16[128,128]{1,0:T(8,128)(2,1)S(1)}, bf16[128,256]{1,0:T(8,128)(2,1)S(1)}) custom-call(f32[2,6144]{1,0:T(2,128)S(1)} %get-tuple-element.19.refs_0_.refs_1_, f32[2,2,128,128]{3,2,1,0:T(8,128)S(1)} %get-tuple-element.17.refs_2_.refs_1_, bf16[2048,384]{1,0:T(8,128)(2,1)S(1)} %get-tuple-element.18.refs_3_.refs_2_, ...), custom_call_target="tpu_custom_call" | custom-call | flops 2000000 | tf_op jit(solution)/shard_map/pallas_call | solution.py:59
  57.8 3.8 %collective-permute-done.13.refs_7_ = bf16[128,256]{1,0:T(8,128)(2,1)S(1)} collective-permute-done((bf16[128,256]{1,0:T(8,128)(2,1)S(1)}, bf16[128,256]{1,0:T(8,128)(2,1)S(1)}, u32[]{:S(2)}, u32[]{:S(2)}) %collective-permute-start.13) | collective-permute-done | bytes 65568 | tf_op jit(solution)/shard_map/ppermute | solution.py:453
  62.7 1.7 %shard_map.104 = (f32[2,2,128,1]{3,2,1,0:T(8,128)S(1)}, f32[2,2,128,1]{3,2,1,0:T(8,128)S(1)}, f32[2,2,128,128]{3,2,1,0:T(8,128)S(1)}) custom-call(bf16[128,128]{1,0:T(8,128)(2,1)S(1)} %get-tuple-element.20.refs_0_.refs_4_, bf16[128,128]{1,0:T(8,128)(2,1)S(1)} %get-tuple-element.21.refs_1_.refs_5_, bf16[320,256]{1,0:T(8,128)(2,1)S(1)} %get-tuple-element.22.refs_2_, ...), custom_call_target="tpu_custom_call" | custom-call | flops 2000000 | tf_op jit(solution)/shard_map/pallas_call | solution.py:59
  64.5 1.7 %shard_map.105 = bf16[4,2,32,128]{3,2,1,0:T(8,128)(2,1)S(1)} custom-call(f32[1]{0:T(128)S(6)} %copy.11.refs_0_, f32[2,2,128,1]{3,2,1,0:T(8,128)S(1)} %get-tuple-element.23.refs_1_, f32[2,2,128,1]{3,2,1,0:T(8,128)S(1)} %get-tuple-element.24.refs_2_, f32[2,2,128,128]{3,2,1,0:T(8,128)S(1)} %get-tuple-element.25.refs_3_, ...), custom_call_target="tpu_custom_call" | custom-call | flops 2000000 | tf_op jit(solution)/shard_map/pallas_call | solution.py:59
  66.2 2.0 %collective-permute-start.16 = (bf16[2,32,128]{2,1,0:T(8,128)(2,1)S(1)}, bf16[2,32,128]{2,1,0:T(8,128)(2,1)S(1)}, u32[]{:S(2)}, u32[]{:S(2)}) collective-permute-start(bf16[2,32,128]{2,1,0:T(8,128)(2,1)S(1)} %get-tuple-element.31), channel_id=1, source_target_pairs={{0,2},{1,3},{2,0},{3,1},{4,6},{5,7},{6,4},{7,5},{8,10},{9,11},{10,... | collective-permute-start | bytes 49160 | tf_op jit(solution)/shard_map/ppermute | solution.py:368
  68.2 1.6 %collective-permute-start.17 = (bf16[2,32,128]{2,1,0:T(8,128)(2,1)S(1)}, bf16[2,32,128]{2,1,0:T(8,128)(2,1)S(1)}, u32[]{:S(2)}, u32[]{:S(2)}) collective-permute-start(bf16[2,32,128]{2,1,0:T(8,128)(2,1)S(1)} %get-tuple-element.30), channel_id=1, source_target_pairs={{0,4},{1,5},{2,6},{3,7},{4,0},{5,1},{6,2},{7,3},{8,12},{9,13},{10,... | collective-permute-start | bytes 49160 | tf_op jit(solution)/shard_map/ppermute | solution.py:368
  71.1 1.7 %collective-permute-done.17.refs_7_ = bf16[2,32,128]{2,1,0:T(8,128)(2,1)S(1)} collective-permute-done((bf16[2,32,128]{2,1,0:T(8,128)(2,1)S(1)}, bf16[2,32,128]{2,1,0:T(8,128)(2,1)S(1)}, u32[]{:S(2)}, u32[]{:S(2)}) %collective-permute-start.17) | collective-permute-done | bytes 16416 | tf_op jit(solution)/shard_map/ppermute | solution.py:368
  72.8 2.5 %collective-permute-done.18.refs_8_ = bf16[2,32,128]{2,1,0:T(8,128)(2,1)S(1)} collective-permute-done((bf16[2,32,128]{2,1,0:T(8,128)(2,1)S(1)}, bf16[2,32,128]{2,1,0:T(8,128)(2,1)S(1)}, u32[]{:S(2)}, u32[]{:S(2)}) %collective-permute-start.18) | collective-permute-done | bytes 16416 | tf_op jit(solution)/shard_map/ppermute | solution.py:368
  75.3 1.6 %shard_map.106 = (f32[32,2048]{1,0:T(8,128)S(1)}, bf16[32,2048]{1,0:T(8,128)(2,1)S(1)}) custom-call(s32[1]{0:T(128)} %bitcast.3.refs_0_, bf16[128,2048]{1,0:T(8,128)(2,1)S(1)} %copy-done.1, bf16[128,2048]{1,0:T(8,128)(2,1)S(1)} %collective-permute-done.3.refs_2_, bf16[128,2048]{1,0:T(8,128)(2,1)} %collective-permute-done.4.refs_3_, ...), custom_call_target="tpu_custom_call" | custom-call | flops 2000000 | tf_op jit(solution)/shard_map/pallas_call | solution.py:59
  77.5 4.4 %collective-permute-done.19.refs_3_ = bf16[32,2048]{1,0:T(8,128)(2,1)S(1)} collective-permute-done((bf16[32,2048]{1,0:T(8,128)(2,1)S(1)}, bf16[32,2048]{1,0:T(8,128)(2,1)S(1)}, u32[]{:S(2)}, u32[]{:S(2)}) %collective-permute-start.19) | collective-permute-done | bytes 131104 | tf_op jit(solution)/shard_map/ppermute | solution.py:376
  (37 shorter events, 8.2 us)
Async XLA Ops:
  0.0 44.9 %copy-start.2 = (bf16[30,2048]{1,0:T(8,128)(2,1)S(1)}, bf16[30,2048]{1,0:T(8,128)(2,1)}, u32[]{:S(2)}) copy-start(bf16[30,2048]{1,0:T(8,128)(2,1)} %refs_0_.2) | copy-start | bytes 368644
  0.0 44.9 %copy-start = (bf16[192,2048]{1,0:T(8,128)(2,1)S(1)}, bf16[192,2048]{1,0:T(8,128)(2,1)}, u32[]{:S(2)}) copy-start(bf16[192,2048]{1,0:T(8,128)(2,1)} %refs_1_.4) | copy-start | bytes 2359300
  0.0 49.6 %collective-permute-start.4 = (bf16[128,2048]{1,0:T(8,128)(2,1)}, bf16[128,2048]{1,0:T(8,128)(2,1)}, u32[]{:S(2)}, u32[]{:S(2)}) collective-permute-start(bf16[128,2048]{1,0:T(8,128)(2,1)} %refs_1_.5), channel_id=1, source_target_pairs={{0,4},{1,5},{2,6},{3,7},{4,0},{5,1},{6,2},{7,3},{8,14},{9,15},{10,... | collective-permute-start | bytes 1572872 | tf_op jit(solution)/shard_map/ppermute | solution.py:521
  6.2 38.7 %all-to-all-start = ((f32[32,2,768]{2,1,0:T(2,128)}), f32[32,2,768]{2,1,0:T(2,128)S(1)}, u32[]{:S(2)}, u32[]{:S(2)}) async-start(f32[32,2,768]{2,1,0:T(2,128)} %shard_map.100), calls=%async_computation | async-start | bytes 393216 | tf_op jit(solution)/shard_map/all_to_all | solution.py:393
  10.0 12.7 %collective-permute-start = (bf16[30,2048]{1,0:T(8,128)(2,1)}, bf16[30,2048]{1,0:T(8,128)(2,1)}, u32[]{:S(2)}, u32[]{:S(2)}) collective-permute-start(bf16[30,2048]{1,0:T(8,128)(2,1)} %refs_0_.2), channel_id=1, source_target_pairs={{0,2},{1,3},{2,0},{3,1},{4,6},{5,7},{6,4},{7,5},{8,10},{9,11},{10,... | collective-permute-start | bytes 368648 | tf_op jit(solution)/shard_map/ppermute | solution.py:368
  11.8 29.2 %collective-permute-start.1 = (bf16[30,2048]{1,0:T(8,128)(2,1)}, bf16[30,2048]{1,0:T(8,128)(2,1)}, u32[]{:S(2)}, u32[]{:S(2)}) collective-permute-start(bf16[30,2048]{1,0:T(8,128)(2,1)} %refs_0_.2), channel_id=1, source_target_pairs={{0,4},{1,5},{2,6},{3,7},{4,0},{5,1},{6,2},{7,3},{8,12},{9,13},{10,... | collective-permute-start | bytes 368648 | tf_op jit(solution)/shard_map/ppermute | solution.py:368
  14.2 30.0 %collective-permute-start.2 = (bf16[30,2048]{1,0:T(8,128)(2,1)}, bf16[30,2048]{1,0:T(8,128)(2,1)S(1)}, u32[]{:S(2)}, u32[]{:S(2)}) collective-permute-start(bf16[30,2048]{1,0:T(8,128)(2,1)} %refs_0_.2), channel_id=1, source_target_pairs={{0,6},{1,7},{2,4},{3,5},{4,2},{5,3},{6,0},{7,1},{8,14},{9,15},{10,... | collective-permute-start | bytes 368648 | tf_op jit(solution)/shard_map/ppermute | solution.py:368
  14.4 35.0 %collective-permute-start.6 = (bf16[30,2048]{1,0:T(8,128)(2,1)}, bf16[30,2048]{1,0:T(8,128)(2,1)}, u32[]{:S(2)}, u32[]{:S(2)}) collective-permute-start(bf16[30,2048]{1,0:T(8,128)(2,1)} %refs_0_.2), channel_id=1, source_target_pairs={{0,1},{1,0},{2,3},{3,2},{4,5},{5,4},{6,7},{7,6},{8,9},{9,8},{10,11... | collective-permute-start | bytes 368648 | tf_op jit(solution)/shard_map/ppermute | solution.py:376
  22.7 26.8 %collective-permute-start.7 = (bf16[30,2048]{1,0:T(8,128)(2,1)}, bf16[30,2048]{1,0:T(8,128)(2,1)}, u32[]{:S(2)}, u32[]{:S(2)}) collective-permute-start(bf16[30,2048]{1,0:T(8,128)(2,1)} %collective-permute-done.refs_5_), channel_id=1, source_target_pairs={{0,1},{1,0},{2,3},{3,2},{4,5},{5,4},{6,7},{7,6},{8,9},{9,8},{10,11... | collective-permute-start | bytes 368648 | tf_op jit(solution)/shard_map/ppermute | solution.py:376
  41.0 9.4 %collective-permute-start.8 = (bf16[30,2048]{1,0:T(8,128)(2,1)}, bf16[30,2048]{1,0:T(8,128)(2,1)}, u32[]{:S(2)}, u32[]{:S(2)}) collective-permute-start(bf16[30,2048]{1,0:T(8,128)(2,1)} %collective-permute-done.1.refs_6_), channel_id=1, source_target_pairs={{0,1},{1,0},{2,3},{3,2},{4,5},{5,4},{6,7},{7,6},{8,9},{9,8},{10,11... | collective-permute-start | bytes 368648 | tf_op jit(solution)/shard_map/ppermute | solution.py:376
  45.8 3.6 %copy-start.1 = (bf16[128,2048]{1,0:T(8,128)(2,1)S(1)}, bf16[128,2048]{1,0:T(8,128)(2,1)}, u32[]{:S(2)}) copy-start(bf16[128,2048]{1,0:T(8,128)(2,1)} %refs_1_.5) | copy-start | bytes 1572868
  47.8 5.4 %collective-permute-start.10 = (bf16[320,256]{1,0:T(8,128)(2,1)S(1)}, bf16[320,256]{1,0:T(8,128)(2,1)S(1)}, u32[]{:S(2)}, u32[]{:S(2)}) collective-permute-start(bf16[320,256]{1,0:T(8,128)(2,1)S(1)} %get-tuple-element.22.refs_2_), channel_id=1, source_target_pairs={{0,16},{8,24},{16,0},{24,8},{1,17},{9,25},{17,1},{25,9},{2,18},{10... | collective-permute-start | bytes 491528 | tf_op jit(solution)/shard_map/ppermute | solution.py:453
  49.4 21.7 %collective-permute-start.3 = (bf16[128,2048]{1,0:T(8,128)(2,1)S(1)}, bf16[128,2048]{1,0:T(8,128)(2,1)S(1)}, u32[]{:S(2)}, u32[]{:S(2)}) collective-permute-start(bf16[128,2048]{1,0:T(8,128)(2,1)S(1)} %copy-done.1), channel_id=1, source_target_pairs={{0,2},{1,3},{2,0},{3,1},{4,6},{5,7},{6,4},{7,5},{8,10},{9,11},{10,... | collective-permute-start | bytes 1572872 | tf_op jit(solution)/shard_map/ppermute | solution.py:368
  49.6 25.8 %collective-permute-start.5 = (bf16[128,2048]{1,0:T(8,128)(2,1)}, bf16[128,2048]{1,0:T(8,128)(2,1)}, u32[]{:S(2)}, u32[]{:S(2)}) collective-permute-start(bf16[128,2048]{1,0:T(8,128)(2,1)} %collective-permute-done.4.refs_3_), channel_id=1, source_target_pairs={{0,8},{8,0},{16,24},{24,16},{1,9},{9,1},{17,25},{25,17},{2,10},{10... | collective-permute-start | bytes 1572872 | tf_op jit(solution)/shard_map/ppermute | solution.py:522
  49.6 5.9 %collective-permute-start.9 = (bf16[30,2048]{1,0:T(8,128)(2,1)S(1)}, bf16[30,2048]{1,0:T(8,128)(2,1)S(1)}, u32[]{:S(2)}, u32[]{:S(2)}) collective-permute-start(bf16[30,2048]{1,0:T(8,128)(2,1)S(1)} %copy-done.4), channel_id=1, source_target_pairs={{0,1},{1,0},{2,3},{3,2},{4,5},{5,4},{6,7},{7,6},{8,9},{9,8},{10,11... | collective-permute-start | bytes 368648 | tf_op jit(solution)/shard_map/ppermute | solution.py:376
  50.4 11.2 %collective-permute-start.11 = (bf16[320,256]{1,0:T(8,128)(2,1)S(1)}, bf16[320,256]{1,0:T(8,128)(2,1)S(1)}, u32[]{:S(2)}, u32[]{:S(2)}) collective-permute-start(bf16[320,256]{1,0:T(8,128)(2,1)S(1)} %get-tuple-element.22.refs_2_), channel_id=1, source_target_pairs={{0,8},{8,0},{16,24},{24,16},{1,9},{9,1},{17,25},{25,17},{2,10},{10... | collective-permute-start | bytes 491528 | tf_op jit(solution)/shard_map/ppermute | solution.py:463
  53.2 9.5 %collective-permute-start.12 = (bf16[320,256]{1,0:T(8,128)(2,1)S(1)}, bf16[320,256]{1,0:T(8,128)(2,1)S(1)}, u32[]{:S(2)}, u32[]{:S(2)}) collective-permute-start(bf16[320,256]{1,0:T(8,128)(2,1)S(1)} %collective-permute-done.10.refs_3_), channel_id=1, source_target_pairs={{0,8},{8,0},{16,24},{24,16},{1,9},{9,1},{17,25},{25,17},{2,10},{10... | collective-permute-start | bytes 491528 | tf_op jit(solution)/shard_map/ppermute | solution.py:463
  57.2 4.3 %collective-permute-start.13 = (bf16[128,256]{1,0:T(8,128)(2,1)S(1)}, bf16[128,256]{1,0:T(8,128)(2,1)S(1)}, u32[]{:S(2)}, u32[]{:S(2)}) collective-permute-start(bf16[128,256]{1,0:T(8,128)(2,1)S(1)} %get-tuple-element.26.refs_6_), channel_id=1, source_target_pairs={{0,16},{8,24},{16,0},{24,8},{1,17},{9,25},{17,1},{25,9},{2,18},{10... | collective-permute-start | bytes 196616 | tf_op jit(solution)/shard_map/ppermute | solution.py:453
  61.6 2.9 %collective-permute-start.14 = (bf16[128,256]{1,0:T(8,128)(2,1)S(1)}, bf16[128,256]{1,0:T(8,128)(2,1)S(1)}, u32[]{:S(2)}, u32[]{:S(2)}) collective-permute-start(bf16[128,256]{1,0:T(8,128)(2,1)S(1)} %get-tuple-element.26.refs_6_), channel_id=1, source_target_pairs={{0,8},{8,0},{16,24},{24,16},{1,9},{9,1},{17,25},{25,17},{2,10},{10... | collective-permute-start | bytes 196616 | tf_op jit(solution)/shard_map/ppermute | solution.py:463
  61.6 2.9 %collective-permute-start.15 = (bf16[128,256]{1,0:T(8,128)(2,1)S(1)}, bf16[128,256]{1,0:T(8,128)(2,1)S(1)}, u32[]{:S(2)}, u32[]{:S(2)}) collective-permute-start(bf16[128,256]{1,0:T(8,128)(2,1)S(1)} %collective-permute-done.13.refs_7_), channel_id=1, source_target_pairs={{0,8},{8,0},{16,24},{24,16},{1,9},{9,1},{17,25},{25,17},{2,10},{10... | collective-permute-start | bytes 196616 | tf_op jit(solution)/shard_map/ppermute | solution.py:463
  66.2 4.9 %collective-permute-start.16 = (bf16[2,32,128]{2,1,0:T(8,128)(2,1)S(1)}, bf16[2,32,128]{2,1,0:T(8,128)(2,1)S(1)}, u32[]{:S(2)}, u32[]{:S(2)}) collective-permute-start(bf16[2,32,128]{2,1,0:T(8,128)(2,1)S(1)} %get-tuple-element.31), channel_id=1, source_target_pairs={{0,2},{1,3},{2,0},{3,1},{4,6},{5,7},{6,4},{7,5},{8,10},{9,11},{10,... | collective-permute-start | bytes 49160 | tf_op jit(solution)/shard_map/ppermute | solution.py:368
  68.2 4.6 %collective-permute-start.17 = (bf16[2,32,128]{2,1,0:T(8,128)(2,1)S(1)}, bf16[2,32,128]{2,1,0:T(8,128)(2,1)S(1)}, u32[]{:S(2)}, u32[]{:S(2)}) collective-permute-start(bf16[2,32,128]{2,1,0:T(8,128)(2,1)S(1)} %get-tuple-element.30), channel_id=1, source_target_pairs={{0,4},{1,5},{2,6},{3,7},{4,0},{5,1},{6,2},{7,3},{8,12},{9,13},{10,... | collective-permute-start | bytes 49160 | tf_op jit(solution)/shard_map/ppermute | solution.py:368
  69.8 5.5 %collective-permute-start.18 = (bf16[2,32,128]{2,1,0:T(8,128)(2,1)S(1)}, bf16[2,32,128]{2,1,0:T(8,128)(2,1)S(1)}, u32[]{:S(2)}, u32[]{:S(2)}) collective-permute-start(bf16[2,32,128]{2,1,0:T(8,128)(2,1)S(1)} %get-tuple-element.29), channel_id=1, source_target_pairs={{0,6},{1,7},{2,4},{3,5},{4,2},{5,3},{6,0},{7,1},{8,14},{9,15},{10,... | collective-permute-start | bytes 49160 | tf_op jit(solution)/shard_map/ppermute | solution.py:368
  76.9 5.0 %collective-permute-start.19 = (bf16[32,2048]{1,0:T(8,128)(2,1)S(1)}, bf16[32,2048]{1,0:T(8,128)(2,1)S(1)}, u32[]{:S(2)}, u32[]{:S(2)}) collective-permute-start(bf16[32,2048]{1,0:T(8,128)(2,1)S(1)} %get-tuple-element.28), channel_id=1, source_target_pairs={{0,1},{1,0},{2,3},{3,2},{4,5},{5,4},{6,7},{7,6},{8,9},{9,8},{10,11... | collective-permute-start | bytes 393224 | tf_op jit(solution)/shard_map/ppermute | solution.py:376
  (2 other events, 1.6 us)

commit v2 on v1

--- a/solution.py
+++ b/solution.py
@@ -172,9 +172,11 @@
 
 
 def first_body(pad, ranks, count, *refs):
-    pieces_ref, context_ref, table_ref, weight_ref = refs[:4]
+    pieces_ref, context_hbm, table_ref, weight_ref = refs[:4]
     blocks = refs[4 : 4 + count]
-    mod_ref, q_ref, kv_ref, rows_ref, ctx_ref = refs[4 + count :]
+    mod_ref, q_ref, kv_ref, rows_ref, context_ref, sem = refs[4 + count :]
+    move = pltpu.make_async_copy(context_hbm, context_ref, sem)
+    move.start()
     width = context_ref.shape[1]
     columns = pieces_ref.shape[2]
     groups = pieces_ref.shape[0] // ranks
@@ -184,18 +186,19 @@
             total = total + pieces_ref[s * ranks + t]
         mod_ref[:, t * columns : (t + 1) * columns] = total
     mod = mod_ref[...]
+    fill_rows(blocks, rows_ref, pad, mod[0:1, :width], 1.0 + mod[0:1, width : 2 * width])
+    project_rows(rows_ref[...], weight_ref, table_ref, 0, q_ref, kv_ref)
     shift, scale = mod[1:2, :width], 1.0 + mod[1:2, width : 2 * width]
     held = context_ref.shape[0]
     step = 16 if held % 16 == 0 else held
+    move.wait()
     for i in range(0, held, step):
-        ctx_ref[i : i + step, :] = modulated(context_ref[i : i + step, :], shift, scale)
-    fill_rows(blocks, rows_ref, pad, mod[0:1, :width], 1.0 + mod[0:1, width : 2 * width])
+        context_ref[i : i + step, :] = modulated(context_ref[i : i + step, :], shift, scale)
     base = count * pad
     wide = 2 * QK_DIM
     kv_ref[base : base + held, :] = jnp.dot(
-        ctx_ref[...], weight_ref[:, wide:], preferred_element_type=F32
+        context_ref[...], weight_ref[:, wide:], preferred_element_type=F32
     ).astype(BF16)
-    project_rows(rows_ref[...], weight_ref, table_ref, 0, q_ref, kv_ref)
 
 
 def second_body(pad, count, j, *refs):
@@ -298,27 +301,29 @@
     repeat(inner, one)
 
 
-def partial_out_body(singles, pairs, inner, pad, *refs):
-    side_ref = refs[0]
-    alone = refs[1 : 2 + len(singles)]
-    paired = refs[2 + len(singles) : 2 + len(singles) + 2 * len(pairs)]
-    rest = refs[2 + len(singles) + 2 * len(pairs) :]
-    outer = 1 + len(singles) + 2 * len(pairs)
+def partial_out_body(slots, share, ranks, inner, pad, *refs):
+    here_ref, own_hbm = refs[:2]
+    held = refs[2 : 2 + len(slots)]
+    rest = refs[2 + len(slots) : -2]
+    own_weight, sem = refs[-2:]
+    move = pltpu.make_async_copy(own_hbm, own_weight, sem)
+    move.start()
+    outer = 1 + len(slots)
     parts, own_ref, others = rest[:outer], rest[outer], rest[1 + outer :]
     rows = inner * pad
+    side = lax.rem(lax.div(here_ref[0], ranks), share)
+    first = jnp.broadcast_to(side, (rows, VAL_DIM)) == 0
 
     def part(k):
         return parts[k][...].reshape(rows, VAL_DIM)
 
-    terms = [(part(0), alone[0])] + [(part(k), w) for k, w in zip(singles, alone[1:])]
-    first = jnp.broadcast_to(side_ref[0], (rows, VAL_DIM)) == 0
-    for i, (a, b) in enumerate(pairs):
-        terms.append((jnp.where(first, part(a), part(b)), paired[2 * i]))
-        terms.append((jnp.where(first, part(b), part(a)), paired[2 * i + 1]))
     total = None
-    for rows_in, weight in terms:
+    for (a, b), weight in zip(slots, held):
+        rows_in = part(a) if a == b else jnp.where(first, part(a), part(b))
         term = jnp.dot(rows_in, weight[...], preferred_element_type=F32)
         total = term if total is None else total + term
+    move.wait()
+    total += jnp.dot(part(0), own_weight[...], preferred_element_type=F32)
     own_ref[...] = total[:pad]
     for j in range(1, inner):
         others[j - 1][...] = total[j * pad : (j + 1) * pad].astype(BF16)
@@ -394,7 +399,10 @@
 
     blocks = {(0, 0): latent}
     for k in range(1, outer):
-        blocks[k, 0] = along_outer(latent, k, ahead)
+        if relayed(k):
+            blocks[k, 0] = along_outer(blocks[k - 1, 0], 1, ahead)
+        else:
+            blocks[k, 0] = along_outer(latent, k, ahead)
     for j in range(1, inner):
         for k in range(outer):
             blocks[k, j] = along_inner(blocks[k, 0], j, ahead)
@@ -424,8 +432,12 @@
         table,
         weight,
         *[blocks[k, 0] for k in range(outer)],
-        scratch=[pltpu.VMEM((tile, width), BF16), pltpu.VMEM((held, width), BF16)],
-        in_specs=[VMEM] * 5 + [NEAR] * (outer - 1),
+        scratch=[
+            pltpu.VMEM((tile, width), BF16),
+            pltpu.VMEM((held, width), BF16),
+            pltpu.SemaphoreType.DMA,
+        ],
+        in_specs=[VMEM, HBM] + [VMEM] * (2 + outer),
     )
     queries, kv = [q_first], [kv_first]
     for j in range(1, inner):
@@ -437,7 +449,6 @@
             weight,
             *[blocks[k, j] for k in range(outer)],
             scratch=[pltpu.VMEM((tile, width), BF16)],
-            in_specs=[VMEM] * 3 + [NEAR] * outer,
         )
         queries.append(q_next)
         kv.append(kv_next)
@@ -503,32 +514,38 @@
     for k in range(1, outer):
         parts.append(along_outer(attended[k], k, behind))
 
-    singles, pairs = plan(groups, outer)
-    side = here_sp % share
-    alone, paired = [], []
-    for k in singles:
-        alone.append(along_outer(w_out, k, behind))
-    for a, b in pairs:
-        moves = [
-            (
-                (s * outer + o) * inner + i,
-                (s * outer + behind(o, b if s % 2 else a, outer)) * inner + i,
-            )
-            for s in range(groups)
-            for o in range(outer)
-            for i in range(inner)
-        ]
-        paired.append(lax.ppermute(w_out, ("sp", "tp"), moves))
-        paired.append(lax.ppermute(paired[-1], "sp", swap))
+    def joint(value, target):
+        moves = []
+        for s in range(groups):
+            for o in range(outer):
+                for i in range(inner):
+                    to_s, to_o = target(s, o)
+                    moves.append(
+                        ((s * outer + o) * inner + i, (to_s * outer + to_o) * inner + i)
+                    )
+        return lax.ppermute(value, ("sp", "tp"), moves)
+
+    slots, weights = [], []
+    if share > 1 and outer == 4:
+        fetched = joint(w_out, lambda s, o: (s, behind(o, 1 if s % 2 else 2, outer)))
+        turned = joint(fetched, lambda s, o: (s ^ 1, o if s % 2 else behind(o, 1, outer)))
+        given = jnp.where(here_sp % 2 == 0, fetched, turned)
+        traded = lax.ppermute(given, "sp", swap)
+        slots, weights = [(2, 1), (1, 3), (3, 2)], [fetched, turned, traded]
+    else:
+        for k in range(1, outer):
+            weights.append(along_outer(w_out, k, behind))
+            slots.append((k, k))
+    depth = w_out.shape[0]
     total = call(
-        functools.partial(partial_out_body, singles, pairs, inner, pad),
+        functools.partial(partial_out_body, slots, share, ranks, inner, pad),
         (sds((pad, width), F32),) + (sds((pad, width), BF16),) * (inner - 1),
-        side.reshape(1).astype(jnp.int32),
+        here,
         w_out,
-        *alone,
-        *paired,
+        *weights,
         *parts,
-        in_specs=[SMEM, VMEM] + [NEAR] * (len(alone) + len(paired)) + [VMEM] * outer,
+        scratch=[pltpu.VMEM((depth, width), BF16), pltpu.SemaphoreType.DMA],
+        in_specs=[SMEM, HBM] + [VMEM] * (len(weights) + outer),
     )
     arrived = []
     for j in range(1, inner):
@@ -543,16 +560,12 @@
     )
 
 
+def relayed(k):
+    return k > 1 and k % 2 == 1
+
+
 def share_of(groups):
     return 2 if groups % 2 == 0 else 1
-
-
-def plan(groups, outer):
-    if share_of(groups) == 1:
-        return tuple(range(1, outer)), ()
-    pairs = tuple((k, k + 1) for k in range(2, outer - 1, 2))
-    paired = {k for pair in pairs for k in pair}
-    return tuple(k for k in range(1, outer) if k not in paired), pairs
 
 
 def solution(mesh):

time: 83.1 us -> 83.7 us (level)
  starting transfers between devices: 26.6 us -> 28.3 us
  local copies, waits for them, and re-layouts: 1.57 us -> 0.01 us
    ppermute x7 -> x6, waiting for transfers between devices: 27.5 us -> 14.7 us  [along_outer(): return lax.ppermute(value, 'tp', pairs)]
    ppermute x2 -> x3, waiting for transfers between devices: 0.01 us -> 11.7 us  [the longest x2 11.7 us: joint(): return lax.ppermute(value, ('sp', 'tp'), moves)]
    all_to_all x1, starting transfers between devices: 3.83 us -> 7.5 us  [shards(): pieces = lax.all_to_all(copies, ('sp', 'tp'), 0, 0)]
    ppermute x5, waiting for transfers between devices: 6.68 us -> 8.45 us  [along_inner(): return lax.ppermute(value, 'tp', pairs)]
    unnamed x10 -> x2, local copies, waits for them, and re-layouts: 1.56 us -> 0.01 us
    ppermute x2, waiting for transfers between devices: 6.43 us -> 5.31 us  [along_lines(): return lax.ppermute(value, 'sp', pairs)]
    pallas_call x8, Pallas kernels: 13.2 us -> 14 us  [call(): pl.pallas_call(body, out_shape=outs, in_specs=in_specs, out_specs=jax.tre...]
    ppermute x7 -> x6, starting transfers between devices: 9.49 us -> 8.7 us  [along_outer(): return lax.ppermute(value, 'tp', pairs)]
  transfers between devices with their start and end apart: 21 -> 21, of which waited for: 8 -> 10; matrix products, arithmetic and copies ran while one was open for 0% -> 0% of each run, Pallas kernels for 13% -> 14%
where the time goes in v2:
time: 83.7 us; the launch traced here: 83.3 us
  waiting for transfers between devices  40.2 us (48%)
  starting transfers between devices  28.3 us (34%)
  Pallas kernels  14 us (17%)
    ppermute x6, waiting for transfers between devices, along_outer(): return lax.ppermute(value, 'tp', pairs)  14.7 us
    pallas_call x8, Pallas kernels, call(): pl.pallas_call(body, out_shape=outs, in_specs=in_specs, out_specs=jax.tre...  14 us
    ppermute x2, waiting for transfers between devices, joint(): return lax.ppermute(value, ('sp', 'tp'), moves)  11.7 us
    ppermute x6, starting transfers between devices, along_outer(): return lax.ppermute(value, 'tp', pairs)  8.7 us
    ppermute x5, waiting for transfers between devices, along_inner(): return lax.ppermute(value, 'tp', pairs)  8.45 us
    all_to_all x1, starting transfers between devices, shards(): pieces = lax.all_to_all(copies, ('sp', 'tp'), 0, 0)  7.5 us
    ppermute x5, starting transfers between devices, along_inner(): return lax.ppermute(value, 'tp', pairs)  5.78 us
    ppermute x2, waiting for transfers between devices, along_lines(): return lax.ppermute(value, 'sp', pairs)  5.31 us
  transfers between devices with their start and end apart: 21, of which 10 were waited for; matrix products, arithmetic and copies ran while one was open for 0% of the time, Pallas kernels for 14%

profile of v2, /device:TPU:0, one launch (start us, length us, event | category | flops | bytes accessed | tf_op | source)
XLA Modules:
  0.0 83.3 jit_solution(6356640419844429066)
XLA Ops:
  0.0 4.1 %collective-permute-start.3 = (bf16[128,2048]{1,0:T(8,128)(2,1)}, bf16[128,2048]{1,0:T(8,128)(2,1)S(1)}, u32[]{:S(2)}, u32[]{:S(2)}) collective-permute-start(bf16[128,2048]{1,0:T(8,128)(2,1)} %refs_1_.5), channel_id=1, source_target_pairs={{0,4},{1,5},{2,6},{3,7},{4,0},{5,1},{6,2},{7,3},{8,10},{9,11},{10,... | collective-permute-start | bytes 1572872 | tf_op jit(solution)/shard_map/ppermute | solution.py:526
  4.1 11.7 %collective-permute-done.3.refs_2_ = bf16[128,2048]{1,0:T(8,128)(2,1)S(1)} collective-permute-done((bf16[128,2048]{1,0:T(8,128)(2,1)}, bf16[128,2048]{1,0:T(8,128)(2,1)S(1)}, u32[]{:S(2)}, u32[]{:S(2)}) %collective-permute-start.3) | collective-permute-done | bytes 524320 | tf_op jit(solution)/shard_map/ppermute | solution.py:526
  15.8 2.1 %shard_map.100 = f32[32,2,768]{2,1,0:T(2,128)} custom-call(f32[1,512]{1,0:T(1,128)} %bitcast.11, f32[1,512]{1,0:T(1,128)} %bitcast.12, bf16[512,768]{1,0:T(8,128)(2,1)} %weight_hbm.1), custom_call_target="tpu_custom_call" | custom-call | flops 2000000 | tf_op jit(solution)/shard_map/pallas_call | solution.py:59
  17.9 7.5 %all-to-all-start = ((f32[32,2,768]{2,1,0:T(2,128)}), f32[32,2,768]{2,1,0:T(2,128)S(1)}, u32[]{:S(2)}, u32[]{:S(2)}) async-start(f32[32,2,768]{2,1,0:T(2,128)} %shard_map.100), calls=%async_computation | async-start | bytes 393216 | tf_op jit(solution)/shard_map/all_to_all | solution.py:398
  25.4 2.7 %collective-permute-start.1 = (bf16[30,2048]{1,0:T(8,128)(2,1)}, bf16[30,2048]{1,0:T(8,128)(2,1)}, u32[]{:S(2)}, u32[]{:S(2)}) collective-permute-start(bf16[30,2048]{1,0:T(8,128)(2,1)} %refs_0_.2), channel_id=1, source_target_pairs={{0,4},{1,5},{2,6},{3,7},{4,0},{5,1},{6,2},{7,3},{8,12},{9,13},{10,... | collective-permute-start | bytes 368648 | tf_op jit(solution)/shard_map/ppermute | solution.py:373
  28.1 1.5 %collective-permute-start = (bf16[30,2048]{1,0:T(8,128)(2,1)}, bf16[30,2048]{1,0:T(8,128)(2,1)S(1)}, u32[]{:S(2)}, u32[]{:S(2)}) collective-permute-start(bf16[30,2048]{1,0:T(8,128)(2,1)} %refs_0_.2), channel_id=1, source_target_pairs={{0,2},{1,3},{2,0},{3,1},{4,6},{5,7},{6,4},{7,5},{8,10},{9,11},{10,... | collective-permute-start | bytes 368648 | tf_op jit(solution)/shard_map/ppermute | solution.py:373
  29.7 9.4 %collective-permute-done.1.refs_6_ = bf16[30,2048]{1,0:T(8,128)(2,1)} collective-permute-done((bf16[30,2048]{1,0:T(8,128)(2,1)}, bf16[30,2048]{1,0:T(8,128)(2,1)}, u32[]{:S(2)}, u32[]{:S(2)}) %collective-permute-start.1) | collective-permute-done | bytes 122912 | tf_op jit(solution)/shard_map/ppermute | solution.py:373
  39.1 1.5 %collective-permute-start.6 = (bf16[30,2048]{1,0:T(8,128)(2,1)}, bf16[30,2048]{1,0:T(8,128)(2,1)S(1)}, u32[]{:S(2)}, u32[]{:S(2)}) collective-permute-start(bf16[30,2048]{1,0:T(8,128)(2,1)} %refs_0_.2), channel_id=1, source_target_pairs={{0,1},{1,0},{2,3},{3,2},{4,5},{5,4},{6,7},{7,6},{8,9},{9,8},{10,11... | collective-permute-start | bytes 368648 | tf_op jit(solution)/shard_map/ppermute | solution.py:381
  42.6 1.7 %collective-permute-done.2.refs_7_ = bf16[30,2048]{1,0:T(8,128)(2,1)} collective-permute-done((bf16[30,2048]{1,0:T(8,128)(2,1)}, bf16[30,2048]{1,0:T(8,128)(2,1)}, u32[]{:S(2)}, u32[]{:S(2)}) %collective-permute-start.2) | collective-permute-done | bytes 122912 | tf_op jit(solution)/shard_map/ppermute | solution.py:373
  44.4 3.3 %shard_map.102 = (f32[2,6144]{1,0:T(2,128)S(1)}, bf16[128,128]{1,0:T(8,128)(2,1)S(1)}, bf16[320,256]{1,0:T(8,128)(2,1)S(1)}) custom-call(f32[32,2,768]{2,1,0:T(2,128)S(1)} %all-to-all-done.refs_0_, bf16[192,2048]{1,0:T(8,128)(2,1)} %refs_1_.4, f32[2,2,128,128]{3,2,1,0:T(8,128)S(1)} %get-tuple-element.17.refs_2_.refs_1_, ...), custom_call_target="tpu_custom_call" | custom-call | flops 2000000 | tf_op jit(solution)/shard_map/pallas_call | solution.py:59
  47.7 1.6 %collective-permute-start.10 = (bf16[320,256]{1,0:T(8,128)(2,1)S(1)}, bf16[320,256]{1,0:T(8,128)(2,1)S(1)}, u32[]{:S(2)}, u32[]{:S(2)}) collective-permute-start(bf16[320,256]{1,0:T(8,128)(2,1)S(1)} %get-tuple-element.22.refs_2_), channel_id=1, source_target_pairs={{0,16},{8,24},{16,0},{24,8},{1,17},{9,25},{17,1},{25,9},{2,18},{10... | collective-permute-start | bytes 491528 | tf_op jit(solution)/shard_map/ppermute | solution.py:464
  49.4 1.6 %collective-permute-start.7 = (bf16[30,2048]{1,0:T(8,128)(2,1)S(1)}, bf16[30,2048]{1,0:T(8,128)(2,1)S(1)}, u32[]{:S(2)}, u32[]{:S(2)}) collective-permute-start(bf16[30,2048]{1,0:T(8,128)(2,1)S(1)} %collective-permute-done.refs_5_), channel_id=1, source_target_pairs={{0,1},{1,0},{2,3},{3,2},{4,5},{5,4},{6,7},{7,6},{8,9},{9,8},{10,11... | collective-permute-start | bytes 368648 | tf_op jit(solution)/shard_map/ppermute | solution.py:381
  51.5 1.6 %collective-permute-done.10.refs_3_ = bf16[320,256]{1,0:T(8,128)(2,1)S(1)} collective-permute-done((bf16[320,256]{1,0:T(8,128)(2,1)S(1)}, bf16[320,256]{1,0:T(8,128)(2,1)S(1)}, u32[]{:S(2)}, u32[]{:S(2)}) %collective-permute-start.10) | collective-permute-done | bytes 163872 | tf_op jit(solution)/shard_map/ppermute | solution.py:464
  53.1 2.7 %collective-permute-done.7.refs_4_ = bf16[30,2048]{1,0:T(8,128)(2,1)S(1)} collective-permute-done((bf16[30,2048]{1,0:T(8,128)(2,1)S(1)}, bf16[30,2048]{1,0:T(8,128)(2,1)S(1)}, u32[]{:S(2)}, u32[]{:S(2)}) %collective-permute-start.7) | collective-permute-done | bytes 122912 | tf_op jit(solution)/shard_map/ppermute | solution.py:381
  55.8 2.3 %collective-permute-done.9.refs_6_ = bf16[30,2048]{1,0:T(8,128)(2,1)S(1)} collective-permute-done((bf16[30,2048]{1,0:T(8,128)(2,1)}, bf16[30,2048]{1,0:T(8,128)(2,1)S(1)}, u32[]{:S(2)}, u32[]{:S(2)}) %collective-permute-start.9) | collective-permute-done | bytes 122912 | tf_op jit(solution)/shard_map/ppermute | solution.py:381
  58.1 1.6 %shard_map.103 = (bf16[128,128]{1,0:T(8,128)(2,1)S(1)}, bf16[128,256]{1,0:T(8,128)(2,1)S(1)}) custom-call(f32[2,6144]{1,0:T(2,128)S(1)} %get-tuple-element.19.refs_0_.refs_1_, f32[2,2,128,128]{3,2,1,0:T(8,128)S(1)} %get-tuple-element.17.refs_2_.refs_1_, bf16[2048,384]{1,0:T(8,128)(2,1)S(1)} %get-tuple-element.18.refs_3_.refs_2_, ...), custom_call_target="tpu_custom_call" | custom-call | flops 2000000 | tf_op jit(solution)/shard_map/pallas_call | solution.py:59
  60.3 3.7 %collective-permute-done.13.refs_7_ = bf16[128,256]{1,0:T(8,128)(2,1)S(1)} collective-permute-done((bf16[128,256]{1,0:T(8,128)(2,1)S(1)}, bf16[128,256]{1,0:T(8,128)(2,1)S(1)}, u32[]{:S(2)}, u32[]{:S(2)}) %collective-permute-start.13) | collective-permute-done | bytes 65568 | tf_op jit(solution)/shard_map/ppermute | solution.py:464
  64.7 1.8 %shard_map.104 = (f32[2,2,128,1]{3,2,1,0:T(8,128)S(1)}, f32[2,2,128,1]{3,2,1,0:T(8,128)S(1)}, f32[2,2,128,128]{3,2,1,0:T(8,128)S(1)}) custom-call(bf16[128,128]{1,0:T(8,128)(2,1)S(1)} %get-tuple-element.20.refs_0_.refs_4_, bf16[128,128]{1,0:T(8,128)(2,1)S(1)} %get-tuple-element.21.refs_1_.refs_5_, bf16[320,256]{1,0:T(8,128)(2,1)S(1)} %get-tuple-element.22.refs_2_, ...), custom_call_target="tpu_custom_call" | custom-call | flops 2000000 | tf_op jit(solution)/shard_map/pallas_call | solution.py:59
  66.5 1.7 %shard_map.105 = bf16[4,2,32,128]{3,2,1,0:T(8,128)(2,1)S(1)} custom-call(f32[1]{0:T(128)S(6)} %copy.11.refs_0_, f32[2,2,128,1]{3,2,1,0:T(8,128)S(1)} %get-tuple-element.23.refs_1_, f32[2,2,128,1]{3,2,1,0:T(8,128)S(1)} %get-tuple-element.24.refs_2_, f32[2,2,128,128]{3,2,1,0:T(8,128)S(1)} %get-tuple-element.25.refs_3_, ...), custom_call_target="tpu_custom_call" | custom-call | flops 2000000 | tf_op jit(solution)/shard_map/pallas_call | solution.py:59
  68.6 2.1 %collective-permute-start.17 = (bf16[2,32,128]{2,1,0:T(8,128)(2,1)S(1)}, bf16[2,32,128]{2,1,0:T(8,128)(2,1)S(1)}, u32[]{:S(2)}, u32[]{:S(2)}) collective-permute-start(bf16[2,32,128]{2,1,0:T(8,128)(2,1)S(1)} %get-tuple-element.30), channel_id=1, source_target_pairs={{0,4},{1,5},{2,6},{3,7},{4,0},{5,1},{6,2},{7,3},{8,12},{9,13},{10,... | collective-permute-start | bytes 49160 | tf_op jit(solution)/shard_map/ppermute | solution.py:373
  70.7 2.0 %collective-permute-start.18 = (bf16[2,32,128]{2,1,0:T(8,128)(2,1)S(1)}, bf16[2,32,128]{2,1,0:T(8,128)(2,1)S(1)}, u32[]{:S(2)}, u32[]{:S(2)}) collective-permute-start(bf16[2,32,128]{2,1,0:T(8,128)(2,1)S(1)} %get-tuple-element.29), channel_id=1, source_target_pairs={{0,6},{1,7},{2,4},{3,5},{4,2},{5,3},{6,0},{7,1},{8,14},{9,15},{10,... | collective-permute-start | bytes 49160 | tf_op jit(solution)/shard_map/ppermute | solution.py:373
  73.3 2.9 %collective-permute-done.18.refs_8_ = bf16[2,32,128]{2,1,0:T(8,128)(2,1)S(1)} collective-permute-done((bf16[2,32,128]{2,1,0:T(8,128)(2,1)S(1)}, bf16[2,32,128]{2,1,0:T(8,128)(2,1)S(1)}, u32[]{:S(2)}, u32[]{:S(2)}) %collective-permute-start.18) | collective-permute-done | bytes 16416 | tf_op jit(solution)/shard_map/ppermute | solution.py:373
  77.5 1.6 %collective-permute-start.19 = (bf16[32,2048]{1,0:T(8,128)(2,1)S(1)}, bf16[32,2048]{1,0:T(8,128)(2,1)S(1)}, u32[]{:S(2)}, u32[]{:S(2)}) collective-permute-start(bf16[32,2048]{1,0:T(8,128)(2,1)S(1)} %get-tuple-element.28), channel_id=1, source_target_pairs={{0,1},{1,0},{2,3},{3,2},{4,5},{5,4},{6,7},{7,6},{8,9},{9,8},{10,11... | collective-permute-start | bytes 393224 | tf_op jit(solution)/shard_map/ppermute | solution.py:381
  79.1 3.4 %collective-permute-done.19.refs_3_ = bf16[32,2048]{1,0:T(8,128)(2,1)S(1)} collective-permute-done((bf16[32,2048]{1,0:T(8,128)(2,1)S(1)}, bf16[32,2048]{1,0:T(8,128)(2,1)S(1)}, u32[]{:S(2)}, u32[]{:S(2)}) %collective-permute-start.19) | collective-permute-done | bytes 131104 | tf_op jit(solution)/shard_map/ppermute | solution.py:381
  (30 shorter events, 6.5 us)
Async XLA Ops:
  0.0 44.4 %copy-start = (bf16[30,2048]{1,0:T(8,128)(2,1)S(1)}, bf16[30,2048]{1,0:T(8,128)(2,1)}, u32[]{:S(2)}) copy-start(bf16[30,2048]{1,0:T(8,128)(2,1)} %refs_0_.2) | copy-start | bytes 368644
  0.0 15.8 %collective-permute-start.3 = (bf16[128,2048]{1,0:T(8,128)(2,1)}, bf16[128,2048]{1,0:T(8,128)(2,1)S(1)}, u32[]{:S(2)}, u32[]{:S(2)}) collective-permute-start(bf16[128,2048]{1,0:T(8,128)(2,1)} %refs_1_.5), channel_id=1, source_target_pairs={{0,4},{1,5},{2,6},{3,7},{4,0},{5,1},{6,2},{7,3},{8,10},{9,11},{10,... | collective-permute-start | bytes 1572872 | tf_op jit(solution)/shard_map/ppermute | solution.py:526
  15.8 33.5 %collective-permute-start.4 = (bf16[128,2048]{1,0:T(8,128)(2,1)S(1)}, bf16[128,2048]{1,0:T(8,128)(2,1)S(1)}, u32[]{:S(2)}, u32[]{:S(2)}) collective-permute-start(bf16[128,2048]{1,0:T(8,128)(2,1)S(1)} %collective-permute-done.3.refs_2_), channel_id=1, source_target_pairs={{0,10},{1,11},{2,8},{3,9},{4,14},{5,15},{6,12},{7,13},{8,0},{9,1},... | collective-permute-start | bytes 1572872 | tf_op jit(solution)/shard_map/ppermute | solution.py:526
  17.9 26.5 %all-to-all-start = ((f32[32,2,768]{2,1,0:T(2,128)}), f32[32,2,768]{2,1,0:T(2,128)S(1)}, u32[]{:S(2)}, u32[]{:S(2)}) async-start(f32[32,2,768]{2,1,0:T(2,128)} %shard_map.100), calls=%async_computation | async-start | bytes 393216 | tf_op jit(solution)/shard_map/all_to_all | solution.py:398
  25.4 13.7 %collective-permute-start.1 = (bf16[30,2048]{1,0:T(8,128)(2,1)}, bf16[30,2048]{1,0:T(8,128)(2,1)}, u32[]{:S(2)}, u32[]{:S(2)}) collective-permute-start(bf16[30,2048]{1,0:T(8,128)(2,1)} %refs_0_.2), channel_id=1, source_target_pairs={{0,4},{1,5},{2,6},{3,7},{4,0},{5,1},{6,2},{7,3},{8,12},{9,13},{10,... | collective-permute-start | bytes 368648 | tf_op jit(solution)/shard_map/ppermute | solution.py:373
  28.1 14.5 %collective-permute-start = (bf16[30,2048]{1,0:T(8,128)(2,1)}, bf16[30,2048]{1,0:T(8,128)(2,1)S(1)}, u32[]{:S(2)}, u32[]{:S(2)}) collective-permute-start(bf16[30,2048]{1,0:T(8,128)(2,1)} %refs_0_.2), channel_id=1, source_target_pairs={{0,2},{1,3},{2,0},{3,1},{4,6},{5,7},{6,4},{7,5},{8,10},{9,11},{10,... | collective-permute-start | bytes 368648 | tf_op jit(solution)/shard_map/ppermute | solution.py:373
  39.1 5.3 %collective-permute-start.2 = (bf16[30,2048]{1,0:T(8,128)(2,1)}, bf16[30,2048]{1,0:T(8,128)(2,1)}, u32[]{:S(2)}, u32[]{:S(2)}) collective-permute-start(bf16[30,2048]{1,0:T(8,128)(2,1)} %collective-permute-done.1.refs_6_), channel_id=1, source_target_pairs={{0,2},{1,3},{2,0},{3,1},{4,6},{5,7},{6,4},{7,5},{8,10},{9,11},{10,... | collective-permute-start | bytes 368648 | tf_op jit(solution)/shard_map/ppermute | solution.py:373
  39.1 11.9 %collective-permute-start.6 = (bf16[30,2048]{1,0:T(8,128)(2,1)}, bf16[30,2048]{1,0:T(8,128)(2,1)S(1)}, u32[]{:S(2)}, u32[]{:S(2)}) collective-permute-start(bf16[30,2048]{1,0:T(8,128)(2,1)} %refs_0_.2), channel_id=1, source_target_pairs={{0,1},{1,0},{2,3},{3,2},{4,5},{5,4},{6,7},{7,6},{8,9},{9,8},{10,11... | collective-permute-start | bytes 368648 | tf_op jit(solution)/shard_map/ppermute | solution.py:381
  42.0 9.5 %collective-permute-start.8 = (bf16[30,2048]{1,0:T(8,128)(2,1)}, bf16[30,2048]{1,0:T(8,128)(2,1)}, u32[]{:S(2)}, u32[]{:S(2)}) collective-permute-start(bf16[30,2048]{1,0:T(8,128)(2,1)} %collective-permute-done.1.refs_6_), channel_id=1, source_target_pairs={{0,1},{1,0},{2,3},{3,2},{4,5},{5,4},{6,7},{7,6},{8,9},{9,8},{10,11... | collective-permute-start | bytes 368648 | tf_op jit(solution)/shard_map/ppermute | solution.py:381
  47.7 5.4 %collective-permute-start.10 = (bf16[320,256]{1,0:T(8,128)(2,1)S(1)}, bf16[320,256]{1,0:T(8,128)(2,1)S(1)}, u32[]{:S(2)}, u32[]{:S(2)}) collective-permute-start(bf16[320,256]{1,0:T(8,128)(2,1)S(1)} %get-tuple-element.22.refs_2_), channel_id=1, source_target_pairs={{0,16},{8,24},{16,0},{24,8},{1,17},{9,25},{17,1},{25,9},{2,18},{10... | collective-permute-start | bytes 491528 | tf_op jit(solution)/shard_map/ppermute | solution.py:464
  49.3 26.9 %collective-permute-start.5 = (bf16[128,2048]{1,0:T(8,128)(2,1)S(1)}, bf16[128,2048]{1,0:T(8,128)(2,1)S(1)}, u32[]{:S(2)}, u32[]{:S(2)}) collective-permute-start(bf16[128,2048]{1,0:T(8,128)(2,1)S(1)} %broadcast_select_fusion), channel_id=1, source_target_pairs={{0,8},{8,0},{16,24},{24,16},{1,9},{9,1},{17,25},{25,17},{2,10},{10... | collective-permute-start | bytes 1572872 | tf_op jit(solution)/shard_map/ppermute | solution.py:533
  49.4 6.4 %collective-permute-start.7 = (bf16[30,2048]{1,0:T(8,128)(2,1)S(1)}, bf16[30,2048]{1,0:T(8,128)(2,1)S(1)}, u32[]{:S(2)}, u32[]{:S(2)}) collective-permute-start(bf16[30,2048]{1,0:T(8,128)(2,1)S(1)} %collective-permute-done.refs_5_), channel_id=1, source_target_pairs={{0,1},{1,0},{2,3},{3,2},{4,5},{5,4},{6,7},{7,6},{8,9},{9,8},{10,11... | collective-permute-start | bytes 368648 | tf_op jit(solution)/shard_map/ppermute | solution.py:381
  51.0 7.1 %collective-permute-start.9 = (bf16[30,2048]{1,0:T(8,128)(2,1)}, bf16[30,2048]{1,0:T(8,128)(2,1)S(1)}, u32[]{:S(2)}, u32[]{:S(2)}) collective-permute-start(bf16[30,2048]{1,0:T(8,128)(2,1)} %collective-permute-done.2.refs_7_), channel_id=1, source_target_pairs={{0,1},{1,0},{2,3},{3,2},{4,5},{5,4},{6,7},{7,6},{8,9},{9,8},{10,11... | collective-permute-start | bytes 368648 | tf_op jit(solution)/shard_map/ppermute | solution.py:381
  51.5 13.2 %collective-permute-start.11 = (bf16[320,256]{1,0:T(8,128)(2,1)S(1)}, bf16[320,256]{1,0:T(8,128)(2,1)S(1)}, u32[]{:S(2)}, u32[]{:S(2)}) collective-permute-start(bf16[320,256]{1,0:T(8,128)(2,1)S(1)} %get-tuple-element.22.refs_2_), channel_id=1, source_target_pairs={{0,8},{8,0},{16,24},{24,16},{1,9},{9,1},{17,25},{25,17},{2,10},{10... | collective-permute-start | bytes 491528 | tf_op jit(solution)/shard_map/ppermute | solution.py:474
  53.1 11.6 %collective-permute-start.12 = (bf16[320,256]{1,0:T(8,128)(2,1)S(1)}, bf16[320,256]{1,0:T(8,128)(2,1)S(1)}, u32[]{:S(2)}, u32[]{:S(2)}) collective-permute-start(bf16[320,256]{1,0:T(8,128)(2,1)S(1)} %collective-permute-done.10.refs_3_), channel_id=1, source_target_pairs={{0,8},{8,0},{16,24},{24,16},{1,9},{9,1},{17,25},{25,17},{2,10},{10... | collective-permute-start | bytes 491528 | tf_op jit(solution)/shard_map/ppermute | solution.py:474
  59.7 4.3 %collective-permute-start.13 = (bf16[128,256]{1,0:T(8,128)(2,1)S(1)}, bf16[128,256]{1,0:T(8,128)(2,1)S(1)}, u32[]{:S(2)}, u32[]{:S(2)}) collective-permute-start(bf16[128,256]{1,0:T(8,128)(2,1)S(1)} %get-tuple-element.26.refs_6_), channel_id=1, source_target_pairs={{0,16},{8,24},{16,0},{24,8},{1,17},{9,25},{17,1},{25,9},{2,18},{10... | collective-permute-start | bytes 196616 | tf_op jit(solution)/shard_map/ppermute | solution.py:464
  60.3 6.2 %collective-permute-start.14 = (bf16[128,256]{1,0:T(8,128)(2,1)S(1)}, bf16[128,256]{1,0:T(8,128)(2,1)S(1)}, u32[]{:S(2)}, u32[]{:S(2)}) collective-permute-start(bf16[128,256]{1,0:T(8,128)(2,1)S(1)} %get-tuple-element.26.refs_6_), channel_id=1, source_target_pairs={{0,8},{8,0},{16,24},{24,16},{1,9},{9,1},{17,25},{25,17},{2,10},{10... | collective-permute-start | bytes 196616 | tf_op jit(solution)/shard_map/ppermute | solution.py:474
  64.1 2.5 %collective-permute-start.15 = (bf16[128,256]{1,0:T(8,128)(2,1)S(1)}, bf16[128,256]{1,0:T(8,128)(2,1)S(1)}, u32[]{:S(2)}, u32[]{:S(2)}) collective-permute-start(bf16[128,256]{1,0:T(8,128)(2,1)S(1)} %collective-permute-done.13.refs_7_), channel_id=1, source_target_pairs={{0,8},{8,0},{16,24},{24,16},{1,9},{9,1},{17,25},{25,17},{2,10},{10... | collective-permute-start | bytes 196616 | tf_op jit(solution)/shard_map/ppermute | solution.py:474
  68.3 4.5 %collective-permute-start.16 = (bf16[2,32,128]{2,1,0:T(8,128)(2,1)S(1)}, bf16[2,32,128]{2,1,0:T(8,128)(2,1)S(1)}, u32[]{:S(2)}, u32[]{:S(2)}) collective-permute-start(bf16[2,32,128]{2,1,0:T(8,128)(2,1)S(1)} %get-tuple-element.31), channel_id=1, source_target_pairs={{0,2},{1,3},{2,0},{3,1},{4,6},{5,7},{6,4},{7,5},{8,10},{9,11},{10,... | collective-permute-start | bytes 49160 | tf_op jit(solution)/shard_map/ppermute | solution.py:373
  68.6 4.7 %collective-permute-start.17 = (bf16[2,32,128]{2,1,0:T(8,128)(2,1)S(1)}, bf16[2,32,128]{2,1,0:T(8,128)(2,1)S(1)}, u32[]{:S(2)}, u32[]{:S(2)}) collective-permute-start(bf16[2,32,128]{2,1,0:T(8,128)(2,1)S(1)} %get-tuple-element.30), channel_id=1, source_target_pairs={{0,4},{1,5},{2,6},{3,7},{4,0},{5,1},{6,2},{7,3},{8,12},{9,13},{10,... | collective-permute-start | bytes 49160 | tf_op jit(solution)/shard_map/ppermute | solution.py:373
  70.7 5.5 %collective-permute-start.18 = (bf16[2,32,128]{2,1,0:T(8,128)(2,1)S(1)}, bf16[2,32,128]{2,1,0:T(8,128)(2,1)S(1)}, u32[]{:S(2)}, u32[]{:S(2)}) collective-permute-start(bf16[2,32,128]{2,1,0:T(8,128)(2,1)S(1)} %get-tuple-element.29), channel_id=1, source_target_pairs={{0,6},{1,7},{2,4},{3,5},{4,2},{5,3},{6,0},{7,1},{8,14},{9,15},{10,... | collective-permute-start | bytes 49160 | tf_op jit(solution)/shard_map/ppermute | solution.py:373
  77.5 5.0 %collective-permute-start.19 = (bf16[32,2048]{1,0:T(8,128)(2,1)S(1)}, bf16[32,2048]{1,0:T(8,128)(2,1)S(1)}, u32[]{:S(2)}, u32[]{:S(2)}) collective-permute-start(bf16[32,2048]{1,0:T(8,128)(2,1)S(1)} %get-tuple-element.28), channel_id=1, source_target_pairs={{0,1},{1,0},{2,3},{3,2},{4,5},{5,4},{6,7},{7,6},{8,9},{9,8},{10,11... | collective-permute-start | bytes 393224 | tf_op jit(solution)/shard_map/ppermute | solution.py:381

commit v3 on v2

--- a/solution.py
+++ b/solution.py
@@ -85,6 +85,7 @@
     rows = (rows / (1.0 + jnp.exp(-rows))).astype(BF16)
     moves[0].wait()
     part = jnp.dot(rows, weight_ref[...], preferred_element_type=F32)
+    part = part.astype(BF16)
     for i in range(out_ref.shape[0]):
         out_ref[i] = part
 
@@ -181,9 +182,9 @@
     columns = pieces_ref.shape[2]
     groups = pieces_ref.shape[0] // ranks
     for t in range(ranks):
-        total = pieces_ref[t]
+        total = pieces_ref[t].astype(F32)
         for s in range(1, groups):
-            total = total + pieces_ref[s * ranks + t]
+            total = total + pieces_ref[s * ranks + t].astype(F32)
         mod_ref[:, t * columns : (t + 1) * columns] = total
     mod = mod_ref[...]
     fill_rows(blocks, rows_ref, pad, mod[0:1, :width], 1.0 + mod[0:1, width : 2 * width])
@@ -383,7 +384,7 @@
     columns = mod_weight.shape[1]
     copies = call(
         partial_body,
-        sds((groups * ranks, 2, columns), F32),
+        sds((groups * ranks, 2, columns), BF16),
         cond_latent.reshape(1, -1),
         cond_context.reshape(1, -1),
         mod_weight,

time: 83.7 us -> 75.8 us (0.906)
  waiting for transfers between devices: 40.2 us -> 30.1 us
  starting transfers between devices: 28.3 us -> 30.6 us
    ppermute x6, waiting for transfers between devices: 14.7 us -> 4.41 us  [along_outer(): return lax.ppermute(value, 'tp', pairs)]
    ppermute x6, starting transfers between devices: 8.7 us -> 12.8 us  [along_outer(): return lax.ppermute(value, 'tp', pairs)]
    all_to_all x1, starting transfers between devices: 7.5 us -> 5.82 us  [shards(): pieces = lax.all_to_all(copies, ('sp', 'tp'), 0, 0)]
  transfers between devices with their start and end apart: 21 -> 21, of which waited for: 10 -> 9; matrix products, arithmetic and copies ran while one was open for 0% -> 0% of each run, Pallas kernels for 14% -> 16%
where the time goes in v3:
time: 75.8 us; the launch traced here: 75.5 us
  starting transfers between devices  30.6 us (40%)
  waiting for transfers between devices  30.1 us (40%)
  Pallas kernels  13.9 us (18%)
  between operations  0.78 us (1%)
    pallas_call x8, Pallas kernels, call(): pl.pallas_call(body, out_shape=outs, in_specs=in_specs, out_specs=jax.tre...  13.9 us
    ppermute x6, starting transfers between devices, along_outer(): return lax.ppermute(value, 'tp', pairs)  12.8 us
    ppermute x2, waiting for transfers between devices, joint(): return lax.ppermute(value, ('sp', 'tp'), moves)  11.7 us
    ppermute x5, waiting for transfers between devices, along_inner(): return lax.ppermute(value, 'tp', pairs)  8.47 us
    all_to_all x1, starting transfers between devices, shards(): pieces = lax.all_to_all(copies, ('sp', 'tp'), 0, 0)  5.82 us
    ppermute x5, starting transfers between devices, along_inner(): return lax.ppermute(value, 'tp', pairs)  5.7 us
    ppermute x2, waiting for transfers between devices, along_lines(): return lax.ppermute(value, 'sp', pairs)  5.52 us
    ppermute x6, waiting for transfers between devices, along_outer(): return lax.ppermute(value, 'tp', pairs)  4.41 us
  transfers between devices with their start and end apart: 21, of which 9 were waited for; matrix products, arithmetic and copies ran while one was open for 0% of the time, Pallas kernels for 16%

profile of v3, /device:TPU:0, one launch (start us, length us, event | category | flops | bytes accessed | tf_op | source)
XLA Modules:
  0.0 75.5 jit_solution(2209937408909441137)
XLA Ops:
  0.0 4.1 %collective-permute-start.3 = (bf16[128,2048]{1,0:T(8,128)(2,1)}, bf16[128,2048]{1,0:T(8,128)(2,1)S(1)}, u32[]{:S(2)}, u32[]{:S(2)}) collective-permute-start(bf16[128,2048]{1,0:T(8,128)(2,1)} %refs_1_.5), channel_id=1, source_target_pairs={{0,4},{1,5},{2,6},{3,7},{4,0},{5,1},{6,2},{7,3},{8,10},{9,11},{10,... | collective-permute-start | bytes 1572872 | tf_op jit(solution)/shard_map/ppermute | solution.py:527
  4.1 11.7 %collective-permute-done.3.refs_2_ = bf16[128,2048]{1,0:T(8,128)(2,1)S(1)} collective-permute-done((bf16[128,2048]{1,0:T(8,128)(2,1)}, bf16[128,2048]{1,0:T(8,128)(2,1)S(1)}, u32[]{:S(2)}, u32[]{:S(2)}) %collective-permute-start.3) | collective-permute-done | bytes 524320 | tf_op jit(solution)/shard_map/ppermute | solution.py:527
  15.8 2.1 %collective-permute-start.1 = (bf16[30,2048]{1,0:T(8,128)(2,1)}, bf16[30,2048]{1,0:T(8,128)(2,1)}, u32[]{:S(2)}, u32[]{:S(2)}) collective-permute-start(bf16[30,2048]{1,0:T(8,128)(2,1)} %refs_0_.2), channel_id=1, source_target_pairs={{0,4},{1,5},{2,6},{3,7},{4,0},{5,1},{6,2},{7,3},{8,12},{9,13},{10,... | collective-permute-start | bytes 368648 | tf_op jit(solution)/shard_map/ppermute | solution.py:374
  17.9 2.0 %shard_map.100 = bf16[32,2,768]{2,1,0:T(2,128)(2,1)} custom-call(f32[1,512]{1,0:T(1,128)} %bitcast.11, f32[1,512]{1,0:T(1,128)} %bitcast.12, bf16[512,768]{1,0:T(8,128)(2,1)} %weight_hbm.1), custom_call_target="tpu_custom_call" | custom-call | flops 2000000 | tf_op jit(solution)/shard_map/pallas_call | solution.py:59
  20.0 5.8 %all-to-all-start = ((bf16[32,2,768]{2,1,0:T(2,128)(2,1)}), bf16[32,2,768]{2,1,0:T(2,128)(2,1)S(1)}, u32[]{:S(2)}, u32[]{:S(2)}) async-start(bf16[32,2,768]{2,1,0:T(2,128)(2,1)} %shard_map.100), calls=%async_computation | async-start | bytes 196608 | tf_op jit(solution)/shard_map/all_to_all | solution.py:399
  25.8 1.8 %collective-permute-start = (bf16[30,2048]{1,0:T(8,128)(2,1)}, bf16[30,2048]{1,0:T(8,128)(2,1)S(1)}, u32[]{:S(2)}, u32[]{:S(2)}) collective-permute-start(bf16[30,2048]{1,0:T(8,128)(2,1)} %refs_0_.2), channel_id=1, source_target_pairs={{0,2},{1,3},{2,0},{3,1},{4,6},{5,7},{6,4},{7,5},{8,10},{9,11},{10,... | collective-permute-start | bytes 368648 | tf_op jit(solution)/shard_map/ppermute | solution.py:374
  27.6 4.3 %collective-permute-start.2 = (bf16[30,2048]{1,0:T(8,128)(2,1)}, bf16[30,2048]{1,0:T(8,128)(2,1)S(1)}, u32[]{:S(2)}, u32[]{:S(2)}) collective-permute-start(bf16[30,2048]{1,0:T(8,128)(2,1)} %collective-permute-done.1.refs_6_), channel_id=1, source_target_pairs={{0,2},{1,3},{2,0},{3,1},{4,6},{5,7},{6,4},{7,5},{8,10},{9,11},{10,... | collective-permute-start | bytes 368648 | tf_op jit(solution)/shard_map/ppermute | solution.py:374
  32.0 1.5 %collective-permute-start.6 = (bf16[30,2048]{1,0:T(8,128)(2,1)}, bf16[30,2048]{1,0:T(8,128)(2,1)S(1)}, u32[]{:S(2)}, u32[]{:S(2)}) collective-permute-start(bf16[30,2048]{1,0:T(8,128)(2,1)} %refs_0_.2), channel_id=1, source_target_pairs={{0,1},{1,0},{2,3},{3,2},{4,5},{5,4},{6,7},{7,6},{8,9},{9,8},{10,11... | collective-permute-start | bytes 368648 | tf_op jit(solution)/shard_map/ppermute | solution.py:382
  35.9 3.3 %shard_map.102 = (f32[2,6144]{1,0:T(2,128)S(1)}, bf16[128,128]{1,0:T(8,128)(2,1)S(1)}, bf16[320,256]{1,0:T(8,128)(2,1)S(1)}) custom-call(bf16[32,2,768]{2,1,0:T(2,128)(2,1)S(1)} %all-to-all-done.refs_0_, bf16[192,2048]{1,0:T(8,128)(2,1)} %refs_1_.4, f32[2,2,128,128]{3,2,1,0:T(8,128)S(1)} %get-tuple-element.17.refs_2_.refs_1_, ...), custom_call_target="tpu_custom_call" | custom-call | flops 2000000 | tf_op jit(solution)/shard_map/pallas_call | solution.py:59
  39.2 1.7 %collective-permute-start.10 = (bf16[320,256]{1,0:T(8,128)(2,1)S(1)}, bf16[320,256]{1,0:T(8,128)(2,1)S(1)}, u32[]{:S(2)}, u32[]{:S(2)}) collective-permute-start(bf16[320,256]{1,0:T(8,128)(2,1)S(1)} %get-tuple-element.22.refs_2_), channel_id=1, source_target_pairs={{0,16},{8,24},{16,0},{24,8},{1,17},{9,25},{17,1},{25,9},{2,18},{10... | collective-permute-start | bytes 491528 | tf_op jit(solution)/shard_map/ppermute | solution.py:465
  41.0 1.5 %collective-permute-start.7 = (bf16[30,2048]{1,0:T(8,128)(2,1)S(1)}, bf16[30,2048]{1,0:T(8,128)(2,1)S(1)}, u32[]{:S(2)}, u32[]{:S(2)}) collective-permute-start(bf16[30,2048]{1,0:T(8,128)(2,1)S(1)} %collective-permute-done.refs_5_), channel_id=1, source_target_pairs={{0,1},{1,0},{2,3},{3,2},{4,5},{5,4},{6,7},{7,6},{8,9},{9,8},{10,11... | collective-permute-start | bytes 368648 | tf_op jit(solution)/shard_map/ppermute | solution.py:382
  43.1 1.6 %collective-permute-done.10.refs_3_ = bf16[320,256]{1,0:T(8,128)(2,1)S(1)} collective-permute-done((bf16[320,256]{1,0:T(8,128)(2,1)S(1)}, bf16[320,256]{1,0:T(8,128)(2,1)S(1)}, u32[]{:S(2)}, u32[]{:S(2)}) %collective-permute-start.10) | collective-permute-done | bytes 163872 | tf_op jit(solution)/shard_map/ppermute | solution.py:465
  44.8 2.7 %collective-permute-done.7.refs_4_ = bf16[30,2048]{1,0:T(8,128)(2,1)S(1)} collective-permute-done((bf16[30,2048]{1,0:T(8,128)(2,1)S(1)}, bf16[30,2048]{1,0:T(8,128)(2,1)S(1)}, u32[]{:S(2)}, u32[]{:S(2)}) %collective-permute-start.7) | collective-permute-done | bytes 122912 | tf_op jit(solution)/shard_map/ppermute | solution.py:382
  47.4 2.3 %collective-permute-done.9.refs_6_ = bf16[30,2048]{1,0:T(8,128)(2,1)S(1)} collective-permute-done((bf16[30,2048]{1,0:T(8,128)(2,1)S(1)}, bf16[30,2048]{1,0:T(8,128)(2,1)S(1)}, u32[]{:S(2)}, u32[]{:S(2)}) %collective-permute-start.9) | collective-permute-done | bytes 122912 | tf_op jit(solution)/shard_map/ppermute | solution.py:382
  49.7 1.6 %shard_map.103 = (bf16[128,128]{1,0:T(8,128)(2,1)S(1)}, bf16[128,256]{1,0:T(8,128)(2,1)S(1)}) custom-call(f32[2,6144]{1,0:T(2,128)S(1)} %get-tuple-element.19.refs_0_.refs_1_, f32[2,2,128,128]{3,2,1,0:T(8,128)S(1)} %get-tuple-element.17.refs_2_.refs_1_, bf16[2048,384]{1,0:T(8,128)(2,1)S(1)} %get-tuple-element.18.refs_3_.refs_2_, ...), custom_call_target="tpu_custom_call" | custom-call | flops 2000000 | tf_op jit(solution)/shard_map/pallas_call | solution.py:59
  51.8 3.9 %collective-permute-done.13.refs_7_ = bf16[128,256]{1,0:T(8,128)(2,1)S(1)} collective-permute-done((bf16[128,256]{1,0:T(8,128)(2,1)S(1)}, bf16[128,256]{1,0:T(8,128)(2,1)S(1)}, u32[]{:S(2)}, u32[]{:S(2)}) %collective-permute-start.13) | collective-permute-done | bytes 65568 | tf_op jit(solution)/shard_map/ppermute | solution.py:465
  56.3 1.7 %shard_map.104 = (f32[2,2,128,1]{3,2,1,0:T(8,128)S(1)}, f32[2,2,128,1]{3,2,1,0:T(8,128)S(1)}, f32[2,2,128,128]{3,2,1,0:T(8,128)S(1)}) custom-call(bf16[128,128]{1,0:T(8,128)(2,1)S(1)} %get-tuple-element.20.refs_0_.refs_4_, bf16[128,128]{1,0:T(8,128)(2,1)S(1)} %get-tuple-element.21.refs_1_.refs_5_, bf16[320,256]{1,0:T(8,128)(2,1)S(1)} %get-tuple-element.22.refs_2_, ...), custom_call_target="tpu_custom_call" | custom-call | flops 2000000 | tf_op jit(solution)/shard_map/pallas_call | solution.py:59
  58.1 1.7 %shard_map.105 = bf16[4,2,32,128]{3,2,1,0:T(8,128)(2,1)S(1)} custom-call(f32[1]{0:T(128)S(6)} %copy.11.refs_0_, f32[2,2,128,1]{3,2,1,0:T(8,128)S(1)} %get-tuple-element.23.refs_1_, f32[2,2,128,1]{3,2,1,0:T(8,128)S(1)} %get-tuple-element.24.refs_2_, f32[2,2,128,128]{3,2,1,0:T(8,128)S(1)} %get-tuple-element.25.refs_3_, ...), custom_call_target="tpu_custom_call" | custom-call | flops 2000000 | tf_op jit(solution)/shard_map/pallas_call | solution.py:59
  61.2 1.6 %collective-permute-start.17 = (bf16[2,32,128]{2,1,0:T(8,128)(2,1)S(1)}, bf16[2,32,128]{2,1,0:T(8,128)(2,1)S(1)}, u32[]{:S(2)}, u32[]{:S(2)}) collective-permute-start(bf16[2,32,128]{2,1,0:T(8,128)(2,1)S(1)} %get-tuple-element.30), channel_id=1, source_target_pairs={{0,4},{1,5},{2,6},{3,7},{4,0},{5,1},{6,2},{7,3},{8,12},{9,13},{10,... | collective-permute-start | bytes 49160 | tf_op jit(solution)/shard_map/ppermute | solution.py:374
  62.8 1.5 %collective-permute-start.18 = (bf16[2,32,128]{2,1,0:T(8,128)(2,1)S(1)}, bf16[2,32,128]{2,1,0:T(8,128)(2,1)S(1)}, u32[]{:S(2)}, u32[]{:S(2)}) collective-permute-start(bf16[2,32,128]{2,1,0:T(8,128)(2,1)S(1)} %get-tuple-element.29), channel_id=1, source_target_pairs={{0,6},{1,7},{2,4},{3,5},{4,2},{5,3},{6,0},{7,1},{8,14},{9,15},{10,... | collective-permute-start | bytes 49160 | tf_op jit(solution)/shard_map/ppermute | solution.py:374
  64.3 1.5 %collective-permute-done.17.refs_7_ = bf16[2,32,128]{2,1,0:T(8,128)(2,1)S(1)} collective-permute-done((bf16[2,32,128]{2,1,0:T(8,128)(2,1)S(1)}, bf16[2,32,128]{2,1,0:T(8,128)(2,1)S(1)}, u32[]{:S(2)}, u32[]{:S(2)}) %collective-permute-start.17) | collective-permute-done | bytes 16416 | tf_op jit(solution)/shard_map/ppermute | solution.py:374
  65.8 2.5 %collective-permute-done.18.refs_8_ = bf16[2,32,128]{2,1,0:T(8,128)(2,1)S(1)} collective-permute-done((bf16[2,32,128]{2,1,0:T(8,128)(2,1)S(1)}, bf16[2,32,128]{2,1,0:T(8,128)(2,1)S(1)}, u32[]{:S(2)}, u32[]{:S(2)}) %collective-permute-start.18) | collective-permute-done | bytes 16416 | tf_op jit(solution)/shard_map/ppermute | solution.py:374
  69.7 1.5 %collective-permute-start.19 = (bf16[32,2048]{1,0:T(8,128)(2,1)S(1)}, bf16[32,2048]{1,0:T(8,128)(2,1)S(1)}, u32[]{:S(2)}, u32[]{:S(2)}) collective-permute-start(bf16[32,2048]{1,0:T(8,128)(2,1)S(1)} %get-tuple-element.28), channel_id=1, source_target_pairs={{0,1},{1,0},{2,3},{3,2},{4,5},{5,4},{6,7},{7,6},{8,9},{9,8},{10,11... | collective-permute-start | bytes 393224 | tf_op jit(solution)/shard_map/ppermute | solution.py:382
  71.2 3.5 %collective-permute-done.19.refs_3_ = bf16[32,2048]{1,0:T(8,128)(2,1)S(1)} collective-permute-done((bf16[32,2048]{1,0:T(8,128)(2,1)S(1)}, bf16[32,2048]{1,0:T(8,128)(2,1)S(1)}, u32[]{:S(2)}, u32[]{:S(2)}) %collective-permute-start.19) | collective-permute-done | bytes 131104 | tf_op jit(solution)/shard_map/ppermute | solution.py:382
  (30 shorter events, 7.0 us)
Async XLA Ops:
  0.0 35.9 %copy-start = (bf16[30,2048]{1,0:T(8,128)(2,1)S(1)}, bf16[30,2048]{1,0:T(8,128)(2,1)}, u32[]{:S(2)}) copy-start(bf16[30,2048]{1,0:T(8,128)(2,1)} %refs_0_.2) | copy-start | bytes 368644
  0.0 15.8 %collective-permute-start.3 = (bf16[128,2048]{1,0:T(8,128)(2,1)}, bf16[128,2048]{1,0:T(8,128)(2,1)S(1)}, u32[]{:S(2)}, u32[]{:S(2)}) collective-permute-start(bf16[128,2048]{1,0:T(8,128)(2,1)} %refs_1_.5), channel_id=1, source_target_pairs={{0,4},{1,5},{2,6},{3,7},{4,0},{5,1},{6,2},{7,3},{8,10},{9,11},{10,... | collective-permute-start | bytes 1572872 | tf_op jit(solution)/shard_map/ppermute | solution.py:527
  15.8 25.1 %collective-permute-start.4 = (bf16[128,2048]{1,0:T(8,128)(2,1)S(1)}, bf16[128,2048]{1,0:T(8,128)(2,1)S(1)}, u32[]{:S(2)}, u32[]{:S(2)}) collective-permute-start(bf16[128,2048]{1,0:T(8,128)(2,1)S(1)} %collective-permute-done.3.refs_2_), channel_id=1, source_target_pairs={{0,10},{1,11},{2,8},{3,9},{4,14},{5,15},{6,12},{7,13},{8,0},{9,1},... | collective-permute-start | bytes 1572872 | tf_op jit(solution)/shard_map/ppermute | solution.py:527
  15.8 11.8 %collective-permute-start.1 = (bf16[30,2048]{1,0:T(8,128)(2,1)}, bf16[30,2048]{1,0:T(8,128)(2,1)}, u32[]{:S(2)}, u32[]{:S(2)}) collective-permute-start(bf16[30,2048]{1,0:T(8,128)(2,1)} %refs_0_.2), channel_id=1, source_target_pairs={{0,4},{1,5},{2,6},{3,7},{4,0},{5,1},{6,2},{7,3},{8,12},{9,13},{10,... | collective-permute-start | bytes 368648 | tf_op jit(solution)/shard_map/ppermute | solution.py:374
  20.0 15.6 %all-to-all-start = ((bf16[32,2,768]{2,1,0:T(2,128)(2,1)}), bf16[32,2,768]{2,1,0:T(2,128)(2,1)S(1)}, u32[]{:S(2)}, u32[]{:S(2)}) async-start(bf16[32,2,768]{2,1,0:T(2,128)(2,1)} %shard_map.100), calls=%async_computation | async-start | bytes 196608 | tf_op jit(solution)/shard_map/all_to_all | solution.py:399
  25.8 9.7 %collective-permute-start = (bf16[30,2048]{1,0:T(8,128)(2,1)}, bf16[30,2048]{1,0:T(8,128)(2,1)S(1)}, u32[]{:S(2)}, u32[]{:S(2)}) collective-permute-start(bf16[30,2048]{1,0:T(8,128)(2,1)} %refs_0_.2), channel_id=1, source_target_pairs={{0,2},{1,3},{2,0},{3,1},{4,6},{5,7},{6,4},{7,5},{8,10},{9,11},{10,... | collective-permute-start | bytes 368648 | tf_op jit(solution)/shard_map/ppermute | solution.py:374
  27.6 8.2 %collective-permute-start.2 = (bf16[30,2048]{1,0:T(8,128)(2,1)}, bf16[30,2048]{1,0:T(8,128)(2,1)S(1)}, u32[]{:S(2)}, u32[]{:S(2)}) collective-permute-start(bf16[30,2048]{1,0:T(8,128)(2,1)} %collective-permute-done.1.refs_6_), channel_id=1, source_target_pairs={{0,2},{1,3},{2,0},{3,1},{4,6},{5,7},{6,4},{7,5},{8,10},{9,11},{10,... | collective-permute-start | bytes 368648 | tf_op jit(solution)/shard_map/ppermute | solution.py:374
  32.0 10.6 %collective-permute-start.6 = (bf16[30,2048]{1,0:T(8,128)(2,1)}, bf16[30,2048]{1,0:T(8,128)(2,1)S(1)}, u32[]{:S(2)}, u32[]{:S(2)}) collective-permute-start(bf16[30,2048]{1,0:T(8,128)(2,1)} %refs_0_.2), channel_id=1, source_target_pairs={{0,1},{1,0},{2,3},{3,2},{4,5},{5,4},{6,7},{7,6},{8,9},{9,8},{10,11... | collective-permute-start | bytes 368648 | tf_op jit(solution)/shard_map/ppermute | solution.py:382
  34.9 8.2 %collective-permute-start.8 = (bf16[30,2048]{1,0:T(8,128)(2,1)}, bf16[30,2048]{1,0:T(8,128)(2,1)}, u32[]{:S(2)}, u32[]{:S(2)}) collective-permute-start(bf16[30,2048]{1,0:T(8,128)(2,1)} %collective-permute-done.1.refs_6_), channel_id=1, source_target_pairs={{0,1},{1,0},{2,3},{3,2},{4,5},{5,4},{6,7},{7,6},{8,9},{9,8},{10,11... | collective-permute-start | bytes 368648 | tf_op jit(solution)/shard_map/ppermute | solution.py:382
  39.2 5.6 %collective-permute-start.10 = (bf16[320,256]{1,0:T(8,128)(2,1)S(1)}, bf16[320,256]{1,0:T(8,128)(2,1)S(1)}, u32[]{:S(2)}, u32[]{:S(2)}) collective-permute-start(bf16[320,256]{1,0:T(8,128)(2,1)S(1)} %get-tuple-element.22.refs_2_), channel_id=1, source_target_pairs={{0,16},{8,24},{16,0},{24,8},{1,17},{9,25},{17,1},{25,9},{2,18},{10... | collective-permute-start | bytes 491528 | tf_op jit(solution)/shard_map/ppermute | solution.py:465
  40.9 27.5 %collective-permute-start.5 = (bf16[128,2048]{1,0:T(8,128)(2,1)S(1)}, bf16[128,2048]{1,0:T(8,128)(2,1)S(1)}, u32[]{:S(2)}, u32[]{:S(2)}) collective-permute-start(bf16[128,2048]{1,0:T(8,128)(2,1)S(1)} %broadcast_select_fusion), channel_id=1, source_target_pairs={{0,8},{8,0},{16,24},{24,16},{1,9},{9,1},{17,25},{25,17},{2,10},{10... | collective-permute-start | bytes 1572872 | tf_op jit(solution)/shard_map/ppermute | solution.py:534
  41.0 6.4 %collective-permute-start.7 = (bf16[30,2048]{1,0:T(8,128)(2,1)S(1)}, bf16[30,2048]{1,0:T(8,128)(2,1)S(1)}, u32[]{:S(2)}, u32[]{:S(2)}) collective-permute-start(bf16[30,2048]{1,0:T(8,128)(2,1)S(1)} %collective-permute-done.refs_5_), channel_id=1, source_target_pairs={{0,1},{1,0},{2,3},{3,2},{4,5},{5,4},{6,7},{7,6},{8,9},{9,8},{10,11... | collective-permute-start | bytes 368648 | tf_op jit(solution)/shard_map/ppermute | solution.py:382
  42.5 7.2 %collective-permute-start.9 = (bf16[30,2048]{1,0:T(8,128)(2,1)S(1)}, bf16[30,2048]{1,0:T(8,128)(2,1)S(1)}, u32[]{:S(2)}, u32[]{:S(2)}) collective-permute-start(bf16[30,2048]{1,0:T(8,128)(2,1)S(1)} %collective-permute-done.2.refs_7_), channel_id=1, source_target_pairs={{0,1},{1,0},{2,3},{3,2},{4,5},{5,4},{6,7},{7,6},{8,9},{9,8},{10,11... | collective-permute-start | bytes 368648 | tf_op jit(solution)/shard_map/ppermute | solution.py:382
  43.1 13.2 %collective-permute-start.11 = (bf16[320,256]{1,0:T(8,128)(2,1)S(1)}, bf16[320,256]{1,0:T(8,128)(2,1)S(1)}, u32[]{:S(2)}, u32[]{:S(2)}) collective-permute-start(bf16[320,256]{1,0:T(8,128)(2,1)S(1)} %get-tuple-element.22.refs_2_), channel_id=1, source_target_pairs={{0,8},{8,0},{16,24},{24,16},{1,9},{9,1},{17,25},{25,17},{2,10},{10... | collective-permute-start | bytes 491528 | tf_op jit(solution)/shard_map/ppermute | solution.py:475
  44.8 11.6 %collective-permute-start.12 = (bf16[320,256]{1,0:T(8,128)(2,1)S(1)}, bf16[320,256]{1,0:T(8,128)(2,1)S(1)}, u32[]{:S(2)}, u32[]{:S(2)}) collective-permute-start(bf16[320,256]{1,0:T(8,128)(2,1)S(1)} %collective-permute-done.10.refs_3_), channel_id=1, source_target_pairs={{0,8},{8,0},{16,24},{24,16},{1,9},{9,1},{17,25},{25,17},{2,10},{10... | collective-permute-start | bytes 491528 | tf_op jit(solution)/shard_map/ppermute | solution.py:475
  51.3 4.3 %collective-permute-start.13 = (bf16[128,256]{1,0:T(8,128)(2,1)S(1)}, bf16[128,256]{1,0:T(8,128)(2,1)S(1)}, u32[]{:S(2)}, u32[]{:S(2)}) collective-permute-start(bf16[128,256]{1,0:T(8,128)(2,1)S(1)} %get-tuple-element.26.refs_6_), channel_id=1, source_target_pairs={{0,16},{8,24},{16,0},{24,8},{1,17},{9,25},{17,1},{25,9},{2,18},{10... | collective-permute-start | bytes 196616 | tf_op jit(solution)/shard_map/ppermute | solution.py:465
  51.8 6.3 %collective-permute-start.14 = (bf16[128,256]{1,0:T(8,128)(2,1)S(1)}, bf16[128,256]{1,0:T(8,128)(2,1)S(1)}, u32[]{:S(2)}, u32[]{:S(2)}) collective-permute-start(bf16[128,256]{1,0:T(8,128)(2,1)S(1)} %get-tuple-element.26.refs_6_), channel_id=1, source_target_pairs={{0,8},{8,0},{16,24},{24,16},{1,9},{9,1},{17,25},{25,17},{2,10},{10... | collective-permute-start | bytes 196616 | tf_op jit(solution)/shard_map/ppermute | solution.py:475
  55.7 2.4 %collective-permute-start.15 = (bf16[128,256]{1,0:T(8,128)(2,1)S(1)}, bf16[128,256]{1,0:T(8,128)(2,1)S(1)}, u32[]{:S(2)}, u32[]{:S(2)}) collective-permute-start(bf16[128,256]{1,0:T(8,128)(2,1)S(1)} %collective-permute-done.13.refs_7_), channel_id=1, source_target_pairs={{0,8},{8,0},{16,24},{24,16},{1,9},{9,1},{17,25},{25,17},{2,10},{10... | collective-permute-start | bytes 196616 | tf_op jit(solution)/shard_map/ppermute | solution.py:475
  59.8 4.5 %collective-permute-start.16 = (bf16[2,32,128]{2,1,0:T(8,128)(2,1)S(1)}, bf16[2,32,128]{2,1,0:T(8,128)(2,1)S(1)}, u32[]{:S(2)}, u32[]{:S(2)}) collective-permute-start(bf16[2,32,128]{2,1,0:T(8,128)(2,1)S(1)} %get-tuple-element.31), channel_id=1, source_target_pairs={{0,2},{1,3},{2,0},{3,1},{4,6},{5,7},{6,4},{7,5},{8,10},{9,11},{10,... | collective-permute-start | bytes 49160 | tf_op jit(solution)/shard_map/ppermute | solution.py:374
  61.2 4.6 %collective-permute-start.17 = (bf16[2,32,128]{2,1,0:T(8,128)(2,1)S(1)}, bf16[2,32,128]{2,1,0:T(8,128)(2,1)S(1)}, u32[]{:S(2)}, u32[]{:S(2)}) collective-permute-start(bf16[2,32,128]{2,1,0:T(8,128)(2,1)S(1)} %get-tuple-element.30), channel_id=1, source_target_pairs={{0,4},{1,5},{2,6},{3,7},{4,0},{5,1},{6,2},{7,3},{8,12},{9,13},{10,... | collective-permute-start | bytes 49160 | tf_op jit(solution)/shard_map/ppermute | solution.py:374
  62.8 5.5 %collective-permute-start.18 = (bf16[2,32,128]{2,1,0:T(8,128)(2,1)S(1)}, bf16[2,32,128]{2,1,0:T(8,128)(2,1)S(1)}, u32[]{:S(2)}, u32[]{:S(2)}) collective-permute-start(bf16[2,32,128]{2,1,0:T(8,128)(2,1)S(1)} %get-tuple-element.29), channel_id=1, source_target_pairs={{0,6},{1,7},{2,4},{3,5},{4,2},{5,3},{6,0},{7,1},{8,14},{9,15},{10,... | collective-permute-start | bytes 49160 | tf_op jit(solution)/shard_map/ppermute | solution.py:374
  69.7 5.0 %collective-permute-start.19 = (bf16[32,2048]{1,0:T(8,128)(2,1)S(1)}, bf16[32,2048]{1,0:T(8,128)(2,1)S(1)}, u32[]{:S(2)}, u32[]{:S(2)}) collective-permute-start(bf16[32,2048]{1,0:T(8,128)(2,1)S(1)} %get-tuple-element.28), channel_id=1, source_target_pairs={{0,1},{1,0},{2,3},{3,2},{4,5},{5,4},{6,7},{7,6},{8,9},{9,8},{10,11... | collective-permute-start | bytes 393224 | tf_op jit(solution)/shard_map/ppermute | solution.py:382

commit v4 on v3

--- a/solution.py
+++ b/solution.py
@@ -71,7 +71,24 @@
     return jax.ShapeDtypeStruct(shape, dtype)
 
 
-def partial_body(latent_hbm, context_hbm, weight_hbm, out_ref, cond_ref, weight_ref, sems):
+def fetch_weights(sources, weight_ref, sems):
+    moves, start = [], 0
+    for i, source in enumerate(sources):
+        columns = source.shape[1]
+        moves.append(
+            pltpu.make_async_copy(source, weight_ref.at[:, start : start + columns], sems.at[i])
+        )
+        moves[-1].start()
+        start += columns
+    return moves
+
+
+def prepare_body(number, pad, ranks, outer, inner, *refs):
+    here_ref, latent_hbm, context_hbm, weight_hbm = refs[:4]
+    sources, exit_hbm = refs[4:7], refs[7]
+    out_ref, table_ref, joined_ref, upper_ref, lower_ref = refs[8:13]
+    cond_ref, weight_ref, sems, more_sems = refs[13:]
+    half = upper_ref.shape[0]
     moves = [
         pltpu.make_async_copy(weight_hbm, weight_ref, sems.at[0]),
         pltpu.make_async_copy(latent_hbm, cond_ref.at[0:1], sems.at[1]),
@@ -79,22 +96,27 @@
     ]
     for move in moves:
         move.start()
+    more = fetch_weights(sources, joined_ref, more_sems)
+    more += [
+        pltpu.make_async_copy(exit_hbm.at[:half], upper_ref, sems.at[3]),
+        pltpu.make_async_copy(exit_hbm.at[half:], lower_ref, sems.at[4]),
+    ]
+    more[-2].start()
+    more[-1].start()
+    make_tables(number, pad, ranks, outer, inner, here_ref[0], table_ref)
     moves[1].wait()
     moves[2].wait()
     rows = cond_ref[...]
     rows = (rows / (1.0 + jnp.exp(-rows))).astype(BF16)
     moves[0].wait()
-    part = jnp.dot(rows, weight_ref[...], preferred_element_type=F32)
-    part = part.astype(BF16)
+    part = jnp.dot(rows, weight_ref[...], preferred_element_type=F32).astype(BF16)
     for i in range(out_ref.shape[0]):
         out_ref[i] = part
-
-
-def table_body(number, pad, ranks, outer, inner, *refs):
-    here_ref = refs[0]
-    sources, (out_ref, weight_ref, sems) = refs[1:4], refs[4:]
-    moves = fetch_weights(sources, weight_ref, sems)
-    here = here_ref[0]
+    for move in more:
+        move.wait()
+
+
+def make_tables(number, pad, ranks, outer, inner, here, out_ref):
     group, rank = lax.div(here, ranks), lax.rem(here, ranks)
     here_outer, here_inner = lax.div(rank, inner), lax.rem(rank, inner)
     lane = lax.broadcasted_iota(jnp.int32, (pad, 2 * QK_DIM), 1)
@@ -121,20 +143,6 @@
             other = pltpu.roll(wave, QK_DIM, 1)
             out_ref[j, 0, k * pad : (k + 1) * pad, :] = jnp.where(low, wave, other)
             out_ref[j, 1, k * pad : (k + 1) * pad, :] = jnp.where(low, other, wave) * sign
-    for move in moves:
-        move.wait()
-
-
-def fetch_weights(sources, weight_ref, sems):
-    moves, start = [], 0
-    for i, source in enumerate(sources):
-        columns = source.shape[1]
-        moves.append(
-            pltpu.make_async_copy(source, weight_ref.at[:, start : start + columns], sems.at[i])
-        )
-        moves[-1].start()
-        start += columns
-    return moves
 
 
 def modulated(values, shift, scale):
@@ -162,23 +170,11 @@
     return (u * cosine + turned * sine).astype(BF16)
 
 
-def project_rows(rows, weight_ref, table_ref, j, q_ref, kv_ref):
-    number = rows.shape[0]
-    wide = 2 * QK_DIM
-    cosine, sine = table_ref[j, 0], table_ref[j, 1]
-    u = jnp.dot(rows, weight_ref[...], preferred_element_type=F32)
-    q_ref[...] = turn(u[:, :wide], cosine, sine)
-    kv_ref[0:number, :wide] = turn(u[:, wide : 2 * wide], cosine, sine)
-    kv_ref[0:number, wide:] = u[:, 2 * wide :].astype(BF16)
-
-
-def first_body(pad, ranks, count, *refs):
-    pieces_ref, context_hbm, table_ref, weight_ref = refs[:4]
-    blocks = refs[4 : 4 + count]
-    mod_ref, q_ref, kv_ref, rows_ref, context_ref, sem = refs[4 + count :]
+def context_body(ranks, *refs):
+    pieces_ref, context_hbm, weight_ref, mod_ref, kv_ref, context_ref, sem = refs
     move = pltpu.make_async_copy(context_hbm, context_ref, sem)
     move.start()
-    width = context_ref.shape[1]
+    held, width = context_ref.shape
     columns = pieces_ref.shape[2]
     groups = pieces_ref.shape[0] // ranks
     for t in range(ranks):
@@ -186,57 +182,54 @@
         for s in range(1, groups):
             total = total + pieces_ref[s * ranks + t].astype(F32)
         mod_ref[:, t * columns : (t + 1) * columns] = total
-    mod = mod_ref[...]
-    fill_rows(blocks, rows_ref, pad, mod[0:1, :width], 1.0 + mod[0:1, width : 2 * width])
-    project_rows(rows_ref[...], weight_ref, table_ref, 0, q_ref, kv_ref)
-    shift, scale = mod[1:2, :width], 1.0 + mod[1:2, width : 2 * width]
-    held = context_ref.shape[0]
+    shift, scale = mod_ref[1:2, :width], 1.0 + mod_ref[1:2, width : 2 * width]
     step = 16 if held % 16 == 0 else held
     move.wait()
     for i in range(0, held, step):
         context_ref[i : i + step, :] = modulated(context_ref[i : i + step, :], shift, scale)
-    base = count * pad
-    wide = 2 * QK_DIM
-    kv_ref[base : base + held, :] = jnp.dot(
-        context_ref[...], weight_ref[:, wide:], preferred_element_type=F32
+    kv_ref[...] = jnp.dot(
+        context_ref[...], weight_ref[:, 2 * QK_DIM :], preferred_element_type=F32
     ).astype(BF16)
 
 
-def second_body(pad, count, j, *refs):
+def rows_body(pad, outer, inner, *refs):
     mod_ref, table_ref, weight_ref = refs[:3]
-    blocks = refs[3 : 3 + count]
-    q_ref, kv_ref, rows_ref = refs[3 + count :]
+    blocks = refs[3:-3]
+    q_ref, kv_ref, rows_ref = refs[-3:]
     width = blocks[0].shape[1]
     fill_rows(
         blocks, rows_ref, pad, mod_ref[0:1, :width], 1.0 + mod_ref[0:1, width : 2 * width]
     )
-    project_rows(rows_ref[...], weight_ref, table_ref, j, q_ref, kv_ref)
-
-
-def gather_pieces(pieces, k_all, v_all, number, pad):
+    tile, wide = outer * pad, 2 * QK_DIM
+    product = jnp.dot(rows_ref[...], weight_ref[...], preferred_element_type=F32)
+    for j in range(inner):
+        u = product[j * tile : (j + 1) * tile]
+        cosine, sine = table_ref[j, 0], table_ref[j, 1]
+        scale = jnp.asarray(QK_DIM ** (-0.5), BF16)
+        q_ref[j] = turn(u[:, :wide], cosine, sine) * scale
+        kv_ref[j * tile : (j + 1) * tile, :wide] = turn(u[:, wide : 2 * wide], cosine, sine)
+        kv_ref[j * tile : (j + 1) * tile, wide:] = u[:, 2 * wide :].astype(BF16)
+
+
+def gather_pieces(pieces, padded, number, pad, k_all, v_all):
     wide = 2 * QK_DIM
-    row = 0
-    for piece, rows in pieces:
-        k_all[row : row + rows, :] = piece[0:rows, :wide]
-        v_all[row : row + rows, :] = piece[0:rows, wide:]
+    row = latents = 0
+    for i, piece in enumerate(pieces):
+        rows = piece.shape[0]
+        k_all[row : row + rows, :] = piece[:, :wide]
+        v_all[row : row + rows, :] = piece[:, wide:]
         row += rows
-    latents = row
-    for piece, rows in pieces:
-        held = piece.shape[0] - rows
-        if held:
-            k_all[row : row + held, :] = piece[rows : rows + held, :wide]
-            v_all[row : row + held, :] = piece[rows : rows + held, wide:]
-            row += held
+        latents += rows if i < padded else 0
     column = lax.broadcasted_iota(jnp.int32, (1, row), 1)
     valid = (column >= latents) | (column % pad < number)
     return jnp.where(valid, 0.0, -1e30)
 
 
-def score(q_all, j, m, k_all, bias):
-    queries = q_all[j] * jnp.asarray(QK_DIM ** (-0.5), BF16)
+def score(q_ref, j, m, k_all):
+    queries = q_ref[j]
     lane = lax.broadcasted_iota(jnp.int32, queries.shape, 1)
     own = jnp.where((lane // QK_DIM) == m, queries, jnp.zeros_like(queries))
-    return bias + lax.dot_general(
+    return lax.dot_general(
         own, k_all[...], (((1,), (1,)), ((), ())), preferred_element_type=F32
     )
 
@@ -249,16 +242,14 @@
         lax.fori_loop(0, count, one, 0)
 
 
-def attend_first_body(number, pad, tile, inner, *refs):
-    q_refs, kv_refs = refs[:inner], refs[inner:-6]
-    top_ref, sum_ref, mix_ref, q_all, k_all, v_all = refs[-6:]
-    for j in range(inner):
-        q_all[j] = q_refs[j][...]
-    bias = gather_pieces([(v, tile) for v in kv_refs], k_all, v_all, number, pad)
+def attend_first_body(number, pad, padded, inner, *refs):
+    q_ref, kv_refs = refs[0], refs[1:-5]
+    top_ref, sum_ref, mix_ref, k_all, v_all = refs[-5:]
+    bias = gather_pieces(kv_refs, padded, number, pad, k_all, v_all)
 
     def one(j, carry):
         for m in range(2):
-            scores = score(q_all, j, m, k_all, bias)
+            scores = score(q_ref, j, m, k_all) + bias
             highest = jnp.max(scores, axis=-1, keepdims=True)
             weights = jnp.exp(scores - highest)
             top_ref[j, m] = highest
@@ -271,18 +262,15 @@
     repeat(inner, one)
 
 
-def attend_last_body(number, pad, tile, outer, inner, *refs):
-    factor_ref, top_ref, sum_ref, mix_ref = refs[:4]
-    q_refs, kv_refs = refs[4 : 4 + inner], refs[4 + inner : -4]
-    out_ref, q_all, k_all, v_all = refs[-4:]
-    for j in range(inner):
-        q_all[j] = q_refs[j][...]
-    bias = gather_pieces([(v, tile) for v in kv_refs], k_all, v_all, number, pad)
+def attend_last_body(number, pad, outer, inner, *refs):
+    factor_ref, top_ref, sum_ref, mix_ref, q_ref = refs[:5]
+    kv_refs, (out_ref, k_all, v_all) = refs[5:-3], refs[-3:]
+    bias = gather_pieces(kv_refs, len(kv_refs), number, pad, k_all, v_all)
 
     def one(j, carry):
         mixed = []
         for m in range(2):
-            scores = score(q_all, j, m, k_all, bias)
+            scores = score(q_ref, j, m, k_all) + bias
             before = top_ref[j, m]
             highest = jnp.maximum(before, jnp.max(scores, axis=-1, keepdims=True))
             fade = jnp.exp(before - highest)
@@ -302,14 +290,13 @@
     repeat(inner, one)
 
 
-def partial_out_body(slots, share, ranks, inner, pad, *refs):
+def partial_out_body(slots, share, ranks, outer, inner, pad, *refs):
     here_ref, own_hbm = refs[:2]
     held = refs[2 : 2 + len(slots)]
     rest = refs[2 + len(slots) : -2]
     own_weight, sem = refs[-2:]
     move = pltpu.make_async_copy(own_hbm, own_weight, sem)
     move.start()
-    outer = 1 + len(slots)
     parts, own_ref, others = rest[:outer], rest[outer], rest[1 + outer :]
     rows = inner * pad
     side = lax.rem(lax.div(here_ref[0], ranks), share)
@@ -318,9 +305,11 @@
     def part(k):
         return parts[k][...].reshape(rows, VAL_DIM)
 
-    total = None
+    total, start = None, 0
     for (a, b), weight in zip(slots, held):
         rows_in = part(a) if a == b else jnp.where(first, part(a), part(b))
+        rows_in = rows_in[:, start : start + weight.shape[0]]
+        start = (start + weight.shape[0]) % VAL_DIM
         term = jnp.dot(rows_in, weight[...], preferred_element_type=F32)
         total = term if total is None else total + term
     move.wait()
@@ -382,18 +371,33 @@
         return lax.ppermute(value, "tp", pairs)
 
     columns = mod_weight.shape[1]
-    copies = call(
-        partial_body,
-        sds((groups * ranks, 2, columns), BF16),
+    here = (here_sp * ranks + here_tp).astype(jnp.int32).reshape(1)
+    depth = w_out.shape[0]
+    half = sds((depth // 2, width), BF16)
+    copies, table, weight, *halves = call(
+        functools.partial(prepare_body, number, pad, ranks, outer, inner),
+        (
+            sds((groups * ranks, 2, columns), BF16),
+            sds((inner, 2, tile, wide), F32),
+            sds((width, wide + wide + VAL_DIM), BF16),
+            half,
+            half,
+        ),
+        here,
         cond_latent.reshape(1, -1),
         cond_context.reshape(1, -1),
         mod_weight,
+        w_query,
+        w_key,
+        w_value,
+        w_out,
         scratch=[
             pltpu.VMEM((2, cond_latent.shape[0]), F32),
             pltpu.VMEM(mod_weight.shape, BF16),
+            pltpu.SemaphoreType.DMA((5,)),
             pltpu.SemaphoreType.DMA((3,)),
         ],
-        in_specs=[HBM] * 3,
+        in_specs=[SMEM] + [HBM] * 7,
         local=True,
     )
     pieces = lax.all_to_all(copies, ("sp", "tp"), 0, 0)
@@ -408,51 +412,27 @@
         for k in range(outer):
             blocks[k, j] = along_inner(blocks[k, 0], j, ahead)
 
-    here = (here_sp * ranks + here_tp).astype(jnp.int32).reshape(1)
-    joined = wide + wide + VAL_DIM
-    table, weight = call(
-        functools.partial(table_body, number, pad, ranks, outer, inner),
-        (sds((inner, 2, tile, wide), F32), sds((width, joined), BF16)),
-        here,
-        w_query,
-        w_key,
-        w_value,
-        scratch=[pltpu.SemaphoreType.DMA((3,))],
-        in_specs=[SMEM] + [HBM] * 3,
-        local=True,
-    )
-    mod, q_first, kv_first = call(
-        functools.partial(first_body, pad, ranks, outer),
-        (
-            sds((2, columns * ranks), F32),
-            sds((tile, wide), BF16),
-            sds((tile + held, wide + VAL_DIM), BF16),
-        ),
+    mod, kv_context = call(
+        functools.partial(context_body, ranks),
+        (sds((2, columns * ranks), F32), sds((held, wide + VAL_DIM), BF16)),
         pieces,
         context,
+        weight,
+        scratch=[pltpu.VMEM((held, width), BF16), pltpu.SemaphoreType.DMA],
+        in_specs=[VMEM, HBM, VMEM],
+        local=True,
+    )
+    queries, kv = call(
+        functools.partial(rows_body, pad, outer, inner),
+        (sds((inner, tile, wide), BF16), sds((inner * tile, wide + VAL_DIM), BF16)),
+        mod,
         table,
         weight,
-        *[blocks[k, 0] for k in range(outer)],
-        scratch=[
-            pltpu.VMEM((tile, width), BF16),
-            pltpu.VMEM((held, width), BF16),
-            pltpu.SemaphoreType.DMA,
-        ],
-        in_specs=[VMEM, HBM] + [VMEM] * (2 + outer),
-    )
-    queries, kv = [q_first], [kv_first]
-    for j in range(1, inner):
-        q_next, kv_next = call(
-            functools.partial(second_body, pad, outer, j),
-            (sds((tile, wide), BF16), sds((tile, wide + VAL_DIM), BF16)),
-            mod,
-            table,
-            weight,
-            *[blocks[k, j] for k in range(outer)],
-            scratch=[pltpu.VMEM((tile, width), BF16)],
-        )
-        queries.append(q_next)
-        kv.append(kv_next)
+        *[blocks[k, j] for j in range(inner) for k in range(outer)],
+        scratch=[pltpu.VMEM((inner * tile, width), BF16)],
+        extra=inner * tile * 6 * QK_DIM * 4,
+        local=True,
+    )
     share = share_of(groups)
     lines = groups // share
 
@@ -475,8 +455,10 @@
                 pieces.append(lax.ppermute(piece, "sp", swap))
         return pieces
 
-    kv = [spread(part) for part in kv]
-    early, late = kv[0], sum(kv[1:], [])
+    near, late = spread(kv_context), spread(kv)
+    first = [i for i in range(len(late)) if i % lines == 0]
+    early = [late[i] for i in first] + near
+    late = [v for i, v in enumerate(late) if i not in first]
     stats = (
         sds((inner, 2, tile, 1), F32),
         sds((inner, 2, tile, 1), F32),
@@ -484,32 +466,30 @@
     )
 
     def room(keys):
-        return [
-            pltpu.VMEM((inner, tile, wide), BF16),
-            pltpu.VMEM((keys, wide), BF16),
-            pltpu.VMEM((keys, VAL_DIM), BF16),
-        ]
-
-    keys = groups * (tile + held)
+        return [pltpu.VMEM((keys, wide), BF16), pltpu.VMEM((keys, VAL_DIM), BF16)]
+
+    keys = groups * held + len(first) * inner * tile
     first_stats = call(
-        functools.partial(attend_first_body, number, pad, tile, inner),
+        functools.partial(attend_first_body, number, pad, len(first), inner),
         stats,
-        *queries,
+        queries,
         *early,
         scratch=room(keys),
         extra=tile * keys * 12,
-    )
-    keys = groups * (inner - 1) * tile
+        local=True,
+    )
+    keys = len(late) * inner * tile
     attended = call(
-        functools.partial(attend_last_body, number, pad, tile, outer, inner),
+        functools.partial(attend_last_body, number, pad, outer, inner),
         sds((outer, inner, pad, VAL_DIM), BF16),
         head_lambda,
         *first_stats,
-        *queries,
+        queries,
         *late,
         scratch=room(keys),
         extra=tile * keys * 12,
-        in_specs=[SMEM] + [VMEM] * (3 + inner + len(late)),
+        in_specs=[SMEM] + [VMEM] * (4 + len(late)),
+        local=True,
     )
     parts = [attended[0]]
     for k in range(1, outer):
@@ -528,18 +508,24 @@
 
     slots, weights = [], []
     if share > 1 and outer == 4:
-        fetched = joint(w_out, lambda s, o: (s, behind(o, 1 if s % 2 else 2, outer)))
-        turned = joint(fetched, lambda s, o: (s ^ 1, o if s % 2 else behind(o, 1, outer)))
-        given = jnp.where(here_sp % 2 == 0, fetched, turned)
-        traded = lax.ppermute(given, "sp", swap)
-        slots, weights = [(2, 1), (1, 3), (3, 2)], [fetched, turned, traded]
+        fetched, turned = [], []
+        for i, part in enumerate(halves):
+            fetched.append(
+                joint(part, lambda s, o: (s, behind(o, 1 if s % 2 else 2, outer)))
+            )
+            turned.append(
+                joint(fetched[i], lambda s, o: (s ^ 1, o if s % 2 else behind(o, 1, outer)))
+            )
+        given = [jnp.where(here_sp % 2 == 0, a, b) for a, b in zip(fetched, turned)]
+        traded = lax.ppermute(jnp.concatenate(given, axis=0), "sp", swap)
+        slots = [(2, 1), (2, 1), (1, 3), (1, 3), (3, 2)]
+        weights = [*fetched, *turned, traded]
     else:
         for k in range(1, outer):
             weights.append(along_outer(w_out, k, behind))
             slots.append((k, k))
-    depth = w_out.shape[0]
     total = call(
-        functools.partial(partial_out_body, slots, share, ranks, inner, pad),
+        functools.partial(partial_out_body, slots, share, ranks, outer, inner, pad),
         (sds((pad, width), F32),) + (sds((pad, width), BF16),) * (inner - 1),
         here,
         w_out,

time: 75.8 us -> 77 us (1.016)
  Pallas kernels: 13.9 us -> 12.3 us
  other arithmetic: 0.06 us -> 0.9 us
  starting transfers between devices: 30.6 us -> 31.4 us
    ppermute x6, waiting for transfers between devices: 4.41 us -> 10.1 us  [along_outer(): return lax.ppermute(value, 'tp', pairs)]
    ppermute x5, waiting for transfers between devices: 8.47 us -> 4.31 us  [along_inner(): return lax.ppermute(value, 'tp', pairs)]
    all_to_all x1, starting transfers between devices: 5.82 us -> 3.53 us  [shards(): pieces = lax.all_to_all(copies, ('sp', 'tp'), 0, 0)]
    ppermute x1, starting transfers between devices: 0.07 us -> 1.8 us  [shards(): traded = lax.ppermute(jnp.concatenate(given, axis=0), 'sp', swap)]
    pallas_call x8 -> x7, Pallas kernels: 13.9 us -> 12.3 us  [call(): pl.pallas_call(body, out_shape=outs, in_specs=in_specs, out_specs=jax.tre...]
    ppermute x2 -> x4, waiting for transfers between devices: 11.7 us -> 10.5 us  [joint(): return lax.ppermute(value, ('sp', 'tp'), moves)]
    concatenate x0 -> x1, other arithmetic: none -> 0.85 us  [shards(): traded = lax.ppermute(jnp.concatenate(given, axis=0), 'sp', swap)]
    ppermute x2 -> x4, starting transfers between devices: 4.07 us -> 4.44 us  [joint(): return lax.ppermute(value, ('sp', 'tp'), moves)]
  transfers between devices with their start and end apart: 21 -> 23, of which waited for: 9 -> 9; matrix products, arithmetic and copies ran while one was open for 0% -> 1% of each run, Pallas kernels for 16% -> 10%
where the time goes in v4:
time: 77 us; the launch traced here: 76.7 us
  starting transfers between devices  31.4 us (41%)
  waiting for transfers between devices  30.6 us (40%)
  Pallas kernels  12.3 us (16%)
  other arithmetic  0.9 us (1%)
  between operations  0.82 us (1%)
    ppermute x6, starting transfers between devices, along_outer(): return lax.ppermute(value, 'tp', pairs)  12.9 us
    pallas_call x7, Pallas kernels, call(): pl.pallas_call(body, out_shape=outs, in_specs=in_specs, out_specs=jax.tre...  12.3 us
    ppermute x4, waiting for transfers between devices, joint(): return lax.ppermute(value, ('sp', 'tp'), moves)  10.5 us
    ppermute x6, waiting for transfers between devices, along_outer(): return lax.ppermute(value, 'tp', pairs)  10.1 us
    ppermute x5, starting transfers between devices, along_inner(): return lax.ppermute(value, 'tp', pairs)  6.08 us
    ppermute x2, waiting for transfers between devices, along_lines(): return lax.ppermute(value, 'sp', pairs)  4.98 us
    ppermute x4, starting transfers between devices, joint(): return lax.ppermute(value, ('sp', 'tp'), moves)  4.44 us
    ppermute x5, waiting for transfers between devices, along_inner(): return lax.ppermute(value, 'tp', pairs)  4.31 us
  transfers between devices with their start and end apart: 23, of which 9 were waited for; matrix products, arithmetic and copies ran while one was open for 1% of the time, Pallas kernels for 10%

profile of v4, /device:TPU:0, one launch (start us, length us, event | category | flops | bytes accessed | tf_op | source)
XLA Modules:
  0.0 76.7 jit_solution(7662596286207806424)
XLA Ops:
  0.0 2.7 %shard_map.100 = (bf16[32,2,768]{2,1,0:T(2,128)(2,1)}, f32[2,2,128,128]{3,2,1,0:T(8,128)S(1)}, bf16[2048,384]{1,0:T(8,128)(2,1)S(1)}, bf16[64,2048]{1,0:T(8,128)(2,1)S(1)}, bf16[64,2048]{1,0:T(8,128)(2,1)S(1)}) custom-call(s32[1]{0:T(128)} %bitcast.refs_0_, f32[1,512]{1,0:T(1,128)} %bitcast.11, f32[1,512]{1,0:T(1,128)} %bitcast.12, ...), custom_call_target="tpu_custom_call" | custom-call | flops 2000000 | tf_op jit(solution)/shard_map/pallas_call | solution.py:59
  3.4 4.1 %collective-permute-start = (bf16[64,2048]{1,0:T(8,128)(2,1)S(1)}, bf16[64,2048]{1,0:T(8,128)(2,1)S(1)}, u32[]{:S(2)}, u32[]{:S(2)}) collective-permute-start(bf16[64,2048]{1,0:T(8,128)(2,1)S(1)} %get-tuple-element.22), channel_id=1, source_target_pairs={{0,4},{1,5},{2,6},{3,7},{4,0},{5,1},{6,2},{7,3},{8,10},{9,11},{10,... | collective-permute-start | bytes 786440 | tf_op jit(solution)/shard_map/ppermute | solution.py:507
  7.5 6.7 %collective-permute-done.refs_2_ = bf16[64,2048]{1,0:T(8,128)(2,1)S(1)} collective-permute-done((bf16[64,2048]{1,0:T(8,128)(2,1)S(1)}, bf16[64,2048]{1,0:T(8,128)(2,1)S(1)}, u32[]{:S(2)}, u32[]{:S(2)}) %collective-permute-start) | collective-permute-done | bytes 262176 | tf_op jit(solution)/shard_map/ppermute | solution.py:507
  14.2 3.4 %collective-permute-start.6 = (bf16[30,2048]{1,0:T(8,128)(2,1)S(1)}, bf16[30,2048]{1,0:T(8,128)(2,1)S(1)}, u32[]{:S(2)}, u32[]{:S(2)}) collective-permute-start(bf16[30,2048]{1,0:T(8,128)(2,1)S(1)} %copy-done), channel_id=1, source_target_pairs={{0,4},{1,5},{2,6},{3,7},{4,0},{5,1},{6,2},{7,3},{8,12},{9,13},{10,... | collective-permute-start | bytes 368648 | tf_op jit(solution)/shard_map/ppermute | solution.py:363
  17.5 1.6 %collective-permute-start.5 = (bf16[30,2048]{1,0:T(8,128)(2,1)S(1)}, bf16[30,2048]{1,0:T(8,128)(2,1)}, u32[]{:S(2)}, u32[]{:S(2)}) collective-permute-start(bf16[30,2048]{1,0:T(8,128)(2,1)S(1)} %copy-done), channel_id=1, source_target_pairs={{0,2},{1,3},{2,0},{3,1},{4,6},{5,7},{6,4},{7,5},{8,10},{9,11},{10,... | collective-permute-start | bytes 368648 | tf_op jit(solution)/shard_map/ppermute | solution.py:363
  19.1 5.6 %collective-permute-done.6.refs_5_ = bf16[30,2048]{1,0:T(8,128)(2,1)S(1)} collective-permute-done((bf16[30,2048]{1,0:T(8,128)(2,1)S(1)}, bf16[30,2048]{1,0:T(8,128)(2,1)S(1)}, u32[]{:S(2)}, u32[]{:S(2)}) %collective-permute-start.6) | collective-permute-done | bytes 122912 | tf_op jit(solution)/shard_map/ppermute | solution.py:363
  24.7 3.5 %collective-permute-start.7 = (bf16[30,2048]{1,0:T(8,128)(2,1)S(1)}, bf16[30,2048]{1,0:T(8,128)(2,1)}, u32[]{:S(2)}, u32[]{:S(2)}) collective-permute-start(bf16[30,2048]{1,0:T(8,128)(2,1)S(1)} %collective-permute-done.6.refs_5_), channel_id=1, source_target_pairs={{0,2},{1,3},{2,0},{3,1},{4,6},{5,7},{6,4},{7,5},{8,10},{9,11},{10,... | collective-permute-start | bytes 368648 | tf_op jit(solution)/shard_map/ppermute | solution.py:363
  28.2 1.5 %collective-permute-start.8 = (bf16[30,2048]{1,0:T(8,128)(2,1)S(1)}, bf16[30,2048]{1,0:T(8,128)(2,1)}, u32[]{:S(2)}, u32[]{:S(2)}) collective-permute-start(bf16[30,2048]{1,0:T(8,128)(2,1)S(1)} %copy-done), channel_id=1, source_target_pairs={{0,1},{1,0},{2,3},{3,2},{4,5},{5,4},{6,7},{7,6},{8,9},{9,8},{10,11... | collective-permute-start | bytes 368648 | tf_op jit(solution)/shard_map/ppermute | solution.py:371
  29.7 3.5 %all-to-all-start = ((bf16[32,2,768]{2,1,0:T(2,128)(2,1)}), bf16[32,2,768]{2,1,0:T(2,128)(2,1)S(1)}, u32[]{:S(2)}, u32[]{:S(2)}) async-start(bf16[32,2,768]{2,1,0:T(2,128)(2,1)} %get-tuple-element.19), calls=%async_computation | async-start | bytes 196608 | tf_op jit(solution)/shard_map/all_to_all | solution.py:403
  33.2 1.8 %collective-permute-start.10 = (bf16[30,2048]{1,0:T(8,128)(2,1)S(1)}, bf16[30,2048]{1,0:T(8,128)(2,1)}, u32[]{:S(2)}, u32[]{:S(2)}) collective-permute-start(bf16[30,2048]{1,0:T(8,128)(2,1)S(1)} %collective-permute-done.6.refs_5_), channel_id=1, source_target_pairs={{0,1},{1,0},{2,3},{3,2},{4,5},{5,4},{6,7},{7,6},{8,9},{9,8},{10,11... | collective-permute-start | bytes 368648 | tf_op jit(solution)/shard_map/ppermute | solution.py:371
  35.3 1.8 %collective-permute-start.11 = (bf16[30,2048]{1,0:T(8,128)(2,1)}, bf16[30,2048]{1,0:T(8,128)(2,1)}, u32[]{:S(2)}, u32[]{:S(2)}) collective-permute-start(bf16[30,2048]{1,0:T(8,128)(2,1)} %collective-permute-done.7.refs_6_), channel_id=1, source_target_pairs={{0,1},{1,0},{2,3},{3,2},{4,5},{5,4},{6,7},{7,6},{8,9},{9,8},{10,11... | collective-permute-start | bytes 368648 | tf_op jit(solution)/shard_map/ppermute | solution.py:371
  37.5 3.9 %collective-permute-done.3.refs_5_ = bf16[64,2048]{1,0:T(8,128)(2,1)S(1)} collective-permute-done((bf16[64,2048]{1,0:T(8,128)(2,1)S(1)}, bf16[64,2048]{1,0:T(8,128)(2,1)S(1)}, u32[]{:S(2)}, u32[]{:S(2)}) %collective-permute-start.3) | collective-permute-done | bytes 262176 | tf_op jit(solution)/shard_map/ppermute | solution.py:507
  42.2 1.8 %collective-permute-start.4 = (bf16[128,2048]{1,0:T(8,128)(2,1)}, bf16[128,2048]{1,0:T(8,128)(2,1)S(1)}, u32[]{:S(2)}, u32[]{:S(2)}) collective-permute-start(bf16[128,2048]{1,0:T(8,128)(2,1)} %pad_maximum_fusion), channel_id=1, source_target_pairs={{0,8},{8,0},{16,24},{24,16},{1,9},{9,1},{17,25},{25,17},{2,10},{10... | collective-permute-start | bytes 1572872 | tf_op jit(solution)/shard_map/ppermute | solution.py:520
  44.0 1.8 %shard_map.101 = (f32[2,6144]{1,0:T(2,128)S(1)}, bf16[192,256]{1,0:T(8,128)(2,1)S(1)}) custom-call(bf16[32,2,768]{2,1,0:T(2,128)(2,1)S(1)} %all-to-all-done.refs_0_, bf16[192,2048]{1,0:T(8,128)(2,1)} %refs_1_.2, bf16[2048,384]{1,0:T(8,128)(2,1)S(1)} %get-tuple-element.20.refs_2_), custom_call_target="tpu_custom_call" | custom-call | flops 2000000 | tf_op jit(solution)/shard_map/pallas_call | solution.py:59
  45.8 2.3 %shard_map.102 = (bf16[2,128,128]{2,1,0:T(8,128)(2,1)S(1)}, bf16[256,256]{1,0:T(8,128)(2,1)S(1)}) custom-call(f32[2,6144]{1,0:T(2,128)S(1)} %get-tuple-element.21.refs_0_.refs_1_, f32[2,2,128,128]{3,2,1,0:T(8,128)S(1)} %copy-done.2, bf16[2048,384]{1,0:T(8,128)(2,1)S(1)} %get-tuple-element.20.refs_2_, bf16[30,2048]{1,0:T(8,128)(2,1)S(1)} %copy-done, ...), custom_call_target="tpu_custom_call" | custom-call | flops 2000000 | tf_op jit(solution)/shard_map/pallas_call | solution.py:59
  48.2 1.5 %collective-permute-start.16 = (bf16[256,256]{1,0:T(8,128)(2,1)S(1)}, bf16[256,256]{1,0:T(8,128)(2,1)S(1)}, u32[]{:S(2)}, u32[]{:S(2)}) collective-permute-start(bf16[256,256]{1,0:T(8,128)(2,1)S(1)} %get-tuple-element.26.refs_1_), channel_id=1, source_target_pairs={{0,16},{8,24},{16,0},{24,8},{1,17},{9,25},{17,1},{25,9},{2,18},{10... | collective-permute-start | bytes 393224 | tf_op jit(solution)/shard_map/ppermute | solution.py:445
  50.3 4.3 %collective-permute-done.16.refs_5_ = bf16[256,256]{1,0:T(8,128)(2,1)S(1)} collective-permute-done((bf16[256,256]{1,0:T(8,128)(2,1)S(1)}, bf16[256,256]{1,0:T(8,128)(2,1)S(1)}, u32[]{:S(2)}, u32[]{:S(2)}) %collective-permute-start.16) | collective-permute-done | bytes 131104 | tf_op jit(solution)/shard_map/ppermute | solution.py:445
  57.1 1.8 %shard_map.103 = (f32[2,2,128,1]{3,2,1,0:T(8,128)S(1)}, f32[2,2,128,1]{3,2,1,0:T(8,128)S(1)}, f32[2,2,128,128]{3,2,1,0:T(8,128)S(1)}) custom-call(bf16[2,128,128]{2,1,0:T(8,128)(2,1)S(1)} %get-tuple-element.25.refs_0_.refs_4_, bf16[256,256]{1,0:T(8,128)(2,1)S(1)} %get-tuple-element.26.refs_1_, bf16[256,256]{1,0:T(8,128)(2,1)S(1)} %collective-permute-done.12.refs_2_, ...), custom_call_target="tpu_custom_call" | custom-call | flops 2000000 | tf_op jit(solution)/shard_map/pallas_call | solution.py:59
  58.8 1.7 %shard_map.104 = bf16[4,2,32,128]{3,2,1,0:T(8,128)(2,1)S(1)} custom-call(f32[1]{0:T(128)S(6)} %copy.11.refs_0_, f32[2,2,128,1]{3,2,1,0:T(8,128)S(1)} %get-tuple-element.28.refs_1_, f32[2,2,128,1]{3,2,1,0:T(8,128)S(1)} %get-tuple-element.29.refs_2_, f32[2,2,128,128]{3,2,1,0:T(8,128)S(1)} %get-tuple-element.30.refs_3_, ...), custom_call_target="tpu_custom_call" | custom-call | flops 2000000 | tf_op jit(solution)/shard_map/pallas_call | solution.py:59
  61.5 2.5 %collective-permute-start.19 = (bf16[2,32,128]{2,1,0:T(8,128)(2,1)S(1)}, bf16[2,32,128]{2,1,0:T(8,128)(2,1)S(1)}, u32[]{:S(2)}, u32[]{:S(2)}) collective-permute-start(bf16[2,32,128]{2,1,0:T(8,128)(2,1)S(1)} %get-tuple-element.34), channel_id=1, source_target_pairs={{0,4},{1,5},{2,6},{3,7},{4,0},{5,1},{6,2},{7,3},{8,12},{9,13},{10,... | collective-permute-start | bytes 49160 | tf_op jit(solution)/shard_map/ppermute | solution.py:363
  65.0 1.2 %collective-permute-done.19.refs_9_ = bf16[2,32,128]{2,1,0:T(8,128)(2,1)S(1)} collective-permute-done((bf16[2,32,128]{2,1,0:T(8,128)(2,1)S(1)}, bf16[2,32,128]{2,1,0:T(8,128)(2,1)S(1)}, u32[]{:S(2)}, u32[]{:S(2)}) %collective-permute-start.19) | collective-permute-done | bytes 16416 | tf_op jit(solution)/shard_map/ppermute | solution.py:363
  66.2 3.4 %collective-permute-done.20.refs_10_ = bf16[2,32,128]{2,1,0:T(8,128)(2,1)S(1)} collective-permute-done((bf16[2,32,128]{2,1,0:T(8,128)(2,1)S(1)}, bf16[2,32,128]{2,1,0:T(8,128)(2,1)S(1)}, u32[]{:S(2)}, u32[]{:S(2)}) %collective-permute-start.20) | collective-permute-done | bytes 16416 | tf_op jit(solution)/shard_map/ppermute | solution.py:363
  69.6 1.3 %shard_map.105 = (f32[32,2048]{1,0:T(8,128)S(1)}, bf16[32,2048]{1,0:T(8,128)(2,1)S(1)}) custom-call(s32[1]{0:T(128)} %bitcast.refs_0_, bf16[128,2048]{1,0:T(8,128)(2,1)} %refs_1_.3, bf16[64,2048]{1,0:T(8,128)(2,1)S(1)} %collective-permute-done.refs_2_, bf16[64,2048]{1,0:T(8,128)(2,1)S(1)} %collective-permute-done.1.refs_3_, ...), custom_call_target="tpu_custom_call" | custom-call | flops 2000000 | tf_op jit(solution)/shard_map/pallas_call | solution.py:59
  71.6 4.3 %collective-permute-done.21.refs_3_ = bf16[32,2048]{1,0:T(8,128)(2,1)S(1)} collective-permute-done((bf16[32,2048]{1,0:T(8,128)(2,1)S(1)}, bf16[32,2048]{1,0:T(8,128)(2,1)S(1)}, u32[]{:S(2)}, u32[]{:S(2)}) %collective-permute-start.21) | collective-permute-done | bytes 131104 | tf_op jit(solution)/shard_map/ppermute | solution.py:371
  (39 shorter events, 8.1 us)
Async XLA Ops:
  0.0 14.2 %copy-start = (bf16[30,2048]{1,0:T(8,128)(2,1)S(1)}, bf16[30,2048]{1,0:T(8,128)(2,1)}, u32[]{:S(2)}) copy-start(bf16[30,2048]{1,0:T(8,128)(2,1)} %refs_0_.2) | copy-start | bytes 368644
  3.4 10.8 %collective-permute-start = (bf16[64,2048]{1,0:T(8,128)(2,1)S(1)}, bf16[64,2048]{1,0:T(8,128)(2,1)S(1)}, u32[]{:S(2)}, u32[]{:S(2)}) collective-permute-start(bf16[64,2048]{1,0:T(8,128)(2,1)S(1)} %get-tuple-element.22), channel_id=1, source_target_pairs={{0,4},{1,5},{2,6},{3,7},{4,0},{5,1},{6,2},{7,3},{8,10},{9,11},{10,... | collective-permute-start | bytes 786440 | tf_op jit(solution)/shard_map/ppermute | solution.py:507
  7.5 27.9 %collective-permute-start.1 = (bf16[64,2048]{1,0:T(8,128)(2,1)S(1)}, bf16[64,2048]{1,0:T(8,128)(2,1)S(1)}, u32[]{:S(2)}, u32[]{:S(2)}) collective-permute-start(bf16[64,2048]{1,0:T(8,128)(2,1)S(1)} %get-tuple-element.23), channel_id=1, source_target_pairs={{0,4},{1,5},{2,6},{3,7},{4,0},{5,1},{6,2},{7,3},{8,10},{9,11},{10,... | collective-permute-start | bytes 786440 | tf_op jit(solution)/shard_map/ppermute | solution.py:507
  14.2 23.0 %collective-permute-start.2 = (bf16[64,2048]{1,0:T(8,128)(2,1)S(1)}, bf16[64,2048]{1,0:T(8,128)(2,1)S(1)}, u32[]{:S(2)}, u32[]{:S(2)}) collective-permute-start(bf16[64,2048]{1,0:T(8,128)(2,1)S(1)} %collective-permute-done.refs_2_), channel_id=1, source_target_pairs={{0,10},{1,11},{2,8},{3,9},{4,14},{5,15},{6,12},{7,13},{8,0},{9,1},... | collective-permute-start | bytes 786440 | tf_op jit(solution)/shard_map/ppermute | solution.py:507
  14.2 10.5 %collective-permute-start.6 = (bf16[30,2048]{1,0:T(8,128)(2,1)S(1)}, bf16[30,2048]{1,0:T(8,128)(2,1)S(1)}, u32[]{:S(2)}, u32[]{:S(2)}) collective-permute-start(bf16[30,2048]{1,0:T(8,128)(2,1)S(1)} %copy-done), channel_id=1, source_target_pairs={{0,4},{1,5},{2,6},{3,7},{4,0},{5,1},{6,2},{7,3},{8,12},{9,13},{10,... | collective-permute-start | bytes 368648 | tf_op jit(solution)/shard_map/ppermute | solution.py:363
  17.5 15.7 %collective-permute-start.5 = (bf16[30,2048]{1,0:T(8,128)(2,1)S(1)}, bf16[30,2048]{1,0:T(8,128)(2,1)}, u32[]{:S(2)}, u32[]{:S(2)}) collective-permute-start(bf16[30,2048]{1,0:T(8,128)(2,1)S(1)} %copy-done), channel_id=1, source_target_pairs={{0,2},{1,3},{2,0},{3,1},{4,6},{5,7},{6,4},{7,5},{8,10},{9,11},{10,... | collective-permute-start | bytes 368648 | tf_op jit(solution)/shard_map/ppermute | solution.py:363
  24.7 10.4 %collective-permute-start.7 = (bf16[30,2048]{1,0:T(8,128)(2,1)S(1)}, bf16[30,2048]{1,0:T(8,128)(2,1)}, u32[]{:S(2)}, u32[]{:S(2)}) collective-permute-start(bf16[30,2048]{1,0:T(8,128)(2,1)S(1)} %collective-permute-done.6.refs_5_), channel_id=1, source_target_pairs={{0,2},{1,3},{2,0},{3,1},{4,6},{5,7},{6,4},{7,5},{8,10},{9,11},{10,... | collective-permute-start | bytes 368648 | tf_op jit(solution)/shard_map/ppermute | solution.py:363
  28.2 17.6 %collective-permute-start.8 = (bf16[30,2048]{1,0:T(8,128)(2,1)S(1)}, bf16[30,2048]{1,0:T(8,128)(2,1)}, u32[]{:S(2)}, u32[]{:S(2)}) collective-permute-start(bf16[30,2048]{1,0:T(8,128)(2,1)S(1)} %copy-done), channel_id=1, source_target_pairs={{0,1},{1,0},{2,3},{3,2},{4,5},{5,4},{6,7},{7,6},{8,9},{9,8},{10,11... | collective-permute-start | bytes 368648 | tf_op jit(solution)/shard_map/ppermute | solution.py:371
  29.7 14.3 %all-to-all-start = ((bf16[32,2,768]{2,1,0:T(2,128)(2,1)}), bf16[32,2,768]{2,1,0:T(2,128)(2,1)S(1)}, u32[]{:S(2)}, u32[]{:S(2)}) async-start(bf16[32,2,768]{2,1,0:T(2,128)(2,1)} %get-tuple-element.19), calls=%async_computation | async-start | bytes 196608 | tf_op jit(solution)/shard_map/all_to_all | solution.py:403
  33.2 12.6 %collective-permute-start.10 = (bf16[30,2048]{1,0:T(8,128)(2,1)S(1)}, bf16[30,2048]{1,0:T(8,128)(2,1)}, u32[]{:S(2)}, u32[]{:S(2)}) collective-permute-start(bf16[30,2048]{1,0:T(8,128)(2,1)S(1)} %collective-permute-done.6.refs_5_), channel_id=1, source_target_pairs={{0,1},{1,0},{2,3},{3,2},{4,5},{5,4},{6,7},{7,6},{8,9},{9,8},{10,11... | collective-permute-start | bytes 368648 | tf_op jit(solution)/shard_map/ppermute | solution.py:371
  35.1 10.7 %collective-permute-start.9 = (bf16[30,2048]{1,0:T(8,128)(2,1)}, bf16[30,2048]{1,0:T(8,128)(2,1)}, u32[]{:S(2)}, u32[]{:S(2)}) collective-permute-start(bf16[30,2048]{1,0:T(8,128)(2,1)} %collective-permute-done.5.refs_4_), channel_id=1, source_target_pairs={{0,1},{1,0},{2,3},{3,2},{4,5},{5,4},{6,7},{7,6},{8,9},{9,8},{10,11... | collective-permute-start | bytes 368648 | tf_op jit(solution)/shard_map/ppermute | solution.py:371
  35.3 10.5 %collective-permute-start.11 = (bf16[30,2048]{1,0:T(8,128)(2,1)}, bf16[30,2048]{1,0:T(8,128)(2,1)}, u32[]{:S(2)}, u32[]{:S(2)}) collective-permute-start(bf16[30,2048]{1,0:T(8,128)(2,1)} %collective-permute-done.7.refs_6_), channel_id=1, source_target_pairs={{0,1},{1,0},{2,3},{3,2},{4,5},{5,4},{6,7},{7,6},{8,9},{9,8},{10,11... | collective-permute-start | bytes 368648 | tf_op jit(solution)/shard_map/ppermute | solution.py:371
  37.1 4.2 %collective-permute-start.3 = (bf16[64,2048]{1,0:T(8,128)(2,1)S(1)}, bf16[64,2048]{1,0:T(8,128)(2,1)S(1)}, u32[]{:S(2)}, u32[]{:S(2)}) collective-permute-start(bf16[64,2048]{1,0:T(8,128)(2,1)S(1)} %collective-permute-done.1.refs_3_), channel_id=1, source_target_pairs={{0,10},{1,11},{2,8},{3,9},{4,14},{5,15},{6,12},{7,13},{8,0},{9,1},... | collective-permute-start | bytes 786440 | tf_op jit(solution)/shard_map/ppermute | solution.py:507
  42.2 27.4 %collective-permute-start.4 = (bf16[128,2048]{1,0:T(8,128)(2,1)}, bf16[128,2048]{1,0:T(8,128)(2,1)S(1)}, u32[]{:S(2)}, u32[]{:S(2)}) collective-permute-start(bf16[128,2048]{1,0:T(8,128)(2,1)} %pad_maximum_fusion), channel_id=1, source_target_pairs={{0,8},{8,0},{16,24},{24,16},{1,9},{9,1},{17,25},{25,17},{2,10},{10... | collective-permute-start | bytes 1572872 | tf_op jit(solution)/shard_map/ppermute | solution.py:520
  48.2 6.4 %collective-permute-start.16 = (bf16[256,256]{1,0:T(8,128)(2,1)S(1)}, bf16[256,256]{1,0:T(8,128)(2,1)S(1)}, u32[]{:S(2)}, u32[]{:S(2)}) collective-permute-start(bf16[256,256]{1,0:T(8,128)(2,1)S(1)} %get-tuple-element.26.refs_1_), channel_id=1, source_target_pairs={{0,16},{8,24},{16,0},{24,8},{1,17},{9,25},{17,1},{25,9},{2,18},{10... | collective-permute-start | bytes 393224 | tf_op jit(solution)/shard_map/ppermute | solution.py:445
  49.7 6.1 %collective-permute-start.13 = (bf16[192,256]{1,0:T(8,128)(2,1)S(1)}, bf16[192,256]{1,0:T(8,128)(2,1)S(1)}, u32[]{:S(2)}, u32[]{:S(2)}) collective-permute-start(bf16[192,256]{1,0:T(8,128)(2,1)S(1)} %get-tuple-element.27.refs_3_), channel_id=1, source_target_pairs={{0,16},{8,24},{16,0},{24,8},{1,17},{9,25},{17,1},{25,9},{2,18},{10... | collective-permute-start | bytes 294920 | tf_op jit(solution)/shard_map/ppermute | solution.py:445
  50.3 6.8 %collective-permute-start.12 = (bf16[256,256]{1,0:T(8,128)(2,1)S(1)}, bf16[256,256]{1,0:T(8,128)(2,1)S(1)}, u32[]{:S(2)}, u32[]{:S(2)}) collective-permute-start(bf16[256,256]{1,0:T(8,128)(2,1)S(1)} %get-tuple-element.26.refs_1_), channel_id=1, source_target_pairs={{0,8},{8,0},{16,24},{24,16},{1,9},{9,1},{17,25},{25,17},{2,10},{10... | collective-permute-start | bytes 393224 | tf_op jit(solution)/shard_map/ppermute | solution.py:455
  54.6 4.2 %collective-permute-start.17 = (bf16[256,256]{1,0:T(8,128)(2,1)S(1)}, bf16[256,256]{1,0:T(8,128)(2,1)S(1)}, u32[]{:S(2)}, u32[]{:S(2)}) collective-permute-start(bf16[256,256]{1,0:T(8,128)(2,1)S(1)} %collective-permute-done.16.refs_5_), channel_id=1, source_target_pairs={{0,8},{8,0},{16,24},{24,16},{1,9},{9,1},{17,25},{25,17},{2,10},{10... | collective-permute-start | bytes 393224 | tf_op jit(solution)/shard_map/ppermute | solution.py:455
  54.6 1.8 %collective-permute-start.14 = (bf16[192,256]{1,0:T(8,128)(2,1)S(1)}, bf16[192,256]{1,0:T(8,128)(2,1)S(1)}, u32[]{:S(2)}, u32[]{:S(2)}) collective-permute-start(bf16[192,256]{1,0:T(8,128)(2,1)S(1)} %get-tuple-element.27.refs_3_), channel_id=1, source_target_pairs={{0,8},{8,0},{16,24},{24,16},{1,9},{9,1},{17,25},{25,17},{2,10},{10... | collective-permute-start | bytes 294920 | tf_op jit(solution)/shard_map/ppermute | solution.py:455
  55.8 1.3 %collective-permute-start.15 = (bf16[192,256]{1,0:T(8,128)(2,1)S(1)}, bf16[192,256]{1,0:T(8,128)(2,1)S(1)}, u32[]{:S(2)}, u32[]{:S(2)}) collective-permute-start(bf16[192,256]{1,0:T(8,128)(2,1)S(1)} %collective-permute-done.13.refs_4_), channel_id=1, source_target_pairs={{0,8},{8,0},{16,24},{24,16},{1,9},{9,1},{17,25},{25,17},{2,10},{10... | collective-permute-start | bytes 294920 | tf_op jit(solution)/shard_map/ppermute | solution.py:455
  60.6 4.5 %collective-permute-start.18 = (bf16[2,32,128]{2,1,0:T(8,128)(2,1)S(1)}, bf16[2,32,128]{2,1,0:T(8,128)(2,1)S(1)}, u32[]{:S(2)}, u32[]{:S(2)}) collective-permute-start(bf16[2,32,128]{2,1,0:T(8,128)(2,1)S(1)} %get-tuple-element.35), channel_id=1, source_target_pairs={{0,2},{1,3},{2,0},{3,1},{4,6},{5,7},{6,4},{7,5},{8,10},{9,11},{10,... | collective-permute-start | bytes 49160 | tf_op jit(solution)/shard_map/ppermute | solution.py:363
  61.5 4.6 %collective-permute-start.19 = (bf16[2,32,128]{2,1,0:T(8,128)(2,1)S(1)}, bf16[2,32,128]{2,1,0:T(8,128)(2,1)S(1)}, u32[]{:S(2)}, u32[]{:S(2)}) collective-permute-start(bf16[2,32,128]{2,1,0:T(8,128)(2,1)S(1)} %get-tuple-element.34), channel_id=1, source_target_pairs={{0,4},{1,5},{2,6},{3,7},{4,0},{5,1},{6,2},{7,3},{8,12},{9,13},{10,... | collective-permute-start | bytes 49160 | tf_op jit(solution)/shard_map/ppermute | solution.py:363
  64.0 5.5 %collective-permute-start.20 = (bf16[2,32,128]{2,1,0:T(8,128)(2,1)S(1)}, bf16[2,32,128]{2,1,0:T(8,128)(2,1)S(1)}, u32[]{:S(2)}, u32[]{:S(2)}) collective-permute-start(bf16[2,32,128]{2,1,0:T(8,128)(2,1)S(1)} %get-tuple-element.33), channel_id=1, source_target_pairs={{0,6},{1,7},{2,4},{3,5},{4,2},{5,3},{6,0},{7,1},{8,14},{9,15},{10,... | collective-permute-start | bytes 49160 | tf_op jit(solution)/shard_map/ppermute | solution.py:363
  70.9 5.0 %collective-permute-start.21 = (bf16[32,2048]{1,0:T(8,128)(2,1)S(1)}, bf16[32,2048]{1,0:T(8,128)(2,1)S(1)}, u32[]{:S(2)}, u32[]{:S(2)}) collective-permute-start(bf16[32,2048]{1,0:T(8,128)(2,1)S(1)} %get-tuple-element.32), channel_id=1, source_target_pairs={{0,1},{1,0},{2,3},{3,2},{4,5},{5,4},{6,7},{7,6},{8,9},{9,8},{10,11... | collective-permute-start | bytes 393224 | tf_op jit(solution)/shard_map/ppermute | solution.py:371
  (2 other events, 2.5 us)

commit v5 on v4

--- a/solution.py
+++ b/solution.py
@@ -85,10 +85,8 @@
 
 def prepare_body(number, pad, ranks, outer, inner, *refs):
     here_ref, latent_hbm, context_hbm, weight_hbm = refs[:4]
-    sources, exit_hbm = refs[4:7], refs[7]
-    out_ref, table_ref, joined_ref, upper_ref, lower_ref = refs[8:13]
-    cond_ref, weight_ref, sems, more_sems = refs[13:]
-    half = upper_ref.shape[0]
+    sources = refs[4:7]
+    out_ref, table_ref, joined_ref, cond_ref, weight_ref, sems, more_sems = refs[7:]
     moves = [
         pltpu.make_async_copy(weight_hbm, weight_ref, sems.at[0]),
         pltpu.make_async_copy(latent_hbm, cond_ref.at[0:1], sems.at[1]),
@@ -97,12 +95,6 @@
     for move in moves:
         move.start()
     more = fetch_weights(sources, joined_ref, more_sems)
-    more += [
-        pltpu.make_async_copy(exit_hbm.at[:half], upper_ref, sems.at[3]),
-        pltpu.make_async_copy(exit_hbm.at[half:], lower_ref, sems.at[4]),
-    ]
-    more[-2].start()
-    more[-1].start()
     make_tables(number, pad, ranks, outer, inner, here_ref[0], table_ref)
     moves[1].wait()
     moves[2].wait()
@@ -372,16 +364,12 @@
 
     columns = mod_weight.shape[1]
     here = (here_sp * ranks + here_tp).astype(jnp.int32).reshape(1)
-    depth = w_out.shape[0]
-    half = sds((depth // 2, width), BF16)
-    copies, table, weight, *halves = call(
+    copies, table, weight = call(
         functools.partial(prepare_body, number, pad, ranks, outer, inner),
         (
             sds((groups * ranks, 2, columns), BF16),
             sds((inner, 2, tile, wide), F32),
             sds((width, wide + wide + VAL_DIM), BF16),
-            half,
-            half,
         ),
         here,
         cond_latent.reshape(1, -1),
@@ -390,14 +378,13 @@
         w_query,
         w_key,
         w_value,
-        w_out,
         scratch=[
             pltpu.VMEM((2, cond_latent.shape[0]), F32),
             pltpu.VMEM(mod_weight.shape, BF16),
-            pltpu.SemaphoreType.DMA((5,)),
+            pltpu.SemaphoreType.DMA((3,)),
             pltpu.SemaphoreType.DMA((3,)),
         ],
-        in_specs=[SMEM] + [HBM] * 7,
+        in_specs=[SMEM] + [HBM] * 6,
         local=True,
     )
     pieces = lax.all_to_all(copies, ("sp", "tp"), 0, 0)
@@ -508,22 +495,16 @@
 
     slots, weights = [], []
     if share > 1 and outer == 4:
-        fetched, turned = [], []
-        for i, part in enumerate(halves):
-            fetched.append(
-                joint(part, lambda s, o: (s, behind(o, 1 if s % 2 else 2, outer)))
-            )
-            turned.append(
-                joint(fetched[i], lambda s, o: (s ^ 1, o if s % 2 else behind(o, 1, outer)))
-            )
-        given = [jnp.where(here_sp % 2 == 0, a, b) for a, b in zip(fetched, turned)]
-        traded = lax.ppermute(jnp.concatenate(given, axis=0), "sp", swap)
-        slots = [(2, 1), (2, 1), (1, 3), (1, 3), (3, 2)]
-        weights = [*fetched, *turned, traded]
+        fetched = joint(w_out, lambda s, o: (s, behind(o, 1 if s % 2 else 2, outer)))
+        turned = joint(fetched, lambda s, o: (s ^ 1, o if s % 2 else behind(o, 1, outer)))
+        given = jnp.where(here_sp % 2 == 0, fetched, turned)
+        traded = lax.ppermute(given, "sp", swap)
+        slots, weights = [(2, 1), (1, 3), (3, 2)], [fetched, turned, traded]
     else:
         for k in range(1, outer):
             weights.append(along_outer(w_out, k, behind))
             slots.append((k, k))
+    depth = w_out.shape[0]
     total = call(
         functools.partial(partial_out_body, slots, share, ranks, outer, inner, pad),
         (sds((pad, width), F32),) + (sds((pad, width), BF16),) * (inner - 1),

time: 77 us -> 85.4 us (1.11)
  waiting for transfers between devices: 30.6 us -> 38.7 us
    ppermute x6, starting transfers between devices: 12.9 us -> 16.7 us  [along_outer(): return lax.ppermute(value, 'tp', pairs)]
    ppermute x5, waiting for transfers between devices: 4.31 us -> 7.3 us  [along_inner(): return lax.ppermute(value, 'tp', pairs)]
    all_to_all x1, waiting for transfers between devices: 0.01 us -> 2.95 us  [shards(): pieces = lax.all_to_all(copies, ('sp', 'tp'), 0, 0)]
    ppermute x1, starting transfers between devices: 1.8 us -> 0.01 us  [shards(): traded = lax.ppermute(given, 'sp', swap)]
    ppermute x6, waiting for transfers between devices: 10.1 us -> 11.7 us  [along_outer(): return lax.ppermute(value, 'tp', pairs)]
    ppermute x4 -> x2, waiting for transfers between devices: 10.5 us -> 11.7 us  [joint(): return lax.ppermute(value, ('sp', 'tp'), moves)]
    all_to_all x1, starting transfers between devices: 3.53 us -> 2.57 us  [shards(): pieces = lax.all_to_all(copies, ('sp', 'tp'), 0, 0)]
    ppermute x4 -> x2, starting transfers between devices: 4.44 us -> 4.07 us  [joint(): return lax.ppermute(value, ('sp', 'tp'), moves)]
  transfers between devices with their start and end apart: 23 -> 21, of which waited for: 9 -> 11; matrix products, arithmetic and copies ran while one was open for 1% -> 1% of each run, Pallas kernels for 10% -> 12%
where the time goes in v5:
time: 85.4 us; the launch traced here: 85.1 us
  waiting for transfers between devices  38.7 us (45%)
  starting transfers between devices  31.8 us (37%)
  Pallas kernels  12.1 us (14%)
  other arithmetic  0.88 us (1%)
    ppermute x6, starting transfers between devices, along_outer(): return lax.ppermute(value, 'tp', pairs)  16.7 us
    pallas_call x7, Pallas kernels, call(): pl.pallas_call(body, out_shape=outs, in_specs=in_specs, out_specs=jax.tre...  12.1 us
    ppermute x2, waiting for transfers between devices, joint(): return lax.ppermute(value, ('sp', 'tp'), moves)  11.7 us
    ppermute x6, waiting for transfers between devices, along_outer(): return lax.ppermute(value, 'tp', pairs)  11.7 us
    ppermute x5, waiting for transfers between devices, along_inner(): return lax.ppermute(value, 'tp', pairs)  7.3 us
    ppermute x5, starting transfers between devices, along_inner(): return lax.ppermute(value, 'tp', pairs)  5.87 us
    ppermute x2, waiting for transfers between devices, along_lines(): return lax.ppermute(value, 'sp', pairs)  4.42 us
    ppermute x2, starting transfers between devices, joint(): return lax.ppermute(value, ('sp', 'tp'), moves)  4.07 us
  transfers between devices with their start and end apart: 21, of which 11 were waited for; matrix products, arithmetic and copies ran while one was open for 1% of the time, Pallas kernels for 12%

profile of v5, /device:TPU:0, one launch (start us, length us, event | category | flops | bytes accessed | tf_op | source)
XLA Modules:
  0.0 85.1 jit_solution(18325728818665545757)
XLA Ops:
  0.0 4.1 %collective-permute-start = (bf16[128,2048]{1,0:T(8,128)(2,1)}, bf16[128,2048]{1,0:T(8,128)(2,1)S(1)}, u32[]{:S(2)}, u32[]{:S(2)}) collective-permute-start(bf16[128,2048]{1,0:T(8,128)(2,1)} %refs_1_.3), channel_id=1, source_target_pairs={{0,4},{1,5},{2,6},{3,7},{4,0},{5,1},{6,2},{7,3},{8,10},{9,11},{10,... | collective-permute-start | bytes 1572872 | tf_op jit(solution)/shard_map/ppermute | solution.py:494
  4.1 11.7 %collective-permute-done.refs_2_ = bf16[128,2048]{1,0:T(8,128)(2,1)S(1)} collective-permute-done((bf16[128,2048]{1,0:T(8,128)(2,1)}, bf16[128,2048]{1,0:T(8,128)(2,1)S(1)}, u32[]{:S(2)}, u32[]{:S(2)}) %collective-permute-start) | collective-permute-done | bytes 524320 | tf_op jit(solution)/shard_map/ppermute | solution.py:494
  15.8 2.1 %collective-permute-start.4 = (bf16[30,2048]{1,0:T(8,128)(2,1)}, bf16[30,2048]{1,0:T(8,128)(2,1)S(1)}, u32[]{:S(2)}, u32[]{:S(2)}) collective-permute-start(bf16[30,2048]{1,0:T(8,128)(2,1)} %refs_0_.2), channel_id=1, source_target_pairs={{0,4},{1,5},{2,6},{3,7},{4,0},{5,1},{6,2},{7,3},{8,12},{9,13},{10,... | collective-permute-start | bytes 368648 | tf_op jit(solution)/shard_map/ppermute | solution.py:355
  17.9 3.6 %collective-permute-start.3 = (bf16[30,2048]{1,0:T(8,128)(2,1)}, bf16[30,2048]{1,0:T(8,128)(2,1)}, u32[]{:S(2)}, u32[]{:S(2)}) collective-permute-start(bf16[30,2048]{1,0:T(8,128)(2,1)} %refs_0_.2), channel_id=1, source_target_pairs={{0,2},{1,3},{2,0},{3,1},{4,6},{5,7},{6,4},{7,5},{8,10},{9,11},{10,... | collective-permute-start | bytes 368648 | tf_op jit(solution)/shard_map/ppermute | solution.py:355
  21.5 6.2 %collective-permute-done.4.refs_5_ = bf16[30,2048]{1,0:T(8,128)(2,1)S(1)} collective-permute-done((bf16[30,2048]{1,0:T(8,128)(2,1)}, bf16[30,2048]{1,0:T(8,128)(2,1)S(1)}, u32[]{:S(2)}, u32[]{:S(2)}) %collective-permute-start.4) | collective-permute-done | bytes 122912 | tf_op jit(solution)/shard_map/ppermute | solution.py:355
  27.7 6.6 %collective-permute-start.5 = (bf16[30,2048]{1,0:T(8,128)(2,1)S(1)}, bf16[30,2048]{1,0:T(8,128)(2,1)}, u32[]{:S(2)}, u32[]{:S(2)}) collective-permute-start(bf16[30,2048]{1,0:T(8,128)(2,1)S(1)} %collective-permute-done.4.refs_5_), channel_id=1, source_target_pairs={{0,2},{1,3},{2,0},{3,1},{4,6},{5,7},{6,4},{7,5},{8,10},{9,11},{10,... | collective-permute-start | bytes 368648 | tf_op jit(solution)/shard_map/ppermute | solution.py:355
  34.3 1.5 %collective-permute-start.6 = (bf16[30,2048]{1,0:T(8,128)(2,1)}, bf16[30,2048]{1,0:T(8,128)(2,1)}, u32[]{:S(2)}, u32[]{:S(2)}) collective-permute-start(bf16[30,2048]{1,0:T(8,128)(2,1)} %refs_0_.2), channel_id=1, source_target_pairs={{0,1},{1,0},{2,3},{3,2},{4,5},{5,4},{6,7},{7,6},{8,9},{9,8},{10,11... | collective-permute-start | bytes 368648 | tf_op jit(solution)/shard_map/ppermute | solution.py:363
  35.8 2.5 %shard_map.100 = (bf16[32,2,768]{2,1,0:T(2,128)(2,1)}, f32[2,2,128,128]{3,2,1,0:T(8,128)S(1)}, bf16[2048,384]{1,0:T(8,128)(2,1)S(1)}) custom-call(s32[1]{0:T(128)} %bitcast.refs_0_, f32[1,512]{1,0:T(1,128)} %bitcast.11, f32[1,512]{1,0:T(1,128)} %bitcast.12, bf16[512,768]{1,0:T(8,128)(2,1)} %refs_3_.2, bf16[2048,128]{1,0:T(8,128)(2,1)} %refs_4_.1, ...), custom_call_target="tpu_custom_call" | custom-call | flops 2000000 | tf_op jit(solution)/shard_map/pallas_call | solution.py:59
  39.0 2.6 %all-to-all-start = ((bf16[32,2,768]{2,1,0:T(2,128)(2,1)}), bf16[32,2,768]{2,1,0:T(2,128)(2,1)S(1)}, u32[]{:S(2)}, u32[]{:S(2)}) async-start(bf16[32,2,768]{2,1,0:T(2,128)(2,1)} %get-tuple-element.17), calls=%async_computation | async-start | bytes 196608 | tf_op jit(solution)/shard_map/all_to_all | solution.py:390
  41.6 1.7 %collective-permute-start.8 = (bf16[30,2048]{1,0:T(8,128)(2,1)S(1)}, bf16[30,2048]{1,0:T(8,128)(2,1)}, u32[]{:S(2)}, u32[]{:S(2)}) collective-permute-start(bf16[30,2048]{1,0:T(8,128)(2,1)S(1)} %collective-permute-done.4.refs_5_), channel_id=1, source_target_pairs={{0,1},{1,0},{2,3},{3,2},{4,5},{5,4},{6,7},{7,6},{8,9},{9,8},{10,11... | collective-permute-start | bytes 368648 | tf_op jit(solution)/shard_map/ppermute | solution.py:363
  43.7 1.6 %collective-permute-start.9 = (bf16[30,2048]{1,0:T(8,128)(2,1)}, bf16[30,2048]{1,0:T(8,128)(2,1)}, u32[]{:S(2)}, u32[]{:S(2)}) collective-permute-start(bf16[30,2048]{1,0:T(8,128)(2,1)} %collective-permute-done.5.refs_6_), channel_id=1, source_target_pairs={{0,1},{1,0},{2,3},{3,2},{4,5},{5,4},{6,7},{7,6},{8,9},{9,8},{10,11... | collective-permute-start | bytes 368648 | tf_op jit(solution)/shard_map/ppermute | solution.py:363
  46.2 3.0 %all-to-all-done.refs_0_ = bf16[32,2,768]{2,1,0:T(2,128)(2,1)S(1)} async-done(((bf16[32,2,768]{2,1,0:T(2,128)(2,1)}), bf16[32,2,768]{2,1,0:T(2,128)(2,1)S(1)}, u32[]{:S(2)}, u32[]{:S(2)}) %all-to-all-start) | async-done | bytes 98336 | tf_op jit(solution)/shard_map/all_to_all | solution.py:390
  49.2 1.8 %shard_map.101 = (f32[2,6144]{1,0:T(2,128)S(1)}, bf16[192,256]{1,0:T(8,128)(2,1)S(1)}) custom-call(bf16[32,2,768]{2,1,0:T(2,128)(2,1)S(1)} %all-to-all-done.refs_0_, bf16[192,2048]{1,0:T(8,128)(2,1)} %refs_1_.2, bf16[2048,384]{1,0:T(8,128)(2,1)S(1)} %get-tuple-element.18.refs_2_), custom_call_target="tpu_custom_call" | custom-call | flops 2000000 | tf_op jit(solution)/shard_map/pallas_call | solution.py:59
  51.7 2.1 %collective-permute-done.9.refs_10_ = bf16[30,2048]{1,0:T(8,128)(2,1)} collective-permute-done((bf16[30,2048]{1,0:T(8,128)(2,1)}, bf16[30,2048]{1,0:T(8,128)(2,1)}, u32[]{:S(2)}, u32[]{:S(2)}) %collective-permute-start.9) | collective-permute-done | bytes 122912 | tf_op jit(solution)/shard_map/ppermute | solution.py:363
  53.9 2.3 %shard_map.102 = (bf16[2,128,128]{2,1,0:T(8,128)(2,1)S(1)}, bf16[256,256]{1,0:T(8,128)(2,1)S(1)}) custom-call(f32[2,6144]{1,0:T(2,128)S(1)} %get-tuple-element.19.refs_0_.refs_1_, f32[2,2,128,128]{3,2,1,0:T(8,128)S(1)} %copy-done.2, bf16[2048,384]{1,0:T(8,128)(2,1)S(1)} %get-tuple-element.18.refs_2_, bf16[30,2048]{1,0:T(8,128)(2,1)S(1)} %copy-done, ...), custom_call_target="tpu_custom_call" | custom-call | flops 2000000 | tf_op jit(solution)/shard_map/pallas_call | solution.py:59
  56.2 1.7 %collective-permute-start.14 = (bf16[256,256]{1,0:T(8,128)(2,1)S(1)}, bf16[256,256]{1,0:T(8,128)(2,1)S(1)}, u32[]{:S(2)}, u32[]{:S(2)}) collective-permute-start(bf16[256,256]{1,0:T(8,128)(2,1)S(1)} %get-tuple-element.22.refs_1_), channel_id=1, source_target_pairs={{0,16},{8,24},{16,0},{24,8},{1,17},{9,25},{17,1},{25,9},{2,18},{10... | collective-permute-start | bytes 393224 | tf_op jit(solution)/shard_map/ppermute | solution.py:432
  58.3 3.9 %collective-permute-done.14.refs_5_ = bf16[256,256]{1,0:T(8,128)(2,1)S(1)} collective-permute-done((bf16[256,256]{1,0:T(8,128)(2,1)S(1)}, bf16[256,256]{1,0:T(8,128)(2,1)S(1)}, u32[]{:S(2)}, u32[]{:S(2)}) %collective-permute-start.14) | collective-permute-done | bytes 131104 | tf_op jit(solution)/shard_map/ppermute | solution.py:432
  64.5 1.8 %shard_map.103 = (f32[2,2,128,1]{3,2,1,0:T(8,128)S(1)}, f32[2,2,128,1]{3,2,1,0:T(8,128)S(1)}, f32[2,2,128,128]{3,2,1,0:T(8,128)S(1)}) custom-call(bf16[2,128,128]{2,1,0:T(8,128)(2,1)S(1)} %get-tuple-element.21.refs_0_.refs_4_, bf16[256,256]{1,0:T(8,128)(2,1)S(1)} %get-tuple-element.22.refs_1_, bf16[256,256]{1,0:T(8,128)(2,1)S(1)} %collective-permute-done.10.refs_2_, ...), custom_call_target="tpu_custom_call" | custom-call | flops 2000000 | tf_op jit(solution)/shard_map/pallas_call | solution.py:59
  66.3 1.7 %shard_map.104 = bf16[4,2,32,128]{3,2,1,0:T(8,128)(2,1)S(1)} custom-call(f32[1]{0:T(128)S(6)} %copy.11.refs_0_, f32[2,2,128,1]{3,2,1,0:T(8,128)S(1)} %get-tuple-element.24.refs_1_, f32[2,2,128,1]{3,2,1,0:T(8,128)S(1)} %get-tuple-element.25.refs_2_, f32[2,2,128,128]{3,2,1,0:T(8,128)S(1)} %get-tuple-element.26.refs_3_, ...), custom_call_target="tpu_custom_call" | custom-call | flops 2000000 | tf_op jit(solution)/shard_map/pallas_call | solution.py:59
  68.0 1.8 %collective-permute-start.16 = (bf16[2,32,128]{2,1,0:T(8,128)(2,1)S(1)}, bf16[2,32,128]{2,1,0:T(8,128)(2,1)S(1)}, u32[]{:S(2)}, u32[]{:S(2)}) collective-permute-start(bf16[2,32,128]{2,1,0:T(8,128)(2,1)S(1)} %get-tuple-element.31), channel_id=1, source_target_pairs={{0,2},{1,3},{2,0},{3,1},{4,6},{5,7},{6,4},{7,5},{8,10},{9,11},{10,... | collective-permute-start | bytes 49160 | tf_op jit(solution)/shard_map/ppermute | solution.py:355
  69.8 2.6 %collective-permute-start.17 = (bf16[2,32,128]{2,1,0:T(8,128)(2,1)S(1)}, bf16[2,32,128]{2,1,0:T(8,128)(2,1)S(1)}, u32[]{:S(2)}, u32[]{:S(2)}) collective-permute-start(bf16[2,32,128]{2,1,0:T(8,128)(2,1)S(1)} %get-tuple-element.30), channel_id=1, source_target_pairs={{0,4},{1,5},{2,6},{3,7},{4,0},{5,1},{6,2},{7,3},{8,12},{9,13},{10,... | collective-permute-start | bytes 49160 | tf_op jit(solution)/shard_map/ppermute | solution.py:355
  72.5 2.0 %collective-permute-done.17.refs_7_ = bf16[2,32,128]{2,1,0:T(8,128)(2,1)S(1)} collective-permute-done((bf16[2,32,128]{2,1,0:T(8,128)(2,1)S(1)}, bf16[2,32,128]{2,1,0:T(8,128)(2,1)S(1)}, u32[]{:S(2)}, u32[]{:S(2)}) %collective-permute-start.17) | collective-permute-done | bytes 16416 | tf_op jit(solution)/shard_map/ppermute | solution.py:355
  74.5 3.5 %collective-permute-done.18.refs_8_ = bf16[2,32,128]{2,1,0:T(8,128)(2,1)S(1)} collective-permute-done((bf16[2,32,128]{2,1,0:T(8,128)(2,1)S(1)}, bf16[2,32,128]{2,1,0:T(8,128)(2,1)S(1)}, u32[]{:S(2)}, u32[]{:S(2)}) %collective-permute-start.18) | collective-permute-done | bytes 16416 | tf_op jit(solution)/shard_map/ppermute | solution.py:355
  79.9 4.4 %collective-permute-done.19.refs_3_ = bf16[32,2048]{1,0:T(8,128)(2,1)S(1)} collective-permute-done((bf16[32,2048]{1,0:T(8,128)(2,1)S(1)}, bf16[32,2048]{1,0:T(8,128)(2,1)S(1)}, u32[]{:S(2)}, u32[]{:S(2)}) %collective-permute-start.19) | collective-permute-done | bytes 131104 | tf_op jit(solution)/shard_map/ppermute | solution.py:363
  (33 shorter events, 7.7 us)
Async XLA Ops:
  0.0 15.8 %collective-permute-start = (bf16[128,2048]{1,0:T(8,128)(2,1)}, bf16[128,2048]{1,0:T(8,128)(2,1)S(1)}, u32[]{:S(2)}, u32[]{:S(2)}) collective-permute-start(bf16[128,2048]{1,0:T(8,128)(2,1)} %refs_1_.3), channel_id=1, source_target_pairs={{0,4},{1,5},{2,6},{3,7},{4,0},{5,1},{6,2},{7,3},{8,10},{9,11},{10,... | collective-permute-start | bytes 1572872 | tf_op jit(solution)/shard_map/ppermute | solution.py:494
  15.8 29.5 %collective-permute-start.1 = (bf16[128,2048]{1,0:T(8,128)(2,1)S(1)}, bf16[128,2048]{1,0:T(8,128)(2,1)S(1)}, u32[]{:S(2)}, u32[]{:S(2)}) collective-permute-start(bf16[128,2048]{1,0:T(8,128)(2,1)S(1)} %collective-permute-done.refs_2_), channel_id=1, source_target_pairs={{0,10},{1,11},{2,8},{3,9},{4,14},{5,15},{6,12},{7,13},{8,0},{9,1},... | collective-permute-start | bytes 1572872 | tf_op jit(solution)/shard_map/ppermute | solution.py:494
  15.8 11.9 %collective-permute-start.4 = (bf16[30,2048]{1,0:T(8,128)(2,1)}, bf16[30,2048]{1,0:T(8,128)(2,1)S(1)}, u32[]{:S(2)}, u32[]{:S(2)}) collective-permute-start(bf16[30,2048]{1,0:T(8,128)(2,1)} %refs_0_.2), channel_id=1, source_target_pairs={{0,4},{1,5},{2,6},{3,7},{4,0},{5,1},{6,2},{7,3},{8,12},{9,13},{10,... | collective-permute-start | bytes 368648 | tf_op jit(solution)/shard_map/ppermute | solution.py:355
  17.9 25.4 %collective-permute-start.3 = (bf16[30,2048]{1,0:T(8,128)(2,1)}, bf16[30,2048]{1,0:T(8,128)(2,1)}, u32[]{:S(2)}, u32[]{:S(2)}) collective-permute-start(bf16[30,2048]{1,0:T(8,128)(2,1)} %refs_0_.2), channel_id=1, source_target_pairs={{0,2},{1,3},{2,0},{3,1},{4,6},{5,7},{6,4},{7,5},{8,10},{9,11},{10,... | collective-permute-start | bytes 368648 | tf_op jit(solution)/shard_map/ppermute | solution.py:355
  27.7 16.0 %collective-permute-start.5 = (bf16[30,2048]{1,0:T(8,128)(2,1)S(1)}, bf16[30,2048]{1,0:T(8,128)(2,1)}, u32[]{:S(2)}, u32[]{:S(2)}) collective-permute-start(bf16[30,2048]{1,0:T(8,128)(2,1)S(1)} %collective-permute-done.4.refs_5_), channel_id=1, source_target_pairs={{0,2},{1,3},{2,0},{3,1},{4,6},{5,7},{6,4},{7,5},{8,10},{9,11},{10,... | collective-permute-start | bytes 368648 | tf_op jit(solution)/shard_map/ppermute | solution.py:355
  34.3 16.7 %collective-permute-start.6 = (bf16[30,2048]{1,0:T(8,128)(2,1)}, bf16[30,2048]{1,0:T(8,128)(2,1)}, u32[]{:S(2)}, u32[]{:S(2)}) collective-permute-start(bf16[30,2048]{1,0:T(8,128)(2,1)} %refs_0_.2), channel_id=1, source_target_pairs={{0,1},{1,0},{2,3},{3,2},{4,5},{5,4},{6,7},{7,6},{8,9},{9,8},{10,11... | collective-permute-start | bytes 368648 | tf_op jit(solution)/shard_map/ppermute | solution.py:363
  38.3 0.7 copy-start.1
  39.0 10.2 %all-to-all-start = ((bf16[32,2,768]{2,1,0:T(2,128)(2,1)}), bf16[32,2,768]{2,1,0:T(2,128)(2,1)S(1)}, u32[]{:S(2)}, u32[]{:S(2)}) async-start(bf16[32,2,768]{2,1,0:T(2,128)(2,1)} %get-tuple-element.17), calls=%async_computation | async-start | bytes 196608 | tf_op jit(solution)/shard_map/all_to_all | solution.py:390
  41.6 9.4 %collective-permute-start.8 = (bf16[30,2048]{1,0:T(8,128)(2,1)S(1)}, bf16[30,2048]{1,0:T(8,128)(2,1)}, u32[]{:S(2)}, u32[]{:S(2)}) collective-permute-start(bf16[30,2048]{1,0:T(8,128)(2,1)S(1)} %collective-permute-done.4.refs_5_), channel_id=1, source_target_pairs={{0,1},{1,0},{2,3},{3,2},{4,5},{5,4},{6,7},{7,6},{8,9},{9,8},{10,11... | collective-permute-start | bytes 368648 | tf_op jit(solution)/shard_map/ppermute | solution.py:363
  43.3 8.4 %collective-permute-start.7 = (bf16[30,2048]{1,0:T(8,128)(2,1)}, bf16[30,2048]{1,0:T(8,128)(2,1)}, u32[]{:S(2)}, u32[]{:S(2)}) collective-permute-start(bf16[30,2048]{1,0:T(8,128)(2,1)} %collective-permute-done.3.refs_4_), channel_id=1, source_target_pairs={{0,1},{1,0},{2,3},{3,2},{4,5},{5,4},{6,7},{7,6},{8,9},{9,8},{10,11... | collective-permute-start | bytes 368648 | tf_op jit(solution)/shard_map/ppermute | solution.py:363
  43.7 10.2 %collective-permute-start.9 = (bf16[30,2048]{1,0:T(8,128)(2,1)}, bf16[30,2048]{1,0:T(8,128)(2,1)}, u32[]{:S(2)}, u32[]{:S(2)}) collective-permute-start(bf16[30,2048]{1,0:T(8,128)(2,1)} %collective-permute-done.5.refs_6_), channel_id=1, source_target_pairs={{0,1},{1,0},{2,3},{3,2},{4,5},{5,4},{6,7},{7,6},{8,9},{9,8},{10,11... | collective-permute-start | bytes 368648 | tf_op jit(solution)/shard_map/ppermute | solution.py:363
  46.2 7.7 %copy-start = (bf16[30,2048]{1,0:T(8,128)(2,1)S(1)}, bf16[30,2048]{1,0:T(8,128)(2,1)}, u32[]{:S(2)}) copy-start(bf16[30,2048]{1,0:T(8,128)(2,1)} %refs_0_.2) | copy-start | bytes 368644
  46.2 31.7 %collective-permute-start.2 = (bf16[128,2048]{1,0:T(8,128)(2,1)}, bf16[128,2048]{1,0:T(8,128)(2,1)S(1)}, u32[]{:S(2)}, u32[]{:S(2)}) collective-permute-start(bf16[128,2048]{1,0:T(8,128)(2,1)} %broadcast_select_fusion), channel_id=1, source_target_pairs={{0,8},{8,0},{16,24},{24,16},{1,9},{9,1},{17,25},{25,17},{2,10},{10... | collective-permute-start | bytes 1572872 | tf_op jit(solution)/shard_map/ppermute | solution.py:501
  49.2 4.7 %copy-start.2 = (f32[2,2,128,128]{3,2,1,0:T(8,128)S(1)}, f32[2,2,128,128]{3,2,1,0:T(8,128)}, u32[]{:S(2)}) copy-start(f32[2,2,128,128]{3,2,1,0:T(8,128)} %copy-done.1) | copy-start | bytes 786436
  56.2 6.0 %collective-permute-start.14 = (bf16[256,256]{1,0:T(8,128)(2,1)S(1)}, bf16[256,256]{1,0:T(8,128)(2,1)S(1)}, u32[]{:S(2)}, u32[]{:S(2)}) collective-permute-start(bf16[256,256]{1,0:T(8,128)(2,1)S(1)} %get-tuple-element.22.refs_1_), channel_id=1, source_target_pairs={{0,16},{8,24},{16,0},{24,8},{1,17},{9,25},{17,1},{25,9},{2,18},{10... | collective-permute-start | bytes 393224 | tf_op jit(solution)/shard_map/ppermute | solution.py:432
  57.9 5.4 %collective-permute-start.11 = (bf16[192,256]{1,0:T(8,128)(2,1)S(1)}, bf16[192,256]{1,0:T(8,128)(2,1)S(1)}, u32[]{:S(2)}, u32[]{:S(2)}) collective-permute-start(bf16[192,256]{1,0:T(8,128)(2,1)S(1)} %get-tuple-element.23.refs_3_), channel_id=1, source_target_pairs={{0,16},{8,24},{16,0},{24,8},{1,17},{9,25},{17,1},{25,9},{2,18},{10... | collective-permute-start | bytes 294920 | tf_op jit(solution)/shard_map/ppermute | solution.py:432
  58.3 6.2 %collective-permute-start.10 = (bf16[256,256]{1,0:T(8,128)(2,1)S(1)}, bf16[256,256]{1,0:T(8,128)(2,1)S(1)}, u32[]{:S(2)}, u32[]{:S(2)}) collective-permute-start(bf16[256,256]{1,0:T(8,128)(2,1)S(1)} %get-tuple-element.22.refs_1_), channel_id=1, source_target_pairs={{0,8},{8,0},{16,24},{24,16},{1,9},{9,1},{17,25},{25,17},{2,10},{10... | collective-permute-start | bytes 393224 | tf_op jit(solution)/shard_map/ppermute | solution.py:442
  62.2 4.1 %collective-permute-start.15 = (bf16[256,256]{1,0:T(8,128)(2,1)S(1)}, bf16[256,256]{1,0:T(8,128)(2,1)S(1)}, u32[]{:S(2)}, u32[]{:S(2)}) collective-permute-start(bf16[256,256]{1,0:T(8,128)(2,1)S(1)} %collective-permute-done.14.refs_5_), channel_id=1, source_target_pairs={{0,8},{8,0},{16,24},{24,16},{1,9},{9,1},{17,25},{25,17},{2,10},{10... | collective-permute-start | bytes 393224 | tf_op jit(solution)/shard_map/ppermute | solution.py:442
  62.2 1.7 %collective-permute-start.12 = (bf16[192,256]{1,0:T(8,128)(2,1)S(1)}, bf16[192,256]{1,0:T(8,128)(2,1)S(1)}, u32[]{:S(2)}, u32[]{:S(2)}) collective-permute-start(bf16[192,256]{1,0:T(8,128)(2,1)S(1)} %get-tuple-element.23.refs_3_), channel_id=1, source_target_pairs={{0,8},{8,0},{16,24},{24,16},{1,9},{9,1},{17,25},{25,17},{2,10},{10... | collective-permute-start | bytes 294920 | tf_op jit(solution)/shard_map/ppermute | solution.py:442
  63.2 1.3 %collective-permute-start.13 = (bf16[192,256]{1,0:T(8,128)(2,1)S(1)}, bf16[192,256]{1,0:T(8,128)(2,1)S(1)}, u32[]{:S(2)}, u32[]{:S(2)}) collective-permute-start(bf16[192,256]{1,0:T(8,128)(2,1)S(1)} %collective-permute-done.11.refs_4_), channel_id=1, source_target_pairs={{0,8},{8,0},{16,24},{24,16},{1,9},{9,1},{17,25},{25,17},{2,10},{10... | collective-permute-start | bytes 294920 | tf_op jit(solution)/shard_map/ppermute | solution.py:442
  68.0 4.5 %collective-permute-start.16 = (bf16[2,32,128]{2,1,0:T(8,128)(2,1)S(1)}, bf16[2,32,128]{2,1,0:T(8,128)(2,1)S(1)}, u32[]{:S(2)}, u32[]{:S(2)}) collective-permute-start(bf16[2,32,128]{2,1,0:T(8,128)(2,1)S(1)} %get-tuple-element.31), channel_id=1, source_target_pairs={{0,2},{1,3},{2,0},{3,1},{4,6},{5,7},{6,4},{7,5},{8,10},{9,11},{10,... | collective-permute-start | bytes 49160 | tf_op jit(solution)/shard_map/ppermute | solution.py:355
  69.8 4.6 %collective-permute-start.17 = (bf16[2,32,128]{2,1,0:T(8,128)(2,1)S(1)}, bf16[2,32,128]{2,1,0:T(8,128)(2,1)S(1)}, u32[]{:S(2)}, u32[]{:S(2)}) collective-permute-start(bf16[2,32,128]{2,1,0:T(8,128)(2,1)S(1)} %get-tuple-element.30), channel_id=1, source_target_pairs={{0,4},{1,5},{2,6},{3,7},{4,0},{5,1},{6,2},{7,3},{8,12},{9,13},{10,... | collective-permute-start | bytes 49160 | tf_op jit(solution)/shard_map/ppermute | solution.py:355
  72.4 5.5 %collective-permute-start.18 = (bf16[2,32,128]{2,1,0:T(8,128)(2,1)S(1)}, bf16[2,32,128]{2,1,0:T(8,128)(2,1)S(1)}, u32[]{:S(2)}, u32[]{:S(2)}) collective-permute-start(bf16[2,32,128]{2,1,0:T(8,128)(2,1)S(1)} %get-tuple-element.29), channel_id=1, source_target_pairs={{0,6},{1,7},{2,4},{3,5},{4,2},{5,3},{6,0},{7,1},{8,14},{9,15},{10,... | collective-permute-start | bytes 49160 | tf_op jit(solution)/shard_map/ppermute | solution.py:355
  79.2 5.0 %collective-permute-start.19 = (bf16[32,2048]{1,0:T(8,128)(2,1)S(1)}, bf16[32,2048]{1,0:T(8,128)(2,1)S(1)}, u32[]{:S(2)}, u32[]{:S(2)}) collective-permute-start(bf16[32,2048]{1,0:T(8,128)(2,1)S(1)} %get-tuple-element.28), channel_id=1, source_target_pairs={{0,1},{1,0},{2,3},{3,2},{4,5},{5,4},{6,7},{7,6},{8,9},{9,8},{10,11... | collective-permute-start | bytes 393224 | tf_op jit(solution)/shard_map/ppermute | solution.py:363

commit v6 on v5

--- a/solution.py
+++ b/solution.py
@@ -283,12 +283,9 @@
 
 
 def partial_out_body(slots, share, ranks, outer, inner, pad, *refs):
-    here_ref, own_hbm = refs[:2]
+    here_ref, own_weight = refs[:2]
     held = refs[2 : 2 + len(slots)]
-    rest = refs[2 + len(slots) : -2]
-    own_weight, sem = refs[-2:]
-    move = pltpu.make_async_copy(own_hbm, own_weight, sem)
-    move.start()
+    rest = refs[2 + len(slots) :]
     parts, own_ref, others = rest[:outer], rest[outer], rest[1 + outer :]
     rows = inner * pad
     side = lax.rem(lax.div(here_ref[0], ranks), share)
@@ -304,7 +301,6 @@
         start = (start + weight.shape[0]) % VAL_DIM
         term = jnp.dot(rows_in, weight[...], preferred_element_type=F32)
         total = term if total is None else total + term
-    move.wait()
     total += jnp.dot(part(0), own_weight[...], preferred_element_type=F32)
     own_ref[...] = total[:pad]
     for j in range(1, inner):
@@ -504,7 +500,6 @@
         for k in range(1, outer):
             weights.append(along_outer(w_out, k, behind))
             slots.append((k, k))
-    depth = w_out.shape[0]
     total = call(
         functools.partial(partial_out_body, slots, share, ranks, outer, inner, pad),
         (sds((pad, width), F32),) + (sds((pad, width), BF16),) * (inner - 1),
@@ -512,8 +507,7 @@
         w_out,
         *weights,
         *parts,
-        scratch=[pltpu.VMEM((depth, width), BF16), pltpu.SemaphoreType.DMA],
-        in_specs=[SMEM, HBM] + [VMEM] * (len(weights) + outer),
+        in_specs=[SMEM] + [VMEM] * (1 + len(weights) + outer),
     )
     arrived = []
     for j in range(1, inner):

time: 85.4 us -> 84.5 us (0.989)
  no operation moved by 1% of the time
where the time goes in v6:
time: 84.5 us; the launch traced here: 84.2 us
  waiting for transfers between devices  38.7 us (46%)
  starting transfers between devices  31.8 us (38%)
  Pallas kernels  11.3 us (13%)
  other arithmetic  0.87 us (1%)
    ppermute x6, starting transfers between devices, along_outer(): return lax.ppermute(value, 'tp', pairs)  16.7 us
    ppermute x2, waiting for transfers between devices, joint(): return lax.ppermute(value, ('sp', 'tp'), moves)  11.7 us
    ppermute x6, waiting for transfers between devices, along_outer(): return lax.ppermute(value, 'tp', pairs)  11.7 us
    pallas_call x7, Pallas kernels, call(): pl.pallas_call(body, out_shape=outs, in_specs=in_specs, out_specs=jax.tre...  11.3 us
    ppermute x5, waiting for transfers between devices, along_inner(): return lax.ppermute(value, 'tp', pairs)  7.3 us
    ppermute x5, starting transfers between devices, along_inner(): return lax.ppermute(value, 'tp', pairs)  5.87 us
    ppermute x2, waiting for transfers between devices, along_lines(): return lax.ppermute(value, 'sp', pairs)  4.41 us
    ppermute x2, starting transfers between devices, joint(): return lax.ppermute(value, ('sp', 'tp'), moves)  4.07 us
  transfers between devices with their start and end apart: 21, of which 11 were waited for; matrix products, arithmetic and copies ran while one was open for 1% of the time, Pallas kernels for 12%

profile of v6, /device:TPU:0, one launch (start us, length us, event | category | flops | bytes accessed | tf_op | source)
XLA Modules:
  0.0 84.2 jit_solution(4576742865099233742)
XLA Ops:
  0.0 4.1 %collective-permute-start = (bf16[128,2048]{1,0:T(8,128)(2,1)}, bf16[128,2048]{1,0:T(8,128)(2,1)S(1)}, u32[]{:S(2)}, u32[]{:S(2)}) collective-permute-start(bf16[128,2048]{1,0:T(8,128)(2,1)} %refs_1_.3), channel_id=1, source_target_pairs={{0,4},{1,5},{2,6},{3,7},{4,0},{5,1},{6,2},{7,3},{8,10},{9,11},{10,... | collective-permute-start | bytes 1572872 | tf_op jit(solution)/shard_map/ppermute | solution.py:490
  4.1 11.7 %collective-permute-done.refs_2_ = bf16[128,2048]{1,0:T(8,128)(2,1)S(1)} collective-permute-done((bf16[128,2048]{1,0:T(8,128)(2,1)}, bf16[128,2048]{1,0:T(8,128)(2,1)S(1)}, u32[]{:S(2)}, u32[]{:S(2)}) %collective-permute-start) | collective-permute-done | bytes 524320 | tf_op jit(solution)/shard_map/ppermute | solution.py:490
  15.8 2.1 %collective-permute-start.4 = (bf16[30,2048]{1,0:T(8,128)(2,1)}, bf16[30,2048]{1,0:T(8,128)(2,1)S(1)}, u32[]{:S(2)}, u32[]{:S(2)}) collective-permute-start(bf16[30,2048]{1,0:T(8,128)(2,1)} %refs_0_.2), channel_id=1, source_target_pairs={{0,4},{1,5},{2,6},{3,7},{4,0},{5,1},{6,2},{7,3},{8,12},{9,13},{10,... | collective-permute-start | bytes 368648 | tf_op jit(solution)/shard_map/ppermute | solution.py:351
  17.9 3.6 %collective-permute-start.3 = (bf16[30,2048]{1,0:T(8,128)(2,1)}, bf16[30,2048]{1,0:T(8,128)(2,1)}, u32[]{:S(2)}, u32[]{:S(2)}) collective-permute-start(bf16[30,2048]{1,0:T(8,128)(2,1)} %refs_0_.2), channel_id=1, source_target_pairs={{0,2},{1,3},{2,0},{3,1},{4,6},{5,7},{6,4},{7,5},{8,10},{9,11},{10,... | collective-permute-start | bytes 368648 | tf_op jit(solution)/shard_map/ppermute | solution.py:351
  21.5 6.2 %collective-permute-done.4.refs_5_ = bf16[30,2048]{1,0:T(8,128)(2,1)S(1)} collective-permute-done((bf16[30,2048]{1,0:T(8,128)(2,1)}, bf16[30,2048]{1,0:T(8,128)(2,1)S(1)}, u32[]{:S(2)}, u32[]{:S(2)}) %collective-permute-start.4) | collective-permute-done | bytes 122912 | tf_op jit(solution)/shard_map/ppermute | solution.py:351
  27.7 6.6 %collective-permute-start.5 = (bf16[30,2048]{1,0:T(8,128)(2,1)S(1)}, bf16[30,2048]{1,0:T(8,128)(2,1)}, u32[]{:S(2)}, u32[]{:S(2)}) collective-permute-start(bf16[30,2048]{1,0:T(8,128)(2,1)S(1)} %collective-permute-done.4.refs_5_), channel_id=1, source_target_pairs={{0,2},{1,3},{2,0},{3,1},{4,6},{5,7},{6,4},{7,5},{8,10},{9,11},{10,... | collective-permute-start | bytes 368648 | tf_op jit(solution)/shard_map/ppermute | solution.py:351
  34.3 1.5 %collective-permute-start.6 = (bf16[30,2048]{1,0:T(8,128)(2,1)}, bf16[30,2048]{1,0:T(8,128)(2,1)}, u32[]{:S(2)}, u32[]{:S(2)}) collective-permute-start(bf16[30,2048]{1,0:T(8,128)(2,1)} %refs_0_.2), channel_id=1, source_target_pairs={{0,1},{1,0},{2,3},{3,2},{4,5},{5,4},{6,7},{7,6},{8,9},{9,8},{10,11... | collective-permute-start | bytes 368648 | tf_op jit(solution)/shard_map/ppermute | solution.py:359
  35.8 2.5 %shard_map.100 = (bf16[32,2,768]{2,1,0:T(2,128)(2,1)}, f32[2,2,128,128]{3,2,1,0:T(8,128)S(1)}, bf16[2048,384]{1,0:T(8,128)(2,1)S(1)}) custom-call(s32[1]{0:T(128)} %bitcast.refs_0_, f32[1,512]{1,0:T(1,128)} %bitcast.11, f32[1,512]{1,0:T(1,128)} %bitcast.12, bf16[512,768]{1,0:T(8,128)(2,1)} %refs_3_.2, bf16[2048,128]{1,0:T(8,128)(2,1)} %refs_4_.1, ...), custom_call_target="tpu_custom_call" | custom-call | flops 2000000 | tf_op jit(solution)/shard_map/pallas_call | solution.py:59
  39.0 2.6 %all-to-all-start = ((bf16[32,2,768]{2,1,0:T(2,128)(2,1)}), bf16[32,2,768]{2,1,0:T(2,128)(2,1)S(1)}, u32[]{:S(2)}, u32[]{:S(2)}) async-start(bf16[32,2,768]{2,1,0:T(2,128)(2,1)} %get-tuple-element.17), calls=%async_computation | async-start | bytes 196608 | tf_op jit(solution)/shard_map/all_to_all | solution.py:386
  41.6 1.7 %collective-permute-start.8 = (bf16[30,2048]{1,0:T(8,128)(2,1)S(1)}, bf16[30,2048]{1,0:T(8,128)(2,1)}, u32[]{:S(2)}, u32[]{:S(2)}) collective-permute-start(bf16[30,2048]{1,0:T(8,128)(2,1)S(1)} %collective-permute-done.4.refs_5_), channel_id=1, source_target_pairs={{0,1},{1,0},{2,3},{3,2},{4,5},{5,4},{6,7},{7,6},{8,9},{9,8},{10,11... | collective-permute-start | bytes 368648 | tf_op jit(solution)/shard_map/ppermute | solution.py:359
  43.7 1.6 %collective-permute-start.9 = (bf16[30,2048]{1,0:T(8,128)(2,1)}, bf16[30,2048]{1,0:T(8,128)(2,1)}, u32[]{:S(2)}, u32[]{:S(2)}) collective-permute-start(bf16[30,2048]{1,0:T(8,128)(2,1)} %collective-permute-done.5.refs_6_), channel_id=1, source_target_pairs={{0,1},{1,0},{2,3},{3,2},{4,5},{5,4},{6,7},{7,6},{8,9},{9,8},{10,11... | collective-permute-start | bytes 368648 | tf_op jit(solution)/shard_map/ppermute | solution.py:359
  46.2 3.0 %all-to-all-done.refs_0_ = bf16[32,2,768]{2,1,0:T(2,128)(2,1)S(1)} async-done(((bf16[32,2,768]{2,1,0:T(2,128)(2,1)}), bf16[32,2,768]{2,1,0:T(2,128)(2,1)S(1)}, u32[]{:S(2)}, u32[]{:S(2)}) %all-to-all-start) | async-done | bytes 98336 | tf_op jit(solution)/shard_map/all_to_all | solution.py:386
  49.2 1.8 %shard_map.101 = (f32[2,6144]{1,0:T(2,128)S(1)}, bf16[192,256]{1,0:T(8,128)(2,1)S(1)}) custom-call(bf16[32,2,768]{2,1,0:T(2,128)(2,1)S(1)} %all-to-all-done.refs_0_, bf16[192,2048]{1,0:T(8,128)(2,1)} %refs_1_.2, bf16[2048,384]{1,0:T(8,128)(2,1)S(1)} %get-tuple-element.18.refs_2_), custom_call_target="tpu_custom_call" | custom-call | flops 2000000 | tf_op jit(solution)/shard_map/pallas_call | solution.py:59
  51.7 2.1 %collective-permute-done.9.refs_10_ = bf16[30,2048]{1,0:T(8,128)(2,1)} collective-permute-done((bf16[30,2048]{1,0:T(8,128)(2,1)}, bf16[30,2048]{1,0:T(8,128)(2,1)}, u32[]{:S(2)}, u32[]{:S(2)}) %collective-permute-start.9) | collective-permute-done | bytes 122912 | tf_op jit(solution)/shard_map/ppermute | solution.py:359
  53.9 2.3 %shard_map.102 = (bf16[2,128,128]{2,1,0:T(8,128)(2,1)S(1)}, bf16[256,256]{1,0:T(8,128)(2,1)S(1)}) custom-call(f32[2,6144]{1,0:T(2,128)S(1)} %get-tuple-element.19.refs_0_.refs_1_, f32[2,2,128,128]{3,2,1,0:T(8,128)S(1)} %copy-done.3, bf16[2048,384]{1,0:T(8,128)(2,1)S(1)} %get-tuple-element.18.refs_2_, bf16[30,2048]{1,0:T(8,128)(2,1)S(1)} %copy-done.1, ...), custom_call_target="tpu_custom_call" | custom-call | flops 2000000 | tf_op jit(solution)/shard_map/pallas_call | solution.py:59
  56.2 1.7 %collective-permute-start.14 = (bf16[256,256]{1,0:T(8,128)(2,1)S(1)}, bf16[256,256]{1,0:T(8,128)(2,1)S(1)}, u32[]{:S(2)}, u32[]{:S(2)}) collective-permute-start(bf16[256,256]{1,0:T(8,128)(2,1)S(1)} %get-tuple-element.22.refs_1_), channel_id=1, source_target_pairs={{0,16},{8,24},{16,0},{24,8},{1,17},{9,25},{17,1},{25,9},{2,18},{10... | collective-permute-start | bytes 393224 | tf_op jit(solution)/shard_map/ppermute | solution.py:428
  58.3 3.9 %collective-permute-done.14.refs_5_ = bf16[256,256]{1,0:T(8,128)(2,1)S(1)} collective-permute-done((bf16[256,256]{1,0:T(8,128)(2,1)S(1)}, bf16[256,256]{1,0:T(8,128)(2,1)S(1)}, u32[]{:S(2)}, u32[]{:S(2)}) %collective-permute-start.14) | collective-permute-done | bytes 131104 | tf_op jit(solution)/shard_map/ppermute | solution.py:428
  64.5 1.8 %shard_map.103 = (f32[2,2,128,1]{3,2,1,0:T(8,128)S(1)}, f32[2,2,128,1]{3,2,1,0:T(8,128)S(1)}, f32[2,2,128,128]{3,2,1,0:T(8,128)S(1)}) custom-call(bf16[2,128,128]{2,1,0:T(8,128)(2,1)S(1)} %get-tuple-element.21.refs_0_.refs_4_, bf16[256,256]{1,0:T(8,128)(2,1)S(1)} %get-tuple-element.22.refs_1_, bf16[256,256]{1,0:T(8,128)(2,1)S(1)} %collective-permute-done.10.refs_2_, ...), custom_call_target="tpu_custom_call" | custom-call | flops 2000000 | tf_op jit(solution)/shard_map/pallas_call | solution.py:59
  66.3 1.7 %shard_map.104 = bf16[4,2,32,128]{3,2,1,0:T(8,128)(2,1)S(1)} custom-call(f32[1]{0:T(128)S(6)} %copy.11.refs_0_, f32[2,2,128,1]{3,2,1,0:T(8,128)S(1)} %get-tuple-element.24.refs_1_, f32[2,2,128,1]{3,2,1,0:T(8,128)S(1)} %get-tuple-element.25.refs_2_, f32[2,2,128,128]{3,2,1,0:T(8,128)S(1)} %get-tuple-element.26.refs_3_, ...), custom_call_target="tpu_custom_call" | custom-call | flops 2000000 | tf_op jit(solution)/shard_map/pallas_call | solution.py:59
  68.0 1.8 %collective-permute-start.16 = (bf16[2,32,128]{2,1,0:T(8,128)(2,1)S(1)}, bf16[2,32,128]{2,1,0:T(8,128)(2,1)S(1)}, u32[]{:S(2)}, u32[]{:S(2)}) collective-permute-start(bf16[2,32,128]{2,1,0:T(8,128)(2,1)S(1)} %get-tuple-element.31), channel_id=1, source_target_pairs={{0,2},{1,3},{2,0},{3,1},{4,6},{5,7},{6,4},{7,5},{8,10},{9,11},{10,... | collective-permute-start | bytes 49160 | tf_op jit(solution)/shard_map/ppermute | solution.py:351
  69.8 2.6 %collective-permute-start.17 = (bf16[2,32,128]{2,1,0:T(8,128)(2,1)S(1)}, bf16[2,32,128]{2,1,0:T(8,128)(2,1)S(1)}, u32[]{:S(2)}, u32[]{:S(2)}) collective-permute-start(bf16[2,32,128]{2,1,0:T(8,128)(2,1)S(1)} %get-tuple-element.30), channel_id=1, source_target_pairs={{0,4},{1,5},{2,6},{3,7},{4,0},{5,1},{6,2},{7,3},{8,12},{9,13},{10,... | collective-permute-start | bytes 49160 | tf_op jit(solution)/shard_map/ppermute | solution.py:351
  72.5 2.0 %collective-permute-done.17.refs_7_ = bf16[2,32,128]{2,1,0:T(8,128)(2,1)S(1)} collective-permute-done((bf16[2,32,128]{2,1,0:T(8,128)(2,1)S(1)}, bf16[2,32,128]{2,1,0:T(8,128)(2,1)S(1)}, u32[]{:S(2)}, u32[]{:S(2)}) %collective-permute-start.17) | collective-permute-done | bytes 16416 | tf_op jit(solution)/shard_map/ppermute | solution.py:351
  74.5 3.5 %collective-permute-done.18.refs_8_ = bf16[2,32,128]{2,1,0:T(8,128)(2,1)S(1)} collective-permute-done((bf16[2,32,128]{2,1,0:T(8,128)(2,1)S(1)}, bf16[2,32,128]{2,1,0:T(8,128)(2,1)S(1)}, u32[]{:S(2)}, u32[]{:S(2)}) %collective-permute-start.18) | collective-permute-done | bytes 16416 | tf_op jit(solution)/shard_map/ppermute | solution.py:351
  79.0 4.4 %collective-permute-done.19.refs_3_ = bf16[32,2048]{1,0:T(8,128)(2,1)S(1)} collective-permute-done((bf16[32,2048]{1,0:T(8,128)(2,1)S(1)}, bf16[32,2048]{1,0:T(8,128)(2,1)S(1)}, u32[]{:S(2)}, u32[]{:S(2)}) %collective-permute-start.19) | collective-permute-done | bytes 131104 | tf_op jit(solution)/shard_map/ppermute | solution.py:359
  (35 shorter events, 6.9 us)
Async XLA Ops:
  0.0 15.8 %collective-permute-start = (bf16[128,2048]{1,0:T(8,128)(2,1)}, bf16[128,2048]{1,0:T(8,128)(2,1)S(1)}, u32[]{:S(2)}, u32[]{:S(2)}) collective-permute-start(bf16[128,2048]{1,0:T(8,128)(2,1)} %refs_1_.3), channel_id=1, source_target_pairs={{0,4},{1,5},{2,6},{3,7},{4,0},{5,1},{6,2},{7,3},{8,10},{9,11},{10,... | collective-permute-start | bytes 1572872 | tf_op jit(solution)/shard_map/ppermute | solution.py:490
  15.8 29.5 %collective-permute-start.1 = (bf16[128,2048]{1,0:T(8,128)(2,1)S(1)}, bf16[128,2048]{1,0:T(8,128)(2,1)S(1)}, u32[]{:S(2)}, u32[]{:S(2)}) collective-permute-start(bf16[128,2048]{1,0:T(8,128)(2,1)S(1)} %collective-permute-done.refs_2_), channel_id=1, source_target_pairs={{0,10},{1,11},{2,8},{3,9},{4,14},{5,15},{6,12},{7,13},{8,0},{9,1},... | collective-permute-start | bytes 1572872 | tf_op jit(solution)/shard_map/ppermute | solution.py:490
  15.8 11.9 %collective-permute-start.4 = (bf16[30,2048]{1,0:T(8,128)(2,1)}, bf16[30,2048]{1,0:T(8,128)(2,1)S(1)}, u32[]{:S(2)}, u32[]{:S(2)}) collective-permute-start(bf16[30,2048]{1,0:T(8,128)(2,1)} %refs_0_.2), channel_id=1, source_target_pairs={{0,4},{1,5},{2,6},{3,7},{4,0},{5,1},{6,2},{7,3},{8,12},{9,13},{10,... | collective-permute-start | bytes 368648 | tf_op jit(solution)/shard_map/ppermute | solution.py:351
  17.9 25.4 %collective-permute-start.3 = (bf16[30,2048]{1,0:T(8,128)(2,1)}, bf16[30,2048]{1,0:T(8,128)(2,1)}, u32[]{:S(2)}, u32[]{:S(2)}) collective-permute-start(bf16[30,2048]{1,0:T(8,128)(2,1)} %refs_0_.2), channel_id=1, source_target_pairs={{0,2},{1,3},{2,0},{3,1},{4,6},{5,7},{6,4},{7,5},{8,10},{9,11},{10,... | collective-permute-start | bytes 368648 | tf_op jit(solution)/shard_map/ppermute | solution.py:351
  27.7 16.0 %collective-permute-start.5 = (bf16[30,2048]{1,0:T(8,128)(2,1)S(1)}, bf16[30,2048]{1,0:T(8,128)(2,1)}, u32[]{:S(2)}, u32[]{:S(2)}) collective-permute-start(bf16[30,2048]{1,0:T(8,128)(2,1)S(1)} %collective-permute-done.4.refs_5_), channel_id=1, source_target_pairs={{0,2},{1,3},{2,0},{3,1},{4,6},{5,7},{6,4},{7,5},{8,10},{9,11},{10,... | collective-permute-start | bytes 368648 | tf_op jit(solution)/shard_map/ppermute | solution.py:351
  34.3 16.7 %collective-permute-start.6 = (bf16[30,2048]{1,0:T(8,128)(2,1)}, bf16[30,2048]{1,0:T(8,128)(2,1)}, u32[]{:S(2)}, u32[]{:S(2)}) collective-permute-start(bf16[30,2048]{1,0:T(8,128)(2,1)} %refs_0_.2), channel_id=1, source_target_pairs={{0,1},{1,0},{2,3},{3,2},{4,5},{5,4},{6,7},{7,6},{8,9},{9,8},{10,11... | collective-permute-start | bytes 368648 | tf_op jit(solution)/shard_map/ppermute | solution.py:359
  39.0 10.2 %all-to-all-start = ((bf16[32,2,768]{2,1,0:T(2,128)(2,1)}), bf16[32,2,768]{2,1,0:T(2,128)(2,1)S(1)}, u32[]{:S(2)}, u32[]{:S(2)}) async-start(bf16[32,2,768]{2,1,0:T(2,128)(2,1)} %get-tuple-element.17), calls=%async_computation | async-start | bytes 196608 | tf_op jit(solution)/shard_map/all_to_all | solution.py:386
  41.6 9.4 %collective-permute-start.8 = (bf16[30,2048]{1,0:T(8,128)(2,1)S(1)}, bf16[30,2048]{1,0:T(8,128)(2,1)}, u32[]{:S(2)}, u32[]{:S(2)}) collective-permute-start(bf16[30,2048]{1,0:T(8,128)(2,1)S(1)} %collective-permute-done.4.refs_5_), channel_id=1, source_target_pairs={{0,1},{1,0},{2,3},{3,2},{4,5},{5,4},{6,7},{7,6},{8,9},{9,8},{10,11... | collective-permute-start | bytes 368648 | tf_op jit(solution)/shard_map/ppermute | solution.py:359
  43.3 8.4 %collective-permute-start.7 = (bf16[30,2048]{1,0:T(8,128)(2,1)}, bf16[30,2048]{1,0:T(8,128)(2,1)}, u32[]{:S(2)}, u32[]{:S(2)}) collective-permute-start(bf16[30,2048]{1,0:T(8,128)(2,1)} %collective-permute-done.3.refs_4_), channel_id=1, source_target_pairs={{0,1},{1,0},{2,3},{3,2},{4,5},{5,4},{6,7},{7,6},{8,9},{9,8},{10,11... | collective-permute-start | bytes 368648 | tf_op jit(solution)/shard_map/ppermute | solution.py:359
  43.7 10.2 %collective-permute-start.9 = (bf16[30,2048]{1,0:T(8,128)(2,1)}, bf16[30,2048]{1,0:T(8,128)(2,1)}, u32[]{:S(2)}, u32[]{:S(2)}) collective-permute-start(bf16[30,2048]{1,0:T(8,128)(2,1)} %collective-permute-done.5.refs_6_), channel_id=1, source_target_pairs={{0,1},{1,0},{2,3},{3,2},{4,5},{5,4},{6,7},{7,6},{8,9},{9,8},{10,11... | collective-permute-start | bytes 368648 | tf_op jit(solution)/shard_map/ppermute | solution.py:359
  46.2 7.7 %copy-start.1 = (bf16[30,2048]{1,0:T(8,128)(2,1)S(1)}, bf16[30,2048]{1,0:T(8,128)(2,1)}, u32[]{:S(2)}) copy-start(bf16[30,2048]{1,0:T(8,128)(2,1)} %refs_0_.2) | copy-start | bytes 368644
  46.2 31.8 %collective-permute-start.2 = (bf16[128,2048]{1,0:T(8,128)(2,1)}, bf16[128,2048]{1,0:T(8,128)(2,1)S(1)}, u32[]{:S(2)}, u32[]{:S(2)}) collective-permute-start(bf16[128,2048]{1,0:T(8,128)(2,1)} %broadcast_select_fusion), channel_id=1, source_target_pairs={{0,8},{8,0},{16,24},{24,16},{1,9},{9,1},{17,25},{25,17},{2,10},{10... | collective-permute-start | bytes 1572872 | tf_op jit(solution)/shard_map/ppermute | solution.py:497
  49.2 4.7 %copy-start.3 = (f32[2,2,128,128]{3,2,1,0:T(8,128)S(1)}, f32[2,2,128,128]{3,2,1,0:T(8,128)}, u32[]{:S(2)}) copy-start(f32[2,2,128,128]{3,2,1,0:T(8,128)} %copy-done.2) | copy-start | bytes 786436
  56.2 21.8 %copy-start = (bf16[128,2048]{1,0:T(8,128)(2,1)S(1)}, bf16[128,2048]{1,0:T(8,128)(2,1)}, u32[]{:S(2)}) copy-start(bf16[128,2048]{1,0:T(8,128)(2,1)} %refs_1_.3) | copy-start | bytes 1572868
  56.2 6.0 %collective-permute-start.14 = (bf16[256,256]{1,0:T(8,128)(2,1)S(1)}, bf16[256,256]{1,0:T(8,128)(2,1)S(1)}, u32[]{:S(2)}, u32[]{:S(2)}) collective-permute-start(bf16[256,256]{1,0:T(8,128)(2,1)S(1)} %get-tuple-element.22.refs_1_), channel_id=1, source_target_pairs={{0,16},{8,24},{16,0},{24,8},{1,17},{9,25},{17,1},{25,9},{2,18},{10... | collective-permute-start | bytes 393224 | tf_op jit(solution)/shard_map/ppermute | solution.py:428
  57.9 5.3 %collective-permute-start.11 = (bf16[192,256]{1,0:T(8,128)(2,1)S(1)}, bf16[192,256]{1,0:T(8,128)(2,1)S(1)}, u32[]{:S(2)}, u32[]{:S(2)}) collective-permute-start(bf16[192,256]{1,0:T(8,128)(2,1)S(1)} %get-tuple-element.23.refs_3_), channel_id=1, source_target_pairs={{0,16},{8,24},{16,0},{24,8},{1,17},{9,25},{17,1},{25,9},{2,18},{10... | collective-permute-start | bytes 294920 | tf_op jit(solution)/shard_map/ppermute | solution.py:428
  58.3 6.2 %collective-permute-start.10 = (bf16[256,256]{1,0:T(8,128)(2,1)S(1)}, bf16[256,256]{1,0:T(8,128)(2,1)S(1)}, u32[]{:S(2)}, u32[]{:S(2)}) collective-permute-start(bf16[256,256]{1,0:T(8,128)(2,1)S(1)} %get-tuple-element.22.refs_1_), channel_id=1, source_target_pairs={{0,8},{8,0},{16,24},{24,16},{1,9},{9,1},{17,25},{25,17},{2,10},{10... | collective-permute-start | bytes 393224 | tf_op jit(solution)/shard_map/ppermute | solution.py:438
  62.2 4.1 %collective-permute-start.15 = (bf16[256,256]{1,0:T(8,128)(2,1)S(1)}, bf16[256,256]{1,0:T(8,128)(2,1)S(1)}, u32[]{:S(2)}, u32[]{:S(2)}) collective-permute-start(bf16[256,256]{1,0:T(8,128)(2,1)S(1)} %collective-permute-done.14.refs_5_), channel_id=1, source_target_pairs={{0,8},{8,0},{16,24},{24,16},{1,9},{9,1},{17,25},{25,17},{2,10},{10... | collective-permute-start | bytes 393224 | tf_op jit(solution)/shard_map/ppermute | solution.py:438
  62.2 1.7 %collective-permute-start.12 = (bf16[192,256]{1,0:T(8,128)(2,1)S(1)}, bf16[192,256]{1,0:T(8,128)(2,1)S(1)}, u32[]{:S(2)}, u32[]{:S(2)}) collective-permute-start(bf16[192,256]{1,0:T(8,128)(2,1)S(1)} %get-tuple-element.23.refs_3_), channel_id=1, source_target_pairs={{0,8},{8,0},{16,24},{24,16},{1,9},{9,1},{17,25},{25,17},{2,10},{10... | collective-permute-start | bytes 294920 | tf_op jit(solution)/shard_map/ppermute | solution.py:438
  63.2 1.3 %collective-permute-start.13 = (bf16[192,256]{1,0:T(8,128)(2,1)S(1)}, bf16[192,256]{1,0:T(8,128)(2,1)S(1)}, u32[]{:S(2)}, u32[]{:S(2)}) collective-permute-start(bf16[192,256]{1,0:T(8,128)(2,1)S(1)} %collective-permute-done.11.refs_4_), channel_id=1, source_target_pairs={{0,8},{8,0},{16,24},{24,16},{1,9},{9,1},{17,25},{25,17},{2,10},{10... | collective-permute-start | bytes 294920 | tf_op jit(solution)/shard_map/ppermute | solution.py:438
  68.0 4.5 %collective-permute-start.16 = (bf16[2,32,128]{2,1,0:T(8,128)(2,1)S(1)}, bf16[2,32,128]{2,1,0:T(8,128)(2,1)S(1)}, u32[]{:S(2)}, u32[]{:S(2)}) collective-permute-start(bf16[2,32,128]{2,1,0:T(8,128)(2,1)S(1)} %get-tuple-element.31), channel_id=1, source_target_pairs={{0,2},{1,3},{2,0},{3,1},{4,6},{5,7},{6,4},{7,5},{8,10},{9,11},{10,... | collective-permute-start | bytes 49160 | tf_op jit(solution)/shard_map/ppermute | solution.py:351
  69.8 4.6 %collective-permute-start.17 = (bf16[2,32,128]{2,1,0:T(8,128)(2,1)S(1)}, bf16[2,32,128]{2,1,0:T(8,128)(2,1)S(1)}, u32[]{:S(2)}, u32[]{:S(2)}) collective-permute-start(bf16[2,32,128]{2,1,0:T(8,128)(2,1)S(1)} %get-tuple-element.30), channel_id=1, source_target_pairs={{0,4},{1,5},{2,6},{3,7},{4,0},{5,1},{6,2},{7,3},{8,12},{9,13},{10,... | collective-permute-start | bytes 49160 | tf_op jit(solution)/shard_map/ppermute | solution.py:351
  72.4 5.5 %collective-permute-start.18 = (bf16[2,32,128]{2,1,0:T(8,128)(2,1)S(1)}, bf16[2,32,128]{2,1,0:T(8,128)(2,1)S(1)}, u32[]{:S(2)}, u32[]{:S(2)}) collective-permute-start(bf16[2,32,128]{2,1,0:T(8,128)(2,1)S(1)} %get-tuple-element.29), channel_id=1, source_target_pairs={{0,6},{1,7},{2,4},{3,5},{4,2},{5,3},{6,0},{7,1},{8,14},{9,15},{10,... | collective-permute-start | bytes 49160 | tf_op jit(solution)/shard_map/ppermute | solution.py:351
  78.4 5.0 %collective-permute-start.19 = (bf16[32,2048]{1,0:T(8,128)(2,1)S(1)}, bf16[32,2048]{1,0:T(8,128)(2,1)S(1)}, u32[]{:S(2)}, u32[]{:S(2)}) collective-permute-start(bf16[32,2048]{1,0:T(8,128)(2,1)S(1)} %get-tuple-element.28), channel_id=1, source_target_pairs={{0,1},{1,0},{2,3},{3,2},{4,5},{5,4},{6,7},{7,6},{8,9},{9,8},{10,11... | collective-permute-start | bytes 393224 | tf_op jit(solution)/shard_map/ppermute | solution.py:359
  (1 other events, 0.7 us)

commit v7 on v6

--- a/solution.py
+++ b/solution.py
@@ -235,8 +235,10 @@
 
 
 def attend_first_body(number, pad, padded, inner, *refs):
-    q_ref, kv_refs = refs[0], refs[1:-5]
-    top_ref, sum_ref, mix_ref, k_all, v_all = refs[-5:]
+    exit_hbm, q_ref, kv_refs = refs[0], refs[1], refs[2:-7]
+    top_ref, sum_ref, mix_ref, exit_ref, k_all, v_all, sem = refs[-7:]
+    move = pltpu.make_async_copy(exit_hbm, exit_ref, sem)
+    move.start()
     bias = gather_pieces(kv_refs, padded, number, pad, k_all, v_all)
 
     def one(j, carry):
@@ -252,6 +254,7 @@
         return carry
 
     repeat(inner, one)
+    move.wait()
 
 
 def attend_last_body(number, pad, outer, inner, *refs):
@@ -452,13 +455,15 @@
         return [pltpu.VMEM((keys, wide), BF16), pltpu.VMEM((keys, VAL_DIM), BF16)]
 
     keys = groups * held + len(first) * inner * tile
-    first_stats = call(
+    *first_stats, exit_weight = call(
         functools.partial(attend_first_body, number, pad, len(first), inner),
-        stats,
+        stats + (sds(w_out.shape, BF16),),
+        w_out,
         queries,
         *early,
-        scratch=room(keys),
+        scratch=room(keys) + [pltpu.SemaphoreType.DMA],
         extra=tile * keys * 12,
+        in_specs=[HBM] + [VMEM] * (1 + len(early)),
         local=True,
     )
     keys = len(late) * inner * tile
@@ -504,7 +509,7 @@
         functools.partial(partial_out_body, slots, share, ranks, outer, inner, pad),
         (sds((pad, width), F32),) + (sds((pad, width), BF16),) * (inner - 1),
         here,
-        w_out,
+        exit_weight,
         *weights,
         *parts,
         in_specs=[SMEM] + [VMEM] * (1 + len(weights) + outer),

time: 84.5 us -> 84.5 us (level)
  no operation moved by 1% of the time
where the time goes in v7:
time: 84.5 us; the launch traced here: 84.2 us
  waiting for transfers between devices  38.7 us (46%)
  starting transfers between devices  31.8 us (38%)
  Pallas kernels  11.3 us (13%)
  other arithmetic  0.88 us (1%)
    ppermute x6, starting transfers between devices, along_outer(): return lax.ppermute(value, 'tp', pairs)  16.7 us
    ppermute x2, waiting for transfers between devices, joint(): return lax.ppermute(value, ('sp', 'tp'), moves)  11.7 us
    ppermute x6, waiting for transfers between devices, along_outer(): return lax.ppermute(value, 'tp', pairs)  11.7 us
    pallas_call x7, Pallas kernels, call(): pl.pallas_call(body, out_shape=outs, in_specs=in_specs, out_specs=jax.tre...  11.3 us
    ppermute x5, waiting for transfers between devices, along_inner(): return lax.ppermute(value, 'tp', pairs)  7.3 us
    ppermute x5, starting transfers between devices, along_inner(): return lax.ppermute(value, 'tp', pairs)  5.88 us
    ppermute x2, waiting for transfers between devices, along_lines(): return lax.ppermute(value, 'sp', pairs)  4.41 us
    ppermute x2, starting transfers between devices, joint(): return lax.ppermute(value, ('sp', 'tp'), moves)  4.07 us
  transfers between devices with their start and end apart: 21, of which 11 were waited for; matrix products, arithmetic and copies ran while one was open for 1% of the time, Pallas kernels for 12%

profile of v7, /device:TPU:0, one launch (start us, length us, event | category | flops | bytes accessed | tf_op | source)
XLA Modules:
  0.0 84.2 jit_solution(11923075317192067858)
XLA Ops:
  0.0 4.1 %collective-permute-start.11 = (bf16[128,2048]{1,0:T(8,128)(2,1)}, bf16[128,2048]{1,0:T(8,128)(2,1)S(1)}, u32[]{:S(2)}, u32[]{:S(2)}) collective-permute-start(bf16[128,2048]{1,0:T(8,128)(2,1)} %refs_0_.3), channel_id=1, source_target_pairs={{0,4},{1,5},{2,6},{3,7},{4,0},{5,1},{6,2},{7,3},{8,10},{9,11},{10,... | collective-permute-start | bytes 1572872 | tf_op jit(solution)/shard_map/ppermute | solution.py:495
  4.1 11.7 %collective-permute-done.11.refs_2_ = bf16[128,2048]{1,0:T(8,128)(2,1)S(1)} collective-permute-done((bf16[128,2048]{1,0:T(8,128)(2,1)}, bf16[128,2048]{1,0:T(8,128)(2,1)S(1)}, u32[]{:S(2)}, u32[]{:S(2)}) %collective-permute-start.11) | collective-permute-done | bytes 524320 | tf_op jit(solution)/shard_map/ppermute | solution.py:495
  15.8 2.1 %collective-permute-start.1 = (bf16[30,2048]{1,0:T(8,128)(2,1)}, bf16[30,2048]{1,0:T(8,128)(2,1)S(1)}, u32[]{:S(2)}, u32[]{:S(2)}) collective-permute-start(bf16[30,2048]{1,0:T(8,128)(2,1)} %refs_0_.4), channel_id=1, source_target_pairs={{0,4},{1,5},{2,6},{3,7},{4,0},{5,1},{6,2},{7,3},{8,12},{9,13},{10,... | collective-permute-start | bytes 368648 | tf_op jit(solution)/shard_map/ppermute | solution.py:354
  17.9 3.6 %collective-permute-start = (bf16[30,2048]{1,0:T(8,128)(2,1)}, bf16[30,2048]{1,0:T(8,128)(2,1)}, u32[]{:S(2)}, u32[]{:S(2)}) collective-permute-start(bf16[30,2048]{1,0:T(8,128)(2,1)} %refs_0_.4), channel_id=1, source_target_pairs={{0,2},{1,3},{2,0},{3,1},{4,6},{5,7},{6,4},{7,5},{8,10},{9,11},{10,... | collective-permute-start | bytes 368648 | tf_op jit(solution)/shard_map/ppermute | solution.py:354
  21.5 6.2 %collective-permute-done.1.refs_5_ = bf16[30,2048]{1,0:T(8,128)(2,1)S(1)} collective-permute-done((bf16[30,2048]{1,0:T(8,128)(2,1)}, bf16[30,2048]{1,0:T(8,128)(2,1)S(1)}, u32[]{:S(2)}, u32[]{:S(2)}) %collective-permute-start.1) | collective-permute-done | bytes 122912 | tf_op jit(solution)/shard_map/ppermute | solution.py:354
  27.7 6.6 %collective-permute-start.2 = (bf16[30,2048]{1,0:T(8,128)(2,1)S(1)}, bf16[30,2048]{1,0:T(8,128)(2,1)}, u32[]{:S(2)}, u32[]{:S(2)}) collective-permute-start(bf16[30,2048]{1,0:T(8,128)(2,1)S(1)} %collective-permute-done.1.refs_5_), channel_id=1, source_target_pairs={{0,2},{1,3},{2,0},{3,1},{4,6},{5,7},{6,4},{7,5},{8,10},{9,11},{10,... | collective-permute-start | bytes 368648 | tf_op jit(solution)/shard_map/ppermute | solution.py:354
  34.3 1.5 %collective-permute-start.3 = (bf16[30,2048]{1,0:T(8,128)(2,1)}, bf16[30,2048]{1,0:T(8,128)(2,1)}, u32[]{:S(2)}, u32[]{:S(2)}) collective-permute-start(bf16[30,2048]{1,0:T(8,128)(2,1)} %refs_0_.4), channel_id=1, source_target_pairs={{0,1},{1,0},{2,3},{3,2},{4,5},{5,4},{6,7},{7,6},{8,9},{9,8},{10,11... | collective-permute-start | bytes 368648 | tf_op jit(solution)/shard_map/ppermute | solution.py:362
  35.8 2.5 %shard_map.100 = (bf16[32,2,768]{2,1,0:T(2,128)(2,1)}, f32[2,2,128,128]{3,2,1,0:T(8,128)S(1)}, bf16[2048,384]{1,0:T(8,128)(2,1)S(1)}) custom-call(s32[1]{0:T(128)} %bitcast.refs_0_, f32[1,512]{1,0:T(1,128)} %bitcast.11, f32[1,512]{1,0:T(1,128)} %bitcast.12, bf16[512,768]{1,0:T(8,128)(2,1)} %refs_3_.2, bf16[2048,128]{1,0:T(8,128)(2,1)} %refs_4_.1, ...), custom_call_target="tpu_custom_call" | custom-call | flops 2000000 | tf_op jit(solution)/shard_map/pallas_call | solution.py:59
  39.0 2.6 %all-to-all-start = ((bf16[32,2,768]{2,1,0:T(2,128)(2,1)}), bf16[32,2,768]{2,1,0:T(2,128)(2,1)S(1)}, u32[]{:S(2)}, u32[]{:S(2)}) async-start(bf16[32,2,768]{2,1,0:T(2,128)(2,1)} %get-tuple-element.18), calls=%async_computation | async-start | bytes 196608 | tf_op jit(solution)/shard_map/all_to_all | solution.py:389
  41.6 1.7 %collective-permute-start.5 = (bf16[30,2048]{1,0:T(8,128)(2,1)S(1)}, bf16[30,2048]{1,0:T(8,128)(2,1)}, u32[]{:S(2)}, u32[]{:S(2)}) collective-permute-start(bf16[30,2048]{1,0:T(8,128)(2,1)S(1)} %collective-permute-done.1.refs_5_), channel_id=1, source_target_pairs={{0,1},{1,0},{2,3},{3,2},{4,5},{5,4},{6,7},{7,6},{8,9},{9,8},{10,11... | collective-permute-start | bytes 368648 | tf_op jit(solution)/shard_map/ppermute | solution.py:362
  43.7 1.6 %collective-permute-start.6 = (bf16[30,2048]{1,0:T(8,128)(2,1)}, bf16[30,2048]{1,0:T(8,128)(2,1)}, u32[]{:S(2)}, u32[]{:S(2)}) collective-permute-start(bf16[30,2048]{1,0:T(8,128)(2,1)} %collective-permute-done.2.refs_6_), channel_id=1, source_target_pairs={{0,1},{1,0},{2,3},{3,2},{4,5},{5,4},{6,7},{7,6},{8,9},{9,8},{10,11... | collective-permute-start | bytes 368648 | tf_op jit(solution)/shard_map/ppermute | solution.py:362
  46.2 3.0 %all-to-all-done.refs_0_ = bf16[32,2,768]{2,1,0:T(2,128)(2,1)S(1)} async-done(((bf16[32,2,768]{2,1,0:T(2,128)(2,1)}), bf16[32,2,768]{2,1,0:T(2,128)(2,1)S(1)}, u32[]{:S(2)}, u32[]{:S(2)}) %all-to-all-start) | async-done | bytes 98336 | tf_op jit(solution)/shard_map/all_to_all | solution.py:389
  49.2 1.8 %shard_map.101 = (f32[2,6144]{1,0:T(2,128)S(1)}, bf16[192,256]{1,0:T(8,128)(2,1)S(1)}) custom-call(bf16[32,2,768]{2,1,0:T(2,128)(2,1)S(1)} %all-to-all-done.refs_0_, bf16[192,2048]{1,0:T(8,128)(2,1)} %refs_1_.1, bf16[2048,384]{1,0:T(8,128)(2,1)S(1)} %get-tuple-element.19.refs_2_), custom_call_target="tpu_custom_call" | custom-call | flops 2000000 | tf_op jit(solution)/shard_map/pallas_call | solution.py:59
  51.7 2.1 %collective-permute-done.6.refs_10_ = bf16[30,2048]{1,0:T(8,128)(2,1)} collective-permute-done((bf16[30,2048]{1,0:T(8,128)(2,1)}, bf16[30,2048]{1,0:T(8,128)(2,1)}, u32[]{:S(2)}, u32[]{:S(2)}) %collective-permute-start.6) | collective-permute-done | bytes 122912 | tf_op jit(solution)/shard_map/ppermute | solution.py:362
  53.9 2.3 %shard_map.102 = (bf16[2,128,128]{2,1,0:T(8,128)(2,1)S(1)}, bf16[256,256]{1,0:T(8,128)(2,1)S(1)}) custom-call(f32[2,6144]{1,0:T(2,128)S(1)} %get-tuple-element.20.refs_0_.refs_1_, f32[2,2,128,128]{3,2,1,0:T(8,128)S(1)} %copy-done.2, bf16[2048,384]{1,0:T(8,128)(2,1)S(1)} %get-tuple-element.19.refs_2_, bf16[30,2048]{1,0:T(8,128)(2,1)S(1)} %copy-done, ...), custom_call_target="tpu_custom_call" | custom-call | flops 2000000 | tf_op jit(solution)/shard_map/pallas_call | solution.py:59
  56.2 1.7 %collective-permute-start.14 = (bf16[256,256]{1,0:T(8,128)(2,1)S(1)}, bf16[256,256]{1,0:T(8,128)(2,1)S(1)}, u32[]{:S(2)}, u32[]{:S(2)}) collective-permute-start(bf16[256,256]{1,0:T(8,128)(2,1)S(1)} %get-tuple-element.23.refs_2_), channel_id=1, source_target_pairs={{0,16},{8,24},{16,0},{24,8},{1,17},{9,25},{17,1},{25,9},{2,18},{10... | collective-permute-start | bytes 393224 | tf_op jit(solution)/shard_map/ppermute | solution.py:431
  58.3 3.9 %collective-permute-done.14.refs_5_ = bf16[256,256]{1,0:T(8,128)(2,1)S(1)} collective-permute-done((bf16[256,256]{1,0:T(8,128)(2,1)S(1)}, bf16[256,256]{1,0:T(8,128)(2,1)S(1)}, u32[]{:S(2)}, u32[]{:S(2)}) %collective-permute-start.14) | collective-permute-done | bytes 131104 | tf_op jit(solution)/shard_map/ppermute | solution.py:431
  64.5 1.8 %shard_map.103 = (f32[2,2,128,1]{3,2,1,0:T(8,128)S(1)}, f32[2,2,128,1]{3,2,1,0:T(8,128)S(1)}, f32[2,2,128,128]{3,2,1,0:T(8,128)S(1)}, bf16[128,2048]{1,0:T(8,128)(2,1)S(1)}) custom-call(bf16[128,2048]{1,0:T(8,128)(2,1)} %refs_0_.3, bf16[2,128,128]{2,1,0:T(8,128)(2,1)S(1)} %get-tuple-element.22.refs_1_.refs_4_, ...), custom_call_target="tpu_custom_call" | custom-call | flops 2000000 | tf_op jit(solution)/shard_map/pallas_call | solution.py:59
  66.3 1.7 %shard_map.104 = bf16[4,2,32,128]{3,2,1,0:T(8,128)(2,1)S(1)} custom-call(f32[1]{0:T(128)S(6)} %copy.11.refs_0_, f32[2,2,128,1]{3,2,1,0:T(8,128)S(1)} %get-tuple-element.26.refs_1_, f32[2,2,128,1]{3,2,1,0:T(8,128)S(1)} %get-tuple-element.27.refs_2_, f32[2,2,128,128]{3,2,1,0:T(8,128)S(1)} %get-tuple-element.28.refs_3_, ...), custom_call_target="tpu_custom_call" | custom-call | flops 2000000 | tf_op jit(solution)/shard_map/pallas_call | solution.py:59
  68.0 1.8 %collective-permute-start.16 = (bf16[2,32,128]{2,1,0:T(8,128)(2,1)S(1)}, bf16[2,32,128]{2,1,0:T(8,128)(2,1)S(1)}, u32[]{:S(2)}, u32[]{:S(2)}) collective-permute-start(bf16[2,32,128]{2,1,0:T(8,128)(2,1)S(1)} %get-tuple-element.33), channel_id=1, source_target_pairs={{0,2},{1,3},{2,0},{3,1},{4,6},{5,7},{6,4},{7,5},{8,10},{9,11},{10,... | collective-permute-start | bytes 49160 | tf_op jit(solution)/shard_map/ppermute | solution.py:354
  69.8 2.6 %collective-permute-start.17 = (bf16[2,32,128]{2,1,0:T(8,128)(2,1)S(1)}, bf16[2,32,128]{2,1,0:T(8,128)(2,1)S(1)}, u32[]{:S(2)}, u32[]{:S(2)}) collective-permute-start(bf16[2,32,128]{2,1,0:T(8,128)(2,1)S(1)} %get-tuple-element.32), channel_id=1, source_target_pairs={{0,4},{1,5},{2,6},{3,7},{4,0},{5,1},{6,2},{7,3},{8,12},{9,13},{10,... | collective-permute-start | bytes 49160 | tf_op jit(solution)/shard_map/ppermute | solution.py:354
  72.5 2.0 %collective-permute-done.17.refs_7_ = bf16[2,32,128]{2,1,0:T(8,128)(2,1)S(1)} collective-permute-done((bf16[2,32,128]{2,1,0:T(8,128)(2,1)S(1)}, bf16[2,32,128]{2,1,0:T(8,128)(2,1)S(1)}, u32[]{:S(2)}, u32[]{:S(2)}) %collective-permute-start.17) | collective-permute-done | bytes 16416 | tf_op jit(solution)/shard_map/ppermute | solution.py:354
  74.5 3.5 %collective-permute-done.18.refs_8_ = bf16[2,32,128]{2,1,0:T(8,128)(2,1)S(1)} collective-permute-done((bf16[2,32,128]{2,1,0:T(8,128)(2,1)S(1)}, bf16[2,32,128]{2,1,0:T(8,128)(2,1)S(1)}, u32[]{:S(2)}, u32[]{:S(2)}) %collective-permute-start.18) | collective-permute-done | bytes 16416 | tf_op jit(solution)/shard_map/ppermute | solution.py:354
  79.1 4.4 %collective-permute-done.19.refs_3_ = bf16[32,2048]{1,0:T(8,128)(2,1)S(1)} collective-permute-done((bf16[32,2048]{1,0:T(8,128)(2,1)S(1)}, bf16[32,2048]{1,0:T(8,128)(2,1)S(1)}, u32[]{:S(2)}, u32[]{:S(2)}) %collective-permute-start.19) | collective-permute-done | bytes 131104 | tf_op jit(solution)/shard_map/ppermute | solution.py:362
  (33 shorter events, 6.9 us)
Async XLA Ops:
  0.0 15.8 %collective-permute-start.11 = (bf16[128,2048]{1,0:T(8,128)(2,1)}, bf16[128,2048]{1,0:T(8,128)(2,1)S(1)}, u32[]{:S(2)}, u32[]{:S(2)}) collective-permute-start(bf16[128,2048]{1,0:T(8,128)(2,1)} %refs_0_.3), channel_id=1, source_target_pairs={{0,4},{1,5},{2,6},{3,7},{4,0},{5,1},{6,2},{7,3},{8,10},{9,11},{10,... | collective-permute-start | bytes 1572872 | tf_op jit(solution)/shard_map/ppermute | solution.py:495
  15.8 29.5 %collective-permute-start.12 = (bf16[128,2048]{1,0:T(8,128)(2,1)S(1)}, bf16[128,2048]{1,0:T(8,128)(2,1)S(1)}, u32[]{:S(2)}, u32[]{:S(2)}) collective-permute-start(bf16[128,2048]{1,0:T(8,128)(2,1)S(1)} %collective-permute-done.11.refs_2_), channel_id=1, source_target_pairs={{0,10},{1,11},{2,8},{3,9},{4,14},{5,15},{6,12},{7,13},{8,0},{9,1},... | collective-permute-start | bytes 1572872 | tf_op jit(solution)/shard_map/ppermute | solution.py:495
  15.8 11.9 %collective-permute-start.1 = (bf16[30,2048]{1,0:T(8,128)(2,1)}, bf16[30,2048]{1,0:T(8,128)(2,1)S(1)}, u32[]{:S(2)}, u32[]{:S(2)}) collective-permute-start(bf16[30,2048]{1,0:T(8,128)(2,1)} %refs_0_.4), channel_id=1, source_target_pairs={{0,4},{1,5},{2,6},{3,7},{4,0},{5,1},{6,2},{7,3},{8,12},{9,13},{10,... | collective-permute-start | bytes 368648 | tf_op jit(solution)/shard_map/ppermute | solution.py:354
  17.9 25.4 %collective-permute-start = (bf16[30,2048]{1,0:T(8,128)(2,1)}, bf16[30,2048]{1,0:T(8,128)(2,1)}, u32[]{:S(2)}, u32[]{:S(2)}) collective-permute-start(bf16[30,2048]{1,0:T(8,128)(2,1)} %refs_0_.4), channel_id=1, source_target_pairs={{0,2},{1,3},{2,0},{3,1},{4,6},{5,7},{6,4},{7,5},{8,10},{9,11},{10,... | collective-permute-start | bytes 368648 | tf_op jit(solution)/shard_map/ppermute | solution.py:354
  27.7 16.0 %collective-permute-start.2 = (bf16[30,2048]{1,0:T(8,128)(2,1)S(1)}, bf16[30,2048]{1,0:T(8,128)(2,1)}, u32[]{:S(2)}, u32[]{:S(2)}) collective-permute-start(bf16[30,2048]{1,0:T(8,128)(2,1)S(1)} %collective-permute-done.1.refs_5_), channel_id=1, source_target_pairs={{0,2},{1,3},{2,0},{3,1},{4,6},{5,7},{6,4},{7,5},{8,10},{9,11},{10,... | collective-permute-start | bytes 368648 | tf_op jit(solution)/shard_map/ppermute | solution.py:354
  34.3 16.7 %collective-permute-start.3 = (bf16[30,2048]{1,0:T(8,128)(2,1)}, bf16[30,2048]{1,0:T(8,128)(2,1)}, u32[]{:S(2)}, u32[]{:S(2)}) collective-permute-start(bf16[30,2048]{1,0:T(8,128)(2,1)} %refs_0_.4), channel_id=1, source_target_pairs={{0,1},{1,0},{2,3},{3,2},{4,5},{5,4},{6,7},{7,6},{8,9},{9,8},{10,11... | collective-permute-start | bytes 368648 | tf_op jit(solution)/shard_map/ppermute | solution.py:362
  38.3 0.7 copy-start.1
  39.0 10.2 %all-to-all-start = ((bf16[32,2,768]{2,1,0:T(2,128)(2,1)}), bf16[32,2,768]{2,1,0:T(2,128)(2,1)S(1)}, u32[]{:S(2)}, u32[]{:S(2)}) async-start(bf16[32,2,768]{2,1,0:T(2,128)(2,1)} %get-tuple-element.18), calls=%async_computation | async-start | bytes 196608 | tf_op jit(solution)/shard_map/all_to_all | solution.py:389
  41.6 9.4 %collective-permute-start.5 = (bf16[30,2048]{1,0:T(8,128)(2,1)S(1)}, bf16[30,2048]{1,0:T(8,128)(2,1)}, u32[]{:S(2)}, u32[]{:S(2)}) collective-permute-start(bf16[30,2048]{1,0:T(8,128)(2,1)S(1)} %collective-permute-done.1.refs_5_), channel_id=1, source_target_pairs={{0,1},{1,0},{2,3},{3,2},{4,5},{5,4},{6,7},{7,6},{8,9},{9,8},{10,11... | collective-permute-start | bytes 368648 | tf_op jit(solution)/shard_map/ppermute | solution.py:362
  43.3 8.4 %collective-permute-start.4 = (bf16[30,2048]{1,0:T(8,128)(2,1)}, bf16[30,2048]{1,0:T(8,128)(2,1)}, u32[]{:S(2)}, u32[]{:S(2)}) collective-permute-start(bf16[30,2048]{1,0:T(8,128)(2,1)} %collective-permute-done.refs_4_), channel_id=1, source_target_pairs={{0,1},{1,0},{2,3},{3,2},{4,5},{5,4},{6,7},{7,6},{8,9},{9,8},{10,11... | collective-permute-start | bytes 368648 | tf_op jit(solution)/shard_map/ppermute | solution.py:362
  43.7 10.2 %collective-permute-start.6 = (bf16[30,2048]{1,0:T(8,128)(2,1)}, bf16[30,2048]{1,0:T(8,128)(2,1)}, u32[]{:S(2)}, u32[]{:S(2)}) collective-permute-start(bf16[30,2048]{1,0:T(8,128)(2,1)} %collective-permute-done.2.refs_6_), channel_id=1, source_target_pairs={{0,1},{1,0},{2,3},{3,2},{4,5},{5,4},{6,7},{7,6},{8,9},{9,8},{10,11... | collective-permute-start | bytes 368648 | tf_op jit(solution)/shard_map/ppermute | solution.py:362
  46.2 7.7 %copy-start = (bf16[30,2048]{1,0:T(8,128)(2,1)S(1)}, bf16[30,2048]{1,0:T(8,128)(2,1)}, u32[]{:S(2)}) copy-start(bf16[30,2048]{1,0:T(8,128)(2,1)} %refs_0_.4) | copy-start | bytes 368644
  46.2 31.7 %collective-permute-start.13 = (bf16[128,2048]{1,0:T(8,128)(2,1)}, bf16[128,2048]{1,0:T(8,128)(2,1)S(1)}, u32[]{:S(2)}, u32[]{:S(2)}) collective-permute-start(bf16[128,2048]{1,0:T(8,128)(2,1)} %broadcast_select_fusion), channel_id=1, source_target_pairs={{0,8},{8,0},{16,24},{24,16},{1,9},{9,1},{17,25},{25,17},{2,10},{10... | collective-permute-start | bytes 1572872 | tf_op jit(solution)/shard_map/ppermute | solution.py:502
  49.2 4.7 %copy-start.2 = (f32[2,2,128,128]{3,2,1,0:T(8,128)S(1)}, f32[2,2,128,128]{3,2,1,0:T(8,128)}, u32[]{:S(2)}) copy-start(f32[2,2,128,128]{3,2,1,0:T(8,128)} %copy-done.1) | copy-start | bytes 786436
  56.2 6.0 %collective-permute-start.14 = (bf16[256,256]{1,0:T(8,128)(2,1)S(1)}, bf16[256,256]{1,0:T(8,128)(2,1)S(1)}, u32[]{:S(2)}, u32[]{:S(2)}) collective-permute-start(bf16[256,256]{1,0:T(8,128)(2,1)S(1)} %get-tuple-element.23.refs_2_), channel_id=1, source_target_pairs={{0,16},{8,24},{16,0},{24,8},{1,17},{9,25},{17,1},{25,9},{2,18},{10... | collective-permute-start | bytes 393224 | tf_op jit(solution)/shard_map/ppermute | solution.py:431
  57.9 5.3 %collective-permute-start.8 = (bf16[192,256]{1,0:T(8,128)(2,1)S(1)}, bf16[192,256]{1,0:T(8,128)(2,1)S(1)}, u32[]{:S(2)}, u32[]{:S(2)}) collective-permute-start(bf16[192,256]{1,0:T(8,128)(2,1)S(1)} %get-tuple-element.24.refs_4_), channel_id=1, source_target_pairs={{0,16},{8,24},{16,0},{24,8},{1,17},{9,25},{17,1},{25,9},{2,18},{10... | collective-permute-start | bytes 294920 | tf_op jit(solution)/shard_map/ppermute | solution.py:431
  58.3 6.2 %collective-permute-start.7 = (bf16[256,256]{1,0:T(8,128)(2,1)S(1)}, bf16[256,256]{1,0:T(8,128)(2,1)S(1)}, u32[]{:S(2)}, u32[]{:S(2)}) collective-permute-start(bf16[256,256]{1,0:T(8,128)(2,1)S(1)} %get-tuple-element.23.refs_2_), channel_id=1, source_target_pairs={{0,8},{8,0},{16,24},{24,16},{1,9},{9,1},{17,25},{25,17},{2,10},{10... | collective-permute-start | bytes 393224 | tf_op jit(solution)/shard_map/ppermute | solution.py:441
  62.2 4.1 %collective-permute-start.15 = (bf16[256,256]{1,0:T(8,128)(2,1)S(1)}, bf16[256,256]{1,0:T(8,128)(2,1)S(1)}, u32[]{:S(2)}, u32[]{:S(2)}) collective-permute-start(bf16[256,256]{1,0:T(8,128)(2,1)S(1)} %collective-permute-done.14.refs_5_), channel_id=1, source_target_pairs={{0,8},{8,0},{16,24},{24,16},{1,9},{9,1},{17,25},{25,17},{2,10},{10... | collective-permute-start | bytes 393224 | tf_op jit(solution)/shard_map/ppermute | solution.py:441
  62.2 1.7 %collective-permute-start.9 = (bf16[192,256]{1,0:T(8,128)(2,1)S(1)}, bf16[192,256]{1,0:T(8,128)(2,1)S(1)}, u32[]{:S(2)}, u32[]{:S(2)}) collective-permute-start(bf16[192,256]{1,0:T(8,128)(2,1)S(1)} %get-tuple-element.24.refs_4_), channel_id=1, source_target_pairs={{0,8},{8,0},{16,24},{24,16},{1,9},{9,1},{17,25},{25,17},{2,10},{10... | collective-permute-start | bytes 294920 | tf_op jit(solution)/shard_map/ppermute | solution.py:441
  63.2 1.3 %collective-permute-start.10 = (bf16[192,256]{1,0:T(8,128)(2,1)S(1)}, bf16[192,256]{1,0:T(8,128)(2,1)S(1)}, u32[]{:S(2)}, u32[]{:S(2)}) collective-permute-start(bf16[192,256]{1,0:T(8,128)(2,1)S(1)} %collective-permute-done.8.refs_5_), channel_id=1, source_target_pairs={{0,8},{8,0},{16,24},{24,16},{1,9},{9,1},{17,25},{25,17},{2,10},{10... | collective-permute-start | bytes 294920 | tf_op jit(solution)/shard_map/ppermute | solution.py:441
  68.0 4.5 %collective-permute-start.16 = (bf16[2,32,128]{2,1,0:T(8,128)(2,1)S(1)}, bf16[2,32,128]{2,1,0:T(8,128)(2,1)S(1)}, u32[]{:S(2)}, u32[]{:S(2)}) collective-permute-start(bf16[2,32,128]{2,1,0:T(8,128)(2,1)S(1)} %get-tuple-element.33), channel_id=1, source_target_pairs={{0,2},{1,3},{2,0},{3,1},{4,6},{5,7},{6,4},{7,5},{8,10},{9,11},{10,... | collective-permute-start | bytes 49160 | tf_op jit(solution)/shard_map/ppermute | solution.py:354
  69.8 4.6 %collective-permute-start.17 = (bf16[2,32,128]{2,1,0:T(8,128)(2,1)S(1)}, bf16[2,32,128]{2,1,0:T(8,128)(2,1)S(1)}, u32[]{:S(2)}, u32[]{:S(2)}) collective-permute-start(bf16[2,32,128]{2,1,0:T(8,128)(2,1)S(1)} %get-tuple-element.32), channel_id=1, source_target_pairs={{0,4},{1,5},{2,6},{3,7},{4,0},{5,1},{6,2},{7,3},{8,12},{9,13},{10,... | collective-permute-start | bytes 49160 | tf_op jit(solution)/shard_map/ppermute | solution.py:354
  72.4 5.5 %collective-permute-start.18 = (bf16[2,32,128]{2,1,0:T(8,128)(2,1)S(1)}, bf16[2,32,128]{2,1,0:T(8,128)(2,1)S(1)}, u32[]{:S(2)}, u32[]{:S(2)}) collective-permute-start(bf16[2,32,128]{2,1,0:T(8,128)(2,1)S(1)} %get-tuple-element.31), channel_id=1, source_target_pairs={{0,6},{1,7},{2,4},{3,5},{4,2},{5,3},{6,0},{7,1},{8,14},{9,15},{10,... | collective-permute-start | bytes 49160 | tf_op jit(solution)/shard_map/ppermute | solution.py:354
  78.4 5.0 %collective-permute-start.19 = (bf16[32,2048]{1,0:T(8,128)(2,1)S(1)}, bf16[32,2048]{1,0:T(8,128)(2,1)S(1)}, u32[]{:S(2)}, u32[]{:S(2)}) collective-permute-start(bf16[32,2048]{1,0:T(8,128)(2,1)S(1)} %get-tuple-element.30), channel_id=1, source_target_pairs={{0,1},{1,0},{2,3},{3,2},{4,5},{5,4},{6,7},{7,6},{8,9},{9,8},{10,11... | collective-permute-start | bytes 393224 | tf_op jit(solution)/shard_map/ppermute | solution.py:362
